TPU v7x, 32 devices: a whole 2x2x4 slice. The times are simulated.
32 devices in a mesh: kv: 8 (over z, y), tp: 4 (over x, core).
Axes of the slice: x: 2, y: 2, z: 4, core: 2. Of those that a mesh axis runs over, the one named last changes fastest.
Arguments:
- tokens: bfloat16 [5120, 4096], P('kv'), may hold values from -48 to 48
- query_weight: bfloat16 [4096, 2048], P(None, 'tp'), may hold values from -0.09375 to 0.09375
- key_weight: bfloat16 [4096, 512], P(None, 'tp'), may hold values from -0.09375 to 0.09375
- value_weight: bfloat16 [4096, 512], P(None, 'tp'), may hold values from -0.09375 to 0.09375
- gate_weight: bfloat16 [4096, 64], replicated, may hold values from -0.09375 to 0.09375
- summary_pos: bfloat16 [32, 64], replicated, may hold values from -6 to 6
- key_mixing: bfloat16 [32, 8], replicated, may hold values from -1 to 1
- value_mixing: bfloat16 [32, 8], replicated, may hold values from -1 to 1
- out_weight: bfloat16 [2048, 4096], P('tp'), may hold values from -0.125 to 0.125
- chosen: int32 [80, 8, 16], P('kv', 'tp'), may hold values from 0 to 79, as said below
Outputs:
- mixed: bfloat16 [5120, 4096], P(('kv', 'tp'))
Inputs may be any that keep to these rules, and one draw needn't show every extreme that they name: `chosen`: entry [b, g, 0] is b itself; every entry is at most b. For the query blocks of one index of kv, one key head and any OTHER index of kv, at most 2 distinct blocks of that index's 64-position blocks are named, and exactly 2 of the index just before. Entries may repeat.
All inputs are finite; a program needn't handle non-finite values.
Results may differ from a plain program's by a relative error of at most 0.013.
The roundings to bfloat16 on the way count: a program that leaves them out, or rounds other values in their place, can miss the bound.
Values may be sent and summed in bfloat16 or wider, within the bound.
No kernel may reach another device: no remote copies, remote signals or barrier semaphores. Data moves between devices by JAX's collectives and lax.ppermute only.
A program may use at most 192 MiB of HBM per device.

v0:
```python
import functools

import jax
import jax.numpy as jnp
from jax import lax
from jax.experimental import pallas as pl
from jax.experimental.pallas import tpu as pltpu
from jax.sharding import PartitionSpec as P


HD = 64
CMP = 32
SB = 64
N_SEL = 16
LANES = 2 * HD
SPAN_PAD = 32
CHUNKS = 4
LOW = -1e30
FLOOR = -1e29
EXP_SCALE = HD ** (-0.5) * 1.4426950408889634
VMEM_LIMIT = 56 * 1024 * 1024


F32 = jnp.float32
BF16 = jnp.bfloat16


def lane_iota(rows):
    return lax.broadcasted_iota(jnp.int32, (rows, LANES), 1)


def row_iota(rows):
    return lax.broadcasted_iota(jnp.int32, (rows, LANES), 0)


def kv_kernel(part_ref, tok_ref, wk_ref, wv_ref, pos_ref, km_ref, vm_ref, kv_ref, sm_ref, acc_ref):
    step = pl.program_id(0)
    weight = jnp.concatenate([wk_ref[...], wv_ref[...]], axis=1)
    piece = jnp.dot(tok_ref[...], weight, preferred_element_type=F32)

    @pl.when(step == 0)
    def _():
        acc_ref[...] = piece

    @pl.when(step > 0)
    def _():
        acc_ref[...] += piece

    @pl.when(step == pl.num_programs(0) - 1)
    def _():
        heads, rows = kv_ref.shape[0], kv_ref.shape[1]
        spans = rows // CMP
        low_half = lane_iota(rows) < HD
        pos = pos_ref[...].astype(F32)
        pos = jnp.concatenate([pos, pos], axis=1)
        columns = lax.broadcasted_iota(jnp.int32, km_ref.shape, 1)
        for g in range(heads):
            pair = g // 2
            k = acc_ref[:, pair * LANES : (pair + 1) * LANES]
            v = acc_ref[:, (heads // 2 + pair) * LANES : (heads // 2 + pair + 1) * LANES]
            if g % 2 == 0:
                both = jnp.where(low_half, k, pltpu.roll(v, HD, 1))
            else:
                both = jnp.where(low_half, pltpu.roll(k, HD, 1), v)
            both = both.astype(BF16)
            kv_ref[g] = both
            mine = columns == part_ref[0] * heads + g
            kmix = jnp.sum(jnp.where(mine, km_ref[...].astype(F32), 0.0), axis=1, keepdims=True)
            vmix = jnp.sum(jnp.where(mine, vm_ref[...].astype(F32), 0.0), axis=1, keepdims=True)
            mix = jnp.where(lane_iota(CMP) < HD, kmix, vmix)
            windows = both.astype(F32).reshape(spans, CMP, LANES) + pos[None]
            total = jnp.sum(windows * mix[None], axis=1)
            pad = jnp.zeros((SPAN_PAD - spans, LANES), F32)
            sm_ref[g] = jnp.concatenate([total, pad], axis=0).astype(BF16)


def project_kv(part, tokens, key_weight, value_weight, pos, kmix, vmix):
    rows, depth = tokens.shape
    width = key_weight.shape[1]
    heads = width // HD
    chunk = depth // 4
    full = lambda shape: pl.BlockSpec(shape, lambda i, s: (0,) * len(shape))
    return pl.pallas_call(
        kv_kernel,
        grid_spec=pltpu.PrefetchScalarGridSpec(
            num_scalar_prefetch=1,
            grid=(depth // chunk,),
            in_specs=[
                pl.BlockSpec((rows, chunk), lambda i, s: (0, i)),
                pl.BlockSpec((chunk, width), lambda i, s: (i, 0)),
                pl.BlockSpec((chunk, width), lambda i, s: (i, 0)),
                full(pos.shape),
                full(kmix.shape),
                full(vmix.shape),
            ],
            out_specs=[full((heads, rows, LANES)), full((heads, SPAN_PAD, LANES))],
            scratch_shapes=[pltpu.VMEM((rows, 2 * width), F32)],
        ),
        out_shape=[
            jax.ShapeDtypeStruct((heads, rows, LANES), BF16),
            jax.ShapeDtypeStruct((heads, SPAN_PAD, LANES), BF16),
        ],
        cost_estimate=pl.CostEstimate(
            flops=4 * rows * depth * width, transcendentals=0, bytes_accessed=2 * depth * (rows + 2 * width)
        ),
        compiler_params=pltpu.CompilerParams(vmem_limit_bytes=VMEM_LIMIT),
        name="kv_proj",
    )(part, tokens, key_weight, value_weight, pos, kmix, vmix)


def q_kernel(part_ref, tok_ref, wq_ref, gw_ref, q_ref, gate_ref, acc_ref, gacc_ref):
    step = pl.program_id(0)
    gates = gate_ref.shape[1]
    start = pl.multiple_of(part_ref[0] * gates, gates)
    gate_rows = gw_ref[pl.ds(start, gates), :]
    piece = jnp.dot(tok_ref[...], wq_ref[...], preferred_element_type=F32)
    gpiece = lax.dot_general(tok_ref[...], gate_rows, (((1,), (1,)), ((), ())), preferred_element_type=F32)

    @pl.when(step == 0)
    def _():
        acc_ref[...] = piece
        gacc_ref[...] = gpiece

    @pl.when(step > 0)
    def _():
        acc_ref[...] += piece
        gacc_ref[...] += gpiece

    @pl.when(step == pl.num_programs(0) - 1)
    def _():
        heads, rows = q_ref.shape[0], q_ref.shape[1]
        lane, inner = lane_iota(rows), lax.rem(row_iota(rows), SB)
        low_half = lane < HD
        ext = jnp.where((lane == HD) | (lane - HD > inner), 1.0, 0.0)
        for h in range(heads):
            slab = acc_ref[:, (h // 2) * LANES : (h // 2 + 1) * LANES]
            if h % 2:
                slab = pltpu.roll(slab, HD, 1)
            q_ref[h] = jnp.where(low_half, slab, ext).astype(BF16)
        gate_ref[...] = jax.nn.sigmoid(gacc_ref[...])


def project_q(part, tokens, query_weight, gate_rows):
    rows, depth = tokens.shape
    width = query_weight.shape[1]
    heads = width // HD
    chunk = depth // 4
    return pl.pallas_call(
        q_kernel,
        grid_spec=pltpu.PrefetchScalarGridSpec(
            num_scalar_prefetch=1,
            grid=(depth // chunk,),
            in_specs=[
                pl.BlockSpec((rows, chunk), lambda i, s: (0, i)),
                pl.BlockSpec((chunk, width), lambda i, s: (i, 0)),
                pl.BlockSpec((gate_rows.shape[0], chunk), lambda i, s: (0, i)),
            ],
            out_specs=[
                pl.BlockSpec((heads, rows, LANES), lambda i, s: (0, 0, 0)),
                pl.BlockSpec((rows, 2 * heads), lambda i, s: (0, 0)),
            ],
            scratch_shapes=[pltpu.VMEM((rows, width), F32), pltpu.VMEM((rows, 2 * heads), F32)],
        ),
        out_shape=[
            jax.ShapeDtypeStruct((heads, rows, LANES), BF16),
            jax.ShapeDtypeStruct((rows, 2 * heads), F32),
        ],
        cost_estimate=pl.CostEstimate(
            flops=3 * rows * depth * width, transcendentals=0, bytes_accessed=2 * depth * (rows + width)
        ),
        compiler_params=pltpu.CompilerParams(vmem_limit_bytes=VMEM_LIMIT),
        name="q_proj",
    )(part, tokens, query_weight, gate_rows)


def select_kernel(count, own_ref, req_ref, kv_ref, sm_ref, *out_refs):
    heads = kv_ref.shape[0]
    own = own_ref[0]
    for shift in range(1, count):
        taker = jnp.minimum(own + shift, count - 1)
        out_ref = out_refs[shift - 1]
        for g in range(heads):
            for j in range(2):
                block = req_ref[taker, own * (2 * heads) + 2 * g + j]
                out_ref[g, j * SB : (j + 1) * SB, :] = kv_ref[g, pl.ds(pl.multiple_of(block * SB, SB), SB), :]
            out_ref[g, 2 * SB :, :] = sm_ref[g]


def select_blocks(count, own, requests, kv, summaries):
    heads = kv.shape[0]
    piece = (heads, 2 * SB + SPAN_PAD, LANES)
    vmem = pl.BlockSpec(memory_space=pltpu.VMEM)
    smem = pl.BlockSpec(memory_space=pltpu.SMEM)
    return pl.pallas_call(
        functools.partial(select_kernel, count),
        in_specs=[smem, smem, vmem, vmem],
        out_specs=[vmem] * (count - 1),
        out_shape=[jax.ShapeDtypeStruct(piece, BF16)] * (count - 1),
        compiler_params=pltpu.CompilerParams(vmem_limit_bytes=VMEM_LIMIT),
        name="select_blocks",
    )(own, requests, kv, summaries)


def attn_kernel(count, *refs):
    base_ref, own_ref, table_ref, q_ref, gate_ref, kv_ref, sm_ref = refs[:7]
    recv_refs = refs[7 : 7 + count - 1]
    out_ref, poolk, poolv, sumk, sumv, kbuf, vbuf = refs[7 + count - 1 :]
    step = pl.program_id(0)
    own = own_ref[0]
    block = base_ref[0] + step
    heads, rows = kv_ref.shape[0], kv_ref.shape[1]
    group = q_ref.shape[0] // heads
    own_blocks = rows // SB
    spans = rows // CMP
    total_blocks = poolk.shape[1] - 1
    lane, row = lane_iota(SB), row_iota(SB)
    keep = jnp.where(lane < HD, 1.0, 0.0).astype(BF16)
    other = jnp.where(lane < HD, 0.0, 1.0).astype(BF16)
    span_lane, span_row = lane_iota(SPAN_PAD), row_iota(SPAN_PAD)

    @pl.when(step == 0)
    def _():
        for g in range(heads):
            for j in range(own_blocks):
                piece = kv_ref[g, j * SB : (j + 1) * SB, :]
                poolk[g, j] = piece * keep
                poolv[g, j] = piece * other + keep
            for k, recv in enumerate(recv_refs):
                for j in range(2):
                    piece = recv[g, j * SB : (j + 1) * SB, :]
                    poolk[g, own_blocks + 2 * k + j] = piece * keep
                    poolv[g, own_blocks + 2 * k + j] = piece * other + keep
            poolk[g, total_blocks] = jnp.where(lane == HD, LOW, 0.0).astype(BF16)
            poolv[g, total_blocks] = jnp.zeros((SB, LANES), BF16)
            for k in range(count):
                piece = sm_ref[g] if k == 0 else recv_refs[k - 1][g, 2 * SB :, :]
                sumv[g, k * SPAN_PAD : (k + 1) * SPAN_PAD] = piece * other[:SPAN_PAD] + keep[:SPAN_PAD]
                if k:
                    hidden = (span_lane == HD) & ((span_row >= spans) | (own < k))
                    bias = jnp.where(hidden, LOW, 0.0).astype(BF16)
                    sumk[g, k * SPAN_PAD : (k + 1) * SPAN_PAD] = piece * keep[:SPAN_PAD] + bias

    diagonal = jnp.where((lane - HD == row) & (row > 0), LOW, 0.0).astype(BF16)
    last = SB // CMP * block
    hidden = (span_lane == HD) & (span_row >= last + SB // CMP)
    for j in range(SB // CMP):
        hidden = hidden | ((span_row == last + j) & (span_lane == HD + (j + 1) * CMP - 1))
    bias = jnp.where(hidden, LOW, 0.0).astype(BF16)
    contract = (((1,), (1,)), ((), ()))
    low_half = lane < HD
    for g in range(heads):
        for s in range(N_SEL):
            place = table_ref[block, g * N_SEL + s]
            piece = poolk[g, place]
            if s == 0:
                piece = piece + diagonal
            kbuf[g, s * SB : (s + 1) * SB, :] = piece
            vbuf[g, s * SB : (s + 1) * SB, :] = poolv[g, place]
        sumk[g, 0:SPAN_PAD] = sm_ref[g] * keep[:SPAN_PAD] + bias
        q = q_ref[g * group : (g + 1) * group].reshape(group * SB, LANES)
        score = lax.dot_general(q, kbuf[g], contract, preferred_element_type=F32)
        top = jnp.max(score, axis=1, keepdims=True)
        weight = jnp.exp2((score - top) * EXP_SCALE).astype(BF16)
        picked = jnp.dot(weight, vbuf[g], preferred_element_type=F32)
        score = lax.dot_general(q, sumk[g], contract, preferred_element_type=F32)
        top = jnp.maximum(jnp.max(score, axis=1, keepdims=True), FLOOR)
        weight = jnp.exp2((score - top) * EXP_SCALE).astype(BF16)
        summed = jnp.dot(weight, sumv[g], preferred_element_type=F32)
        for pair in range(group // 2):
            mixed = []
            for r in (2 * pair, 2 * pair + 1):
                h = g * group + r
                a = summed[r * SB : (r + 1) * SB]
                c = picked[r * SB : (r + 1) * SB]
                ca = gate_ref[:, 2 * h : 2 * h + 1] / jnp.maximum(a, 1e-30)
                cc = gate_ref[:, 2 * h + 1 : 2 * h + 2] / c
                if r % 2 == 0:
                    mixed.append(pltpu.roll(a, HD, 1) * ca + pltpu.roll(c, HD, 1) * cc)
                else:
                    mixed.append(a * pltpu.roll(ca, HD, 1) + c * pltpu.roll(cc, HD, 1))
            both = jnp.where(low_half, mixed[0], mixed[1]).astype(BF16)
            at = (g * group) // 2 + pair
            out_ref[:, at * LANES : (at + 1) * LANES] = both


def attend(count, blocks, base, own, table, q, gates, kv, summaries, received):
    heads, rows = kv.shape[0], kv.shape[1]
    total = rows // SB + 2 * (count - 1)
    full = lambda shape: pl.BlockSpec(shape, lambda i, *s: (0,) * len(shape))
    return pl.pallas_call(
        functools.partial(attn_kernel, count),
        grid_spec=pltpu.PrefetchScalarGridSpec(
            num_scalar_prefetch=3,
            grid=(blocks,),
            in_specs=[
                pl.BlockSpec((q.shape[0], SB, LANES), lambda i, base, *s: (0, base[0] + i, 0)),
                pl.BlockSpec((SB, gates.shape[1]), lambda i, base, *s: (base[0] + i, 0)),
                full(kv.shape),
                full(summaries.shape),
                *[full(r.shape) for r in received],
            ],
            out_specs=pl.BlockSpec((SB, q.shape[0] * HD), lambda i, *s: (i, 0)),
            scratch_shapes=[
                pltpu.VMEM((heads, total + 1, SB, LANES), BF16),
                pltpu.VMEM((heads, total + 1, SB, LANES), BF16),
                pltpu.VMEM((heads, count * SPAN_PAD, LANES), BF16),
                pltpu.VMEM((heads, count * SPAN_PAD, LANES), BF16),
                pltpu.VMEM((heads, N_SEL * SB, LANES), BF16),
                pltpu.VMEM((heads, N_SEL * SB, LANES), BF16),
            ],
        ),
        out_shape=jax.ShapeDtypeStruct((blocks * SB, q.shape[0] * HD), BF16),
        cost_estimate=pl.CostEstimate(
            flops=blocks * q.shape[0] * SB * (N_SEL * SB + count * SPAN_PAD) * LANES * 4,
            transcendentals=blocks * q.shape[0] * SB * N_SEL * SB,
            bytes_accessed=4 * kv.size,
        ),
        compiler_params=pltpu.CompilerParams(vmem_limit_bytes=VMEM_LIMIT),
        name="attend",
    )(base, own, table, q, gates, kv, summaries, *received)


def local(count, parts, tokens, query_weight, key_weight, value_weight, gate_weight, summary_pos, key_mixing,
          value_mixing, out_weight, chosen):
    rows = tokens.shape[0]
    own = lax.axis_index("kv").astype(jnp.int32)
    part = lax.axis_index("tp").astype(jnp.int32)
    own_blocks = rows // SB
    heads = key_weight.shape[1] // HD
    own1, part1 = own.reshape(1), part.reshape(1)

    source = chosen // own_blocks
    place = chosen - source * own_blocks
    match = source[None] == jnp.arange(count, dtype=jnp.int32)[:, None, None, None]
    lowest = jnp.min(jnp.where(match, place[None], own_blocks - 1), axis=(1, 3))
    highest = jnp.max(jnp.where(match, place[None], 0), axis=(1, 3))
    request = jnp.stack([lowest, highest], axis=-1).reshape(1, count * heads * 2)
    everyone = jnp.where(jnp.arange(count, dtype=jnp.int32)[:, None] == own, request, 0)
    if count & (count - 1) == 0:
        bit, stage = 1, 0
        while bit < count:
            got = lax.ppermute(everyone, "kv", [(i, i ^ bit) for i in range(count)])
            everyone = everyone + got
            if stage == 0:
                chosen = lax.optimization_barrier((chosen, got))[0]
            bit, stage = 2 * bit, stage + 1
    else:
        everyone = lax.all_gather(request, "kv", axis=0, tiled=True)

    kv, summaries = project_kv(part1, tokens, key_weight, value_weight, summary_pos, key_mixing, value_mixing)
    q, gates = project_q(part1, tokens, query_weight, gate_weight.T)

    pieces = select_blocks(count, own1, everyone, kv, summaries)
    received = []
    for k in range(1, count):
        received.append(lax.ppermute(pieces[k - 1], "kv", [(i, i + k) for i in range(count - k)]))

    source = chosen // own_blocks
    place = chosen - source * own_blocks
    match = source[None] == jnp.arange(count, dtype=jnp.int32)[:, None, None, None]

    high_at = jnp.sum(jnp.where(match, highest[:, None, :, None], 0), axis=0)
    away = own_blocks + 2 * (own - source - 1) + (place == high_at).astype(jnp.int32)
    index = jnp.where(source == own, place, away)
    slots = jnp.arange(N_SEL, dtype=jnp.int32)
    earlier = slots[None, :] < slots[:, None]
    repeated = jnp.any((chosen[..., :, None] == chosen[..., None, :]) & earlier, axis=-1)
    first = jnp.logical_not(repeated)
    rank = jnp.sum((first[..., None, :] & earlier).astype(jnp.int32), axis=-1)
    at = (rank[..., None, :] == slots[:, None]) & first[..., None, :]
    fill = own_blocks + 2 * (count - 1)
    table = jnp.where(jnp.any(at, axis=-1), jnp.sum(jnp.where(at, index[..., None, :], 0), axis=-1), fill)
    table = table.reshape(own_blocks, heads * N_SEL)

    half_blocks = own_blocks // 2
    half = part // 2
    core = part % 2
    third = rows // parts

    def halves(which):
        return attend(count, half_blocks, (which * half_blocks).reshape(1), own1, table, q, gates, kv, summaries,
                      received)

    def product(att, columns):
        return jnp.dot(att, columns, preferred_element_type=F32).astype(BF16)

    def rows_of(att, which):
        return lax.dynamic_slice_in_dim(att, which * third, third, 0)

    swap = [(i, i ^ 1) for i in range(parts)]
    cross = [(i, i ^ 2) for i in range(parts)]
    width = out_weight.shape[1] // CHUNKS
    far = halves(1 - half)
    far_keep, far_send = rows_of(far, core), rows_of(far, 1 - core)
    crossed = []
    for c in range(CHUNKS):
        columns = out_weight[:, c * width : (c + 1) * width]
        piece = product(far_send, columns)
        got = lax.ppermute(piece, "tp", swap)
        kept = product(far_keep, columns)
        both = (got.astype(F32) + kept.astype(F32)).astype(BF16)
        crossed.append(lax.ppermute(both, "tp", cross))
    near = halves(half)
    got = lax.ppermute(product(rows_of(near, 1 - core), out_weight), "tp", swap)
    kept = product(rows_of(near, core), out_weight)
    base = got.astype(F32) + kept.astype(F32)
    return jnp.concatenate(
        [
            (base[:, c * width : (c + 1) * width] + crossed[c].astype(F32)).astype(BF16)
            for c in range(CHUNKS)
        ],
        axis=1,
    )


def solution(mesh):
    placed = (
        P("kv", None),
        P(None, "tp"),
        P(None, "tp"),
        P(None, "tp"),
        P(),
        P(),
        P(),
        P(),
        P("tp", None),
        P("kv", "tp", None),
    )
    count = mesh.shape["kv"]

    def body(*args):
        return local(count, mesh.shape["tp"], *args)

    return jax.shard_map(
        body, mesh=mesh, in_specs=placed, out_specs=P(("kv", "tp"), None), check_vma=False
    )
```

profile of v0, /device:TPU:0, one launch (start us, length us, event | category | flops | bytes accessed | tf_op | source)
XLA Modules:
  0.0 118.4 jit_solution(11800355801546177905)
XLA Ops:
  1.2 3.0 %collective-permute-start = (s32[8,32]{1,0:T(8,128)S(1)}, s32[8,32]{1,0:T(8,128)S(1)}, u32[]{:S(2)}, u32[]{:S(2)}) collective-permute-start(s32[8,32]{1,0:T(8,128)S(1)} %broadcast_select_fusion.1), channel_id=1, source_target_pairs={{0,4},{4,0},{8,12},{12,8},{16,20},{20,16},{24,28},{28,24},{1,5},{5... | collective-permute-start | bytes 3080 | tf_op jit(solution)/shard_map/ppermute | solution.py:342
  4.2 1.3 %copy.20.km_ref = bf16[32,8]{1,0:T(8,128)(2,1)} copy(bf16[32,8]{0,1:T(8,128)(2,1)} %param.16) | data formatting | bytes 1024 | tf_op args[6]
  5.5 1.4 %copy.21.vm_ref = bf16[32,8]{1,0:T(8,128)(2,1)} copy(bf16[32,8]{0,1:T(8,128)(2,1)} %param.17) | data formatting | bytes 1024 | tf_op args[7]
  6.9 8.9 %q_proj.1 = (bf16[8,640,128]{2,1,0:T(8,128)(2,1)}, f32[640,16]{1,0:T(8,128)}) custom-call(s32[1]{0:T(128)} %bitcast.4.part_ref, bf16[640,4096]{1,0:T(8,128)(2,1)} %tok_ref.3, bf16[4096,512]{1,0:T(8,128)(2,1)} %wq_ref.1, bf16[64,4096]{1,0:T(8,128)(2,1)} %bitcast.11), custom_call_target="tpu_custom_call" | custom-call | flops 4026531840 | bytes 9437184 | tf_op jit(solution)/shard_map/q_proj/pallas_call | solution.py:148
  15.8 5.8 %kv_proj.1 = (bf16[2,640,128]{2,1,0:T(8,128)(2,1)}, bf16[2,32,128]{2,1,0:T(8,128)(2,1)}) custom-call(s32[1]{0:T(128)} %bitcast.4.part_ref, bf16[640,4096]{1,0:T(8,128)(2,1)} %tok_ref.3, bf16[4096,128]{1,0:T(8,128)(2,1)} %wk_ref.1, bf16[4096,128]{1,0:T(8,128)(2,1)} %wv_ref.1, bf16[32,64]{1,0:T(8,128)(2,1)} %pos_ref.1, bf16[32,8]{1,0:T(8,128)(2,1)} %copy.20.km_ref, ...), custom_call_target="tpu_custom_call" | custom-call | flops 1342177280 | bytes 7340032 | tf_op jit(solution)/shard_map/kv_proj/pallas_call | solution.py:83
  22.4 1.6 %collective-permute-start.1 = (s32[8,32]{1,0:T(8,128)S(1)}, s32[8,32]{1,0:T(8,128)S(1)}, u32[]{:S(2)}, u32[]{:S(2)}) collective-permute-start(s32[8,32]{1,0:T(8,128)S(1)} %fusion.58), channel_id=1, source_target_pairs={{0,8},{4,12},{8,0},{12,4},{16,24},{20,28},{24,16},{28,20},{1,9},{5... | collective-permute-start | bytes 3080 | tf_op jit(solution)/shard_map/ppermute | solution.py:342
  24.4 1.6 %collective-permute-done.1 = s32[8,32]{1,0:T(8,128)S(1)} collective-permute-done((s32[8,32]{1,0:T(8,128)S(1)}, s32[8,32]{1,0:T(8,128)S(1)}, u32[]{:S(2)}, u32[]{:S(2)}) %collective-permute-start.1) | collective-permute-done | bytes 1056 | tf_op jit(solution)/shard_map/ppermute | solution.py:342
  26.1 2.6 %collective-permute-start.2 = (s32[8,32]{1,0:T(8,128)S(1)}, s32[8,32]{1,0:T(8,128)S(1)}, u32[]{:S(2)}, u32[]{:S(2)}) collective-permute-start(s32[8,32]{1,0:T(8,128)S(1)} %fusion.61), channel_id=1, source_target_pairs={{0,16},{4,20},{8,24},{12,28},{16,0},{20,4},{24,8},{28,12},{1,17},{... | collective-permute-start | bytes 3080 | tf_op jit(solution)/shard_map/ppermute | solution.py:342
  29.1 1.5 %collective-permute-done.2 = s32[8,32]{1,0:T(8,128)S(1)} collective-permute-done((s32[8,32]{1,0:T(8,128)S(1)}, s32[8,32]{1,0:T(8,128)S(1)}, u32[]{:S(2)}, u32[]{:S(2)}) %collective-permute-start.2) | collective-permute-done | bytes 1056 | tf_op jit(solution)/shard_map/ppermute | solution.py:342
  31.2 1.9 %select_blocks.1 = (bf16[2,160,128]{2,1,0:T(8,128)(2,1)}, bf16[2,160,128]{2,1,0:T(8,128)(2,1)}, bf16[2,160,128]{2,1,0:T(8,128)(2,1)}, bf16[2,160,128]{2,1,0:T(8,...) custom-call(s32[1]{0:T(128)} %bitcast.1.own_ref.refs_1_, ...), custom_call_target="tpu_custom_call" | custom-call | tf_op jit(solution)/shard_map/select_blocks/pallas_call | solution.py:194
  33.1 2.1 %collective-permute-start.3 = (bf16[2,160,128]{2,1,0:T(8,128)(2,1)}, bf16[2,160,128]{2,1,0:T(8,128)(2,1)S(1)}, u32[]{:S(2)}, u32[]{:S(2)}) collective-permute-start(bf16[2,160,128]{2,1,0:T(8,128)(2,1)} %get-tuple-element.22), channel_id=1, source_target_pairs={{0,4},{4,8},{8,12},{12,16},{16,20},{20,24},{24,28},{1,5},{5,9},{9,... | collective-permute-start | bytes 245768 | tf_op jit(solution)/shard_map/ppermute | solution.py:356
  35.1 3.8 %collective-permute-start.4 = (bf16[2,160,128]{2,1,0:T(8,128)(2,1)}, bf16[2,160,128]{2,1,0:T(8,128)(2,1)S(1)}, u32[]{:S(2)}, u32[]{:S(2)}) collective-permute-start(bf16[2,160,128]{2,1,0:T(8,128)(2,1)} %get-tuple-element.23), channel_id=1, source_target_pairs={{0,8},{4,12},{8,16},{12,20},{16,24},{20,28},{1,9},{5,13},{9,17},{1... | collective-permute-start | bytes 245768 | tf_op jit(solution)/shard_map/ppermute | solution.py:356
  39.4 5.5 %collective-permute-start.5 = (bf16[2,160,128]{2,1,0:T(8,128)(2,1)}, bf16[2,160,128]{2,1,0:T(8,128)(2,1)S(1)}, u32[]{:S(2)}, u32[]{:S(2)}) collective-permute-start(bf16[2,160,128]{2,1,0:T(8,128)(2,1)} %get-tuple-element.24), channel_id=1, source_target_pairs={{0,12},{4,16},{8,20},{12,24},{16,28},{1,13},{5,17},{9,21},{13,25},... | collective-permute-start | bytes 245768 | tf_op jit(solution)/shard_map/ppermute | solution.py:356
  48.8 1.5 %collective-permute-start.9 = (bf16[2,160,128]{2,1,0:T(8,128)(2,1)}, bf16[2,160,128]{2,1,0:T(8,128)(2,1)S(1)}, u32[]{:S(2)}, u32[]{:S(2)}) collective-permute-start(bf16[2,160,128]{2,1,0:T(8,128)(2,1)} %get-tuple-element.28), channel_id=1, source_target_pairs={{0,28},{1,29},{2,30},{3,31}} | collective-permute-start | bytes 245768 | tf_op jit(solution)/shard_map/ppermute | solution.py:356
  53.1 13.1 %attend.3 = bf16[320,512]{1,0:T(8,128)(2,1)} custom-call(s32[1]{0:T(128)} %bitcast.6.refs_0_, s32[1]{0:T(128)} %bitcast.1.own_ref.refs_1_, s32[10,32]{1,0:T(8,128)} %select_n.67.refs_2_, bf16[8,640,128]{2,1,0:T(8,128)(2,1)} %get-tuple-element.18.refs_3_, f32[640,16]{1,0:T(8,128)} %get-tuple-element.19.refs_4_, ...), custom_call_target="tpu_custom_call" | custom-call | flops 1677721600 | bytes 655360 | tf_op jit(solution)/shard_map/attend/pallas_call | solution.py:290
  66.2 1.3 %convolution_convert_fusion.7 = bf16[160,1024]{1,0:T(8,128)(2,1)S(1)} fusion(bf16[512,4096]{1,0:T(8,128)(2,1)S(1)} %copy-done, bf16[320,512]{1,0:T(8,128)(2,1)} %attend.3, s32[]{:T(128)S(6)} %select_n.69), kind=kOutput, calls=%fused_computation.10 | convolution fusion | flops 167936000 | bytes 1540100 | tf_op jit(solution)/shard_map/dot_general | solution.py:385
  69.7 12.6 %attend.2 = bf16[320,512]{1,0:T(8,128)(2,1)} custom-call(s32[1]{0:T(128)} %bitcast.refs_0_, s32[1]{0:T(128)} %bitcast.1.own_ref.refs_1_, s32[10,32]{1,0:T(8,128)} %select_n.67.refs_2_, bf16[8,640,128]{2,1,0:T(8,128)(2,1)} %get-tuple-element.18.refs_3_, f32[640,16]{1,0:T(8,128)} %get-tuple-element.19.refs_4_, ...), custom_call_target="tpu_custom_call" | custom-call | flops 1677721600 | bytes 655360 | tf_op jit(solution)/shard_map/attend/pallas_call | solution.py:290
  82.3 1.8 %convolution_convert_fusion.1 = bf16[160,4096]{1,0:T(8,128)(2,1)S(1)} fusion(bf16[512,4096]{1,0:T(8,128)(2,1)S(1)} %copy-done, bf16[320,512]{1,0:T(8,128)(2,1)} %attend.2, s32[]{:T(128)S(6)} %select_n.69), kind=kOutput, calls=%fused_computation.2 | convolution fusion | flops 671744000 | bytes 5668868 | tf_op jit(solution)/shard_map/dot_general | solution.py:385
  85.5 1.6 %collective-permute-start.12 = (bf16[160,1024]{1,0:T(8,128)(2,1)S(1)}, bf16[160,1024]{1,0:T(8,128)(2,1)S(1)}, u32[]{:S(2)}, u32[]{:S(2)}) collective-permute-start(bf16[160,1024]{1,0:T(8,128)(2,1)S(1)} %add_convert_fusion.3), channel_id=1, source_target_pairs={{0,2},{1,3},{2,0},{3,1},{4,6},{5,7},{6,4},{7,5},{8,10},{9,11},{10,... | collective-permute-start | bytes 983048 | tf_op jit(solution)/shard_map/ppermute | solution.py:402
  88.4 1.6 %collective-permute-start.16 = (bf16[160,1024]{1,0:T(8,128)(2,1)S(1)}, bf16[160,1024]{1,0:T(8,128)(2,1)S(1)}, u32[]{:S(2)}, u32[]{:S(2)}) collective-permute-start(bf16[160,1024]{1,0:T(8,128)(2,1)S(1)} %add_convert_fusion.1), channel_id=1, source_target_pairs={{0,2},{1,3},{2,0},{3,1},{4,6},{5,7},{6,4},{7,5},{8,10},{9,11},{10,... | collective-permute-start | bytes 983048 | tf_op jit(solution)/shard_map/ppermute | solution.py:402
  91.8 4.4 %collective-permute-done.12 = bf16[160,1024]{1,0:T(8,128)(2,1)S(1)} collective-permute-done((bf16[160,1024]{1,0:T(8,128)(2,1)S(1)}, bf16[160,1024]{1,0:T(8,128)(2,1)S(1)}, u32[]{:S(2)}, u32[]{:S(2)}) %collective-permute-start.12) | collective-permute-done | bytes 327712 | tf_op jit(solution)/shard_map/ppermute | solution.py:402
  96.2 7.0 %collective-permute-done.18 = bf16[160,1024]{1,0:T(8,128)(2,1)S(1)} collective-permute-done((bf16[160,1024]{1,0:T(8,128)(2,1)S(1)}, bf16[160,1024]{1,0:T(8,128)(2,1)S(1)}, u32[]{:S(2)}, u32[]{:S(2)}) %collective-permute-start.18) | collective-permute-done | bytes 327712 | tf_op jit(solution)/shard_map/ppermute | solution.py:402
  103.2 7.0 %collective-permute-done.16 = bf16[160,1024]{1,0:T(8,128)(2,1)S(1)} collective-permute-done((bf16[160,1024]{1,0:T(8,128)(2,1)S(1)}, bf16[160,1024]{1,0:T(8,128)(2,1)S(1)}, u32[]{:S(2)}, u32[]{:S(2)}) %collective-permute-start.16) | collective-permute-done | bytes 327712 | tf_op jit(solution)/shard_map/ppermute | solution.py:402
  110.2 6.5 %collective-permute-done.14 = bf16[160,1024]{1,0:T(8,128)(2,1)S(1)} collective-permute-done((bf16[160,1024]{1,0:T(8,128)(2,1)S(1)}, bf16[160,1024]{1,0:T(8,128)(2,1)S(1)}, u32[]{:S(2)}, u32[]{:S(2)}) %collective-permute-start.14) | collective-permute-done | bytes 327712 | tf_op jit(solution)/shard_map/ppermute | solution.py:402
  (76 shorter events, 18.9 us)
Async XLA Ops:
  1.2 20.4 %collective-permute-start = (s32[8,32]{1,0:T(8,128)S(1)}, s32[8,32]{1,0:T(8,128)S(1)}, u32[]{:S(2)}, u32[]{:S(2)}) collective-permute-start(s32[8,32]{1,0:T(8,128)S(1)} %broadcast_select_fusion.1), channel_id=1, source_target_pairs={{0,4},{4,0},{8,12},{12,8},{16,20},{20,16},{24,28},{28,24},{1,5},{5... | collective-permute-start | bytes 3080 | tf_op jit(solution)/shard_map/ppermute | solution.py:342
  15.8 5.8 %copy-start.2 = (s32[10,2,16]{2,1,0:T(2,128)S(1)}, s32[10,2,16]{2,1,0:T(2,128)}, u32[]{:S(2)}) copy-start(s32[10,2,16]{2,1,0:T(2,128)} %param.19) | copy-start | bytes 3844
  22.4 3.6 %collective-permute-start.1 = (s32[8,32]{1,0:T(8,128)S(1)}, s32[8,32]{1,0:T(8,128)S(1)}, u32[]{:S(2)}, u32[]{:S(2)}) collective-permute-start(s32[8,32]{1,0:T(8,128)S(1)} %fusion.58), channel_id=1, source_target_pairs={{0,8},{4,12},{8,0},{12,4},{16,24},{20,28},{24,16},{28,20},{1,9},{5... | collective-permute-start | bytes 3080 | tf_op jit(solution)/shard_map/ppermute | solution.py:342
  26.1 4.5 %collective-permute-start.2 = (s32[8,32]{1,0:T(8,128)S(1)}, s32[8,32]{1,0:T(8,128)S(1)}, u32[]{:S(2)}, u32[]{:S(2)}) collective-permute-start(s32[8,32]{1,0:T(8,128)S(1)} %fusion.61), channel_id=1, source_target_pairs={{0,16},{4,20},{8,24},{12,28},{16,0},{20,4},{24,8},{28,12},{1,17},{... | collective-permute-start | bytes 3080 | tf_op jit(solution)/shard_map/ppermute | solution.py:342
  33.1 14.4 %collective-permute-start.3 = (bf16[2,160,128]{2,1,0:T(8,128)(2,1)}, bf16[2,160,128]{2,1,0:T(8,128)(2,1)S(1)}, u32[]{:S(2)}, u32[]{:S(2)}) collective-permute-start(bf16[2,160,128]{2,1,0:T(8,128)(2,1)} %get-tuple-element.22), channel_id=1, source_target_pairs={{0,4},{4,8},{8,12},{12,16},{16,20},{20,24},{24,28},{1,5},{5,9},{9,... | collective-permute-start | bytes 245768 | tf_op jit(solution)/shard_map/ppermute | solution.py:356
  35.1 13.7 %collective-permute-start.4 = (bf16[2,160,128]{2,1,0:T(8,128)(2,1)}, bf16[2,160,128]{2,1,0:T(8,128)(2,1)S(1)}, u32[]{:S(2)}, u32[]{:S(2)}) collective-permute-start(bf16[2,160,128]{2,1,0:T(8,128)(2,1)} %get-tuple-element.23), channel_id=1, source_target_pairs={{0,8},{4,12},{8,16},{12,20},{16,24},{20,28},{1,9},{5,13},{9,17},{1... | collective-permute-start | bytes 245768 | tf_op jit(solution)/shard_map/ppermute | solution.py:356
  39.4 11.6 %collective-permute-start.5 = (bf16[2,160,128]{2,1,0:T(8,128)(2,1)}, bf16[2,160,128]{2,1,0:T(8,128)(2,1)S(1)}, u32[]{:S(2)}, u32[]{:S(2)}) collective-permute-start(bf16[2,160,128]{2,1,0:T(8,128)(2,1)} %get-tuple-element.24), channel_id=1, source_target_pairs={{0,12},{4,16},{8,20},{12,24},{16,28},{1,13},{5,17},{9,21},{13,25},... | collective-permute-start | bytes 245768 | tf_op jit(solution)/shard_map/ppermute | solution.py:356
  44.9 6.1 %collective-permute-start.6 = (bf16[2,160,128]{2,1,0:T(8,128)(2,1)}, bf16[2,160,128]{2,1,0:T(8,128)(2,1)S(1)}, u32[]{:S(2)}, u32[]{:S(2)}) collective-permute-start(bf16[2,160,128]{2,1,0:T(8,128)(2,1)} %get-tuple-element.25), channel_id=1, source_target_pairs={{0,16},{4,20},{8,24},{12,28},{1,17},{5,21},{9,25},{13,29},{2,18},{... | collective-permute-start | bytes 245768 | tf_op jit(solution)/shard_map/ppermute | solution.py:356
  46.2 4.8 %collective-permute-start.7 = (bf16[2,160,128]{2,1,0:T(8,128)(2,1)}, bf16[2,160,128]{2,1,0:T(8,128)(2,1)S(1)}, u32[]{:S(2)}, u32[]{:S(2)}) collective-permute-start(bf16[2,160,128]{2,1,0:T(8,128)(2,1)} %get-tuple-element.26), channel_id=1, source_target_pairs={{0,20},{4,24},{8,28},{1,21},{5,25},{9,29},{2,22},{6,26},{10,30},{3... | collective-permute-start | bytes 245768 | tf_op jit(solution)/shard_map/ppermute | solution.py:356
  47.5 5.0 %copy-start.3 = (bf16[2,160,128]{2,1,0:T(8,128)(2,1)}, bf16[2,160,128]{2,1,0:T(8,128)(2,1)S(1)}, u32[]{:S(2)}) copy-start(bf16[2,160,128]{2,1,0:T(8,128)(2,1)S(1)} %collective-permute-done.3.refs_7_) | copy-start | bytes 245764
  47.5 3.7 %collective-permute-start.8 = (bf16[2,160,128]{2,1,0:T(8,128)(2,1)}, bf16[2,160,128]{2,1,0:T(8,128)(2,1)S(1)}, u32[]{:S(2)}, u32[]{:S(2)}) collective-permute-start(bf16[2,160,128]{2,1,0:T(8,128)(2,1)} %get-tuple-element.27), channel_id=1, source_target_pairs={{0,24},{4,28},{1,25},{5,29},{2,26},{6,30},{3,27},{7,31}} | collective-permute-start | bytes 245768 | tf_op jit(solution)/shard_map/ppermute | solution.py:356
  48.8 3.7 %copy-start.4 = (bf16[2,160,128]{2,1,0:T(8,128)(2,1)}, bf16[2,160,128]{2,1,0:T(8,128)(2,1)S(1)}, u32[]{:S(2)}) copy-start(bf16[2,160,128]{2,1,0:T(8,128)(2,1)S(1)} %collective-permute-done.4.refs_8_) | copy-start | bytes 245764
  48.8 3.7 %collective-permute-start.9 = (bf16[2,160,128]{2,1,0:T(8,128)(2,1)}, bf16[2,160,128]{2,1,0:T(8,128)(2,1)S(1)}, u32[]{:S(2)}, u32[]{:S(2)}) collective-permute-start(bf16[2,160,128]{2,1,0:T(8,128)(2,1)} %get-tuple-element.28), channel_id=1, source_target_pairs={{0,28},{1,29},{2,30},{3,31}} | collective-permute-start | bytes 245768 | tf_op jit(solution)/shard_map/ppermute | solution.py:356
  53.1 13.1 %copy-start = (bf16[512,4096]{1,0:T(8,128)(2,1)S(1)}, bf16[512,4096]{1,0:T(8,128)(2,1)}, u32[]{:S(2)}) copy-start(bf16[512,4096]{1,0:T(8,128)(2,1)} %param.18) | copy-start | bytes 12582916
  69.1 16.1 %collective-permute-start.11 = (bf16[160,1024]{1,0:T(8,128)(2,1)S(1)}, bf16[160,1024]{1,0:T(8,128)(2,1)S(1)}, u32[]{:S(2)}, u32[]{:S(2)}) collective-permute-start(bf16[160,1024]{1,0:T(8,128)(2,1)S(1)} %convolution_convert_fusion.9), channel_id=1, source_target_pairs={{0,1},{1,0},{2,3},{3,2},{4,5},{5,4},{6,7},{7,6},{8,9},{9,8},{10,11... | collective-permute-start | bytes 983048 | tf_op jit(solution)/shard_map/ppermute | solution.py:399
  69.2 17.9 %collective-permute-start.17 = (bf16[160,1024]{1,0:T(8,128)(2,1)S(1)}, bf16[160,1024]{1,0:T(8,128)(2,1)S(1)}, u32[]{:S(2)}, u32[]{:S(2)}) collective-permute-start(bf16[160,1024]{1,0:T(8,128)(2,1)S(1)} %convolution_convert_fusion.3), channel_id=1, source_target_pairs={{0,1},{1,0},{2,3},{3,2},{4,5},{5,4},{6,7},{7,6},{8,9},{9,8},{10,11... | collective-permute-start | bytes 983048 | tf_op jit(solution)/shard_map/ppermute | solution.py:399
  84.1 6.8 %collective-permute-start.10 = (bf16[160,4096]{1,0:T(8,128)(2,1)S(1)}, bf16[160,4096]{1,0:T(8,128)(2,1)S(1)}, u32[]{:S(2)}, u32[]{:S(2)}) collective-permute-start(bf16[160,4096]{1,0:T(8,128)(2,1)S(1)} %convolution_convert_fusion.1), channel_id=1, source_target_pairs={{0,1},{1,0},{2,3},{3,2},{4,5},{5,4},{6,7},{7,6},{8,9},{9,8},{10,11... | collective-permute-start | bytes 3932168 | tf_op jit(solution)/shard_map/ppermute | solution.py:404
  84.6 3.5 %collective-permute-start.15 = (bf16[160,1024]{1,0:T(8,128)(2,1)S(1)}, bf16[160,1024]{1,0:T(8,128)(2,1)S(1)}, u32[]{:S(2)}, u32[]{:S(2)}) collective-permute-start(bf16[160,1024]{1,0:T(8,128)(2,1)S(1)} %convolution_convert_fusion.5), channel_id=1, source_target_pairs={{0,1},{1,0},{2,3},{3,2},{4,5},{5,4},{6,7},{7,6},{8,9},{9,8},{10,11... | collective-permute-start | bytes 983048 | tf_op jit(solution)/shard_map/ppermute | solution.py:399
  85.1 4.9 %collective-permute-start.13 = (bf16[160,1024]{1,0:T(8,128)(2,1)S(1)}, bf16[160,1024]{1,0:T(8,128)(2,1)S(1)}, u32[]{:S(2)}, u32[]{:S(2)}) collective-permute-start(bf16[160,1024]{1,0:T(8,128)(2,1)S(1)} %convolution_convert_fusion.7), channel_id=1, source_target_pairs={{0,1},{1,0},{2,3},{3,2},{4,5},{5,4},{6,7},{7,6},{8,9},{9,8},{10,11... | collective-permute-start | bytes 983048 | tf_op jit(solution)/shard_map/ppermute | solution.py:399
  85.5 5.4 %copy-start.1 = (bf16[320,512]{1,0:T(8,128)(2,1)S(1)}, bf16[320,512]{1,0:T(8,128)(2,1)}, u32[]{:S(2)}) copy-start(bf16[320,512]{1,0:T(8,128)(2,1)} %attend.2) | copy-start | bytes 983044
  85.5 10.6 %collective-permute-start.12 = (bf16[160,1024]{1,0:T(8,128)(2,1)S(1)}, bf16[160,1024]{1,0:T(8,128)(2,1)S(1)}, u32[]{:S(2)}, u32[]{:S(2)}) collective-permute-start(bf16[160,1024]{1,0:T(8,128)(2,1)S(1)} %add_convert_fusion.3), channel_id=1, source_target_pairs={{0,2},{1,3},{2,0},{3,1},{4,6},{5,7},{6,4},{7,5},{8,10},{9,11},{10,... | collective-permute-start | bytes 983048 | tf_op jit(solution)/shard_map/ppermute | solution.py:402
  87.5 15.8 %collective-permute-start.18 = (bf16[160,1024]{1,0:T(8,128)(2,1)S(1)}, bf16[160,1024]{1,0:T(8,128)(2,1)S(1)}, u32[]{:S(2)}, u32[]{:S(2)}) collective-permute-start(bf16[160,1024]{1,0:T(8,128)(2,1)S(1)} %add_convert_fusion), channel_id=1, source_target_pairs={{0,2},{1,3},{2,0},{3,1},{4,6},{5,7},{6,4},{7,5},{8,10},{9,11},{10,... | collective-permute-start | bytes 983048 | tf_op jit(solution)/shard_map/ppermute | solution.py:402
  88.4 21.8 %collective-permute-start.16 = (bf16[160,1024]{1,0:T(8,128)(2,1)S(1)}, bf16[160,1024]{1,0:T(8,128)(2,1)S(1)}, u32[]{:S(2)}, u32[]{:S(2)}) collective-permute-start(bf16[160,1024]{1,0:T(8,128)(2,1)S(1)} %add_convert_fusion.1), channel_id=1, source_target_pairs={{0,2},{1,3},{2,0},{3,1},{4,6},{5,7},{6,4},{7,5},{8,10},{9,11},{10,... | collective-permute-start | bytes 983048 | tf_op jit(solution)/shard_map/ppermute | solution.py:402
  90.3 26.4 %collective-permute-start.14 = (bf16[160,1024]{1,0:T(8,128)(2,1)S(1)}, bf16[160,1024]{1,0:T(8,128)(2,1)S(1)}, u32[]{:S(2)}, u32[]{:S(2)}) collective-permute-start(bf16[160,1024]{1,0:T(8,128)(2,1)S(1)} %add_convert_fusion.2), channel_id=1, source_target_pairs={{0,2},{1,3},{2,0},{3,1},{4,6},{5,7},{6,4},{7,5},{8,10},{9,11},{10,... | collective-permute-start | bytes 983048 | tf_op jit(solution)/shard_map/ppermute | solution.py:402
  (6 other events, 9.0 us)
where the time goes:
time: 119 us; the launch traced here: 118 us
  Pallas kernels  42.2 us (35%)
  starting transfers between devices  29.5 us (25%)
  waiting for transfers between devices  29.4 us (25%)
  matrix products  7.3 us (6%)
  other arithmetic  5.43 us (5%)
  local copies, waits for them, and re-layouts  4.18 us (4%)
    pallas_call x2, Pallas kernels, attend(): pl.pallas_call(functools.partial(attn_kernel, count), grid_spec=pltpu.Pre...  25.7 us
    ppermute x4, waiting for transfers between devices, local(): crossed.append(lax.ppermute(both, 'tp', cross))  24.9 us
    ppermute x7, starting transfers between devices, local(): lax.ppermute(pieces[k - 1], 'kv', [(i, i + k) for i in range(count - k)])  16.7 us
    pallas_call x1, Pallas kernels, project_q(): pl.pallas_call(q_kernel, grid_spec=pltpu.PrefetchScalarGridSpec(num_scala...  8.86 us
    dot_general x10, matrix products, product(): return jnp.dot(att, columns, preferred_element_type=F32).astype(BF16)  7.3 us
    ppermute x3, starting transfers between devices, local(): got = lax.ppermute(everyone, 'kv', [(i, i ^ bit) for i in range(count)])  7.18 us
    pallas_call x1, Pallas kernels, project_kv(): pl.pallas_call(kv_kernel, grid_spec=pltpu.PrefetchScalarGridSpec(num_scal...  5.79 us
    ppermute x4, starting transfers between devices, local(): crossed.append(lax.ppermute(both, 'tp', cross))  4.31 us
  transfers between devices with their start and end apart: 19, of which 8 were waited for; matrix products, arithmetic and copies ran while one was open for 8% of the time, Pallas kernels for 23%

commit v1 on v0

--- a/solution.py
+++ b/solution.py
@@ -33,88 +33,16 @@
     return lax.broadcasted_iota(jnp.int32, (rows, LANES), 0)
 
 
-def kv_kernel(part_ref, tok_ref, wk_ref, wv_ref, pos_ref, km_ref, vm_ref, kv_ref, sm_ref, acc_ref):
-    step = pl.program_id(0)
-    weight = jnp.concatenate([wk_ref[...], wv_ref[...]], axis=1)
-    piece = jnp.dot(tok_ref[...], weight, preferred_element_type=F32)
-
-    @pl.when(step == 0)
-    def _():
-        acc_ref[...] = piece
-
-    @pl.when(step > 0)
-    def _():
-        acc_ref[...] += piece
-
-    @pl.when(step == pl.num_programs(0) - 1)
-    def _():
-        heads, rows = kv_ref.shape[0], kv_ref.shape[1]
-        spans = rows // CMP
-        low_half = lane_iota(rows) < HD
-        pos = pos_ref[...].astype(F32)
-        pos = jnp.concatenate([pos, pos], axis=1)
-        columns = lax.broadcasted_iota(jnp.int32, km_ref.shape, 1)
-        for g in range(heads):
-            pair = g // 2
-            k = acc_ref[:, pair * LANES : (pair + 1) * LANES]
-            v = acc_ref[:, (heads // 2 + pair) * LANES : (heads // 2 + pair + 1) * LANES]
-            if g % 2 == 0:
-                both = jnp.where(low_half, k, pltpu.roll(v, HD, 1))
-            else:
-                both = jnp.where(low_half, pltpu.roll(k, HD, 1), v)
-            both = both.astype(BF16)
-            kv_ref[g] = both
-            mine = columns == part_ref[0] * heads + g
-            kmix = jnp.sum(jnp.where(mine, km_ref[...].astype(F32), 0.0), axis=1, keepdims=True)
-            vmix = jnp.sum(jnp.where(mine, vm_ref[...].astype(F32), 0.0), axis=1, keepdims=True)
-            mix = jnp.where(lane_iota(CMP) < HD, kmix, vmix)
-            windows = both.astype(F32).reshape(spans, CMP, LANES) + pos[None]
-            total = jnp.sum(windows * mix[None], axis=1)
-            pad = jnp.zeros((SPAN_PAD - spans, LANES), F32)
-            sm_ref[g] = jnp.concatenate([total, pad], axis=0).astype(BF16)
-
-
-def project_kv(part, tokens, key_weight, value_weight, pos, kmix, vmix):
-    rows, depth = tokens.shape
-    width = key_weight.shape[1]
-    heads = width // HD
-    chunk = depth // 4
-    full = lambda shape: pl.BlockSpec(shape, lambda i, s: (0,) * len(shape))
-    return pl.pallas_call(
-        kv_kernel,
-        grid_spec=pltpu.PrefetchScalarGridSpec(
-            num_scalar_prefetch=1,
-            grid=(depth // chunk,),
-            in_specs=[
-                pl.BlockSpec((rows, chunk), lambda i, s: (0, i)),
-                pl.BlockSpec((chunk, width), lambda i, s: (i, 0)),
-                pl.BlockSpec((chunk, width), lambda i, s: (i, 0)),
-                full(pos.shape),
-                full(kmix.shape),
-                full(vmix.shape),
-            ],
-            out_specs=[full((heads, rows, LANES)), full((heads, SPAN_PAD, LANES))],
-            scratch_shapes=[pltpu.VMEM((rows, 2 * width), F32)],
-        ),
-        out_shape=[
-            jax.ShapeDtypeStruct((heads, rows, LANES), BF16),
-            jax.ShapeDtypeStruct((heads, SPAN_PAD, LANES), BF16),
-        ],
-        cost_estimate=pl.CostEstimate(
-            flops=4 * rows * depth * width, transcendentals=0, bytes_accessed=2 * depth * (rows + 2 * width)
-        ),
-        compiler_params=pltpu.CompilerParams(vmem_limit_bytes=VMEM_LIMIT),
-        name="kv_proj",
-    )(part, tokens, key_weight, value_weight, pos, kmix, vmix)
-
-
-def q_kernel(part_ref, tok_ref, wq_ref, gw_ref, q_ref, gate_ref, acc_ref, gacc_ref):
+def proj_kernel(part_ref, tok_ref, wq_ref, wk_ref, wv_ref, gw_ref, pos_ref, km_ref, vm_ref, q_ref, gate_ref, kv_ref,
+                sm_ref, acc_ref, gacc_ref):
     step = pl.program_id(0)
     gates = gate_ref.shape[1]
     start = pl.multiple_of(part_ref[0] * gates, gates)
-    gate_rows = gw_ref[pl.ds(start, gates), :]
-    piece = jnp.dot(tok_ref[...], wq_ref[...], preferred_element_type=F32)
-    gpiece = lax.dot_general(tok_ref[...], gate_rows, (((1,), (1,)), ((), ())), preferred_element_type=F32)
+    weight = jnp.concatenate([wq_ref[...], wk_ref[...], wv_ref[...]], axis=1)
+    piece = jnp.dot(tok_ref[...], weight, preferred_element_type=F32)
+    gpiece = lax.dot_general(
+        tok_ref[...], gw_ref[pl.ds(start, gates), :], (((1,), (1,)), ((), ())), preferred_element_type=F32
+    )
 
     @pl.when(step == 0)
     def _():
@@ -129,6 +57,7 @@
     @pl.when(step == pl.num_programs(0) - 1)
     def _():
         heads, rows = q_ref.shape[0], q_ref.shape[1]
+        key_heads = kv_ref.shape[0]
         lane, inner = lane_iota(rows), lax.rem(row_iota(rows), SB)
         low_half = lane < HD
         ext = jnp.where((lane == HD) | (lane - HD > inner), 1.0, 0.0)
@@ -139,38 +68,75 @@
             q_ref[h] = jnp.where(low_half, slab, ext).astype(BF16)
         gate_ref[...] = jax.nn.sigmoid(gacc_ref[...])
 
-
-def project_q(part, tokens, query_weight, gate_rows):
+        spans = rows // CMP
+        pos = pos_ref[...].astype(F32)
+        pos = jnp.concatenate([pos, pos], axis=1)
+        line = lax.broadcasted_iota(jnp.int32, km_ref.shape, 0)
+        eye = lax.broadcasted_iota(jnp.int32, (CMP, CMP), 0) == lax.broadcasted_iota(jnp.int32, (CMP, CMP), 1)
+
+        def column(ref, head):
+            kept = jnp.sum(jnp.where(line == head, ref[...].astype(F32), 0.0), axis=0, keepdims=True)
+            return jnp.sum(jnp.where(eye, kept, 0.0), axis=1, keepdims=True)
+
+        at_k, at_v = heads * HD, heads * HD + key_heads * HD
+        for g in range(key_heads):
+            k = acc_ref[:, at_k + (g // 2) * LANES : at_k + (g // 2 + 1) * LANES]
+            v = acc_ref[:, at_v + (g // 2) * LANES : at_v + (g // 2 + 1) * LANES]
+            if g % 2 == 0:
+                both = jnp.where(low_half, k, pltpu.roll(v, HD, 1))
+            else:
+                both = jnp.where(low_half, pltpu.roll(k, HD, 1), v)
+            both = both.astype(BF16)
+            kv_ref[g] = both
+            head = part_ref[0] * key_heads + g
+            mix = jnp.where(lane_iota(CMP) < HD, column(km_ref, head), column(vm_ref, head))
+            windows = both.astype(F32).reshape(spans, CMP, LANES) + pos[None]
+            total = jnp.sum(windows * mix[None], axis=1)
+            pad = jnp.zeros((SPAN_PAD - spans, LANES), F32)
+            sm_ref[g] = jnp.concatenate([total, pad], axis=0).astype(BF16)
+
+
+def project(part, tokens, query_weight, key_weight, value_weight, gate_rows, pos, kmix, vmix):
     rows, depth = tokens.shape
-    width = query_weight.shape[1]
-    heads = width // HD
+    qwidth, width = query_weight.shape[1], key_weight.shape[1]
+    heads, key_heads = qwidth // HD, width // HD
     chunk = depth // 4
+    full = lambda shape: pl.BlockSpec(shape, lambda i, s: (0,) * len(shape))
     return pl.pallas_call(
-        q_kernel,
+        proj_kernel,
         grid_spec=pltpu.PrefetchScalarGridSpec(
             num_scalar_prefetch=1,
             grid=(depth // chunk,),
             in_specs=[
                 pl.BlockSpec((rows, chunk), lambda i, s: (0, i)),
+                pl.BlockSpec((chunk, qwidth), lambda i, s: (i, 0)),
+                pl.BlockSpec((chunk, width), lambda i, s: (i, 0)),
                 pl.BlockSpec((chunk, width), lambda i, s: (i, 0)),
                 pl.BlockSpec((gate_rows.shape[0], chunk), lambda i, s: (0, i)),
+                full(pos.shape),
+                full(kmix.shape),
+                full(vmix.shape),
             ],
             out_specs=[
-                pl.BlockSpec((heads, rows, LANES), lambda i, s: (0, 0, 0)),
-                pl.BlockSpec((rows, 2 * heads), lambda i, s: (0, 0)),
+                full((heads, rows, LANES)),
+                full((rows, 2 * heads)),
+                full((key_heads, rows, LANES)),
+                full((key_heads, SPAN_PAD, LANES)),
             ],
-            scratch_shapes=[pltpu.VMEM((rows, width), F32), pltpu.VMEM((rows, 2 * heads), F32)],
+            scratch_shapes=[pltpu.VMEM((rows, qwidth + 2 * width), F32), pltpu.VMEM((rows, 2 * heads), F32)],
         ),
         out_shape=[
             jax.ShapeDtypeStruct((heads, rows, LANES), BF16),
             jax.ShapeDtypeStruct((rows, 2 * heads), F32),
+            jax.ShapeDtypeStruct((key_heads, rows, LANES), BF16),
+            jax.ShapeDtypeStruct((key_heads, SPAN_PAD, LANES), BF16),
         ],
         cost_estimate=pl.CostEstimate(
-            flops=3 * rows * depth * width, transcendentals=0, bytes_accessed=2 * depth * (rows + width)
+            flops=2 * rows * depth * (qwidth + 3 * width), transcendentals=0, bytes_accessed=2 * depth * (rows + qwidth)
         ),
         compiler_params=pltpu.CompilerParams(vmem_limit_bytes=VMEM_LIMIT),
-        name="q_proj",
-    )(part, tokens, query_weight, gate_rows)
+        name="project",
+    )(part, tokens, query_weight, key_weight, value_weight, gate_rows, pos, kmix, vmix)
 
 
 def select_kernel(count, own_ref, req_ref, kv_ref, sm_ref, *out_refs):
@@ -347,8 +313,10 @@
     else:
         everyone = lax.all_gather(request, "kv", axis=0, tiled=True)
 
-    kv, summaries = project_kv(part1, tokens, key_weight, value_weight, summary_pos, key_mixing, value_mixing)
-    q, gates = project_q(part1, tokens, query_weight, gate_weight.T)
+    q, gates, kv, summaries = project(
+        part1, tokens, query_weight, key_weight, value_weight, gate_weight.T, summary_pos, key_mixing.T,
+        value_mixing.T,
+    )
 
     pieces = select_blocks(count, own1, everyone, kv, summaries)
     received = []

time: 119 us -> 113 us (0.950)
  Pallas kernels: 42.2 us -> 38.6 us
  local copies, waits for them, and re-layouts: 4.18 us -> 1.49 us
    pallas_call x2 -> x1, Pallas kernels: 14.7 us -> 11.1 us  [project(): pl.pallas_call(proj_kernel, grid_spec=pltpu.PrefetchScalarGridSpec(num_sc...]
    unnamed x24 -> x22, local copies, waits for them, and re-layouts: 3.33 us -> 0.63 us
  transfers between devices with their start and end apart: 19 -> 19, of which waited for: 8 -> 8; matrix products, arithmetic and copies ran while one was open for 8% -> 6% of each run, Pallas kernels for 23% -> 21%
where the time goes in v1:
time: 113 us; the launch traced here: 112 us
  Pallas kernels  38.6 us (34%)
  starting transfers between devices  29.5 us (26%)
  waiting for transfers between devices  29.4 us (26%)
  matrix products  7.3 us (6%)
  other arithmetic  5.43 us (5%)
  local copies, waits for them, and re-layouts  1.49 us (1%)
    pallas_call x2, Pallas kernels, attend(): pl.pallas_call(functools.partial(attn_kernel, count), grid_spec=pltpu.Pre...  25.7 us
    ppermute x4, waiting for transfers between devices, local(): crossed.append(lax.ppermute(both, 'tp', cross))  24.9 us
    ppermute x7, starting transfers between devices, local(): lax.ppermute(pieces[k - 1], 'kv', [(i, i + k) for i in range(count - k)])  16.7 us
    pallas_call x1, Pallas kernels, project(): pl.pallas_call(proj_kernel, grid_spec=pltpu.PrefetchScalarGridSpec(num_sc...  11.1 us
    dot_general x10, matrix products, product(): return jnp.dot(att, columns, preferred_element_type=F32).astype(BF16)  7.3 us
    ppermute x3, starting transfers between devices, local(): got = lax.ppermute(everyone, 'kv', [(i, i ^ bit) for i in range(count)])  7.17 us
    ppermute x4, starting transfers between devices, local(): crossed.append(lax.ppermute(both, 'tp', cross))  4.31 us
    ppermute x3, waiting for transfers between devices, local(): got = lax.ppermute(everyone, 'kv', [(i, i ^ bit) for i in range(count)])  3.08 us
  transfers between devices with their start and end apart: 19, of which 8 were waited for; matrix products, arithmetic and copies ran while one was open for 6% of the time, Pallas kernels for 21%

profile of v1, /device:TPU:0, one launch (start us, length us, event | category | flops | bytes accessed | tf_op | source)
XLA Modules:
  0.0 112.1 jit_solution(16336096241147981357)
XLA Ops:
  1.2 3.0 %collective-permute-start = (s32[8,32]{1,0:T(8,128)S(1)}, s32[8,32]{1,0:T(8,128)S(1)}, u32[]{:S(2)}, u32[]{:S(2)}) collective-permute-start(s32[8,32]{1,0:T(8,128)S(1)} %broadcast_select_fusion.1), channel_id=1, source_target_pairs={{0,4},{4,0},{8,12},{12,8},{16,20},{20,16},{24,28},{28,24},{1,5},{5... | collective-permute-start | bytes 3080 | tf_op jit(solution)/shard_map/ppermute | solution.py:308
  4.2 11.1 %project.1 = (bf16[8,640,128]{2,1,0:T(8,128)(2,1)}, f32[640,16]{1,0:T(8,128)}, bf16[2,640,128]{2,1,0:T(8,128)(2,1)}, bf16[2,32,128]{2,1,0:T(8,128)(2,1)}) custom-call(s32[1]{0:T(128)} %bitcast.4.part_ref, bf16[640,4096]{1,0:T(8,128)(2,1)} %tok_ref.1, bf16[4096,512]{1,0:T(8,128)(2,1)} %wq_ref.1, bf16[4096,128]{1,0:T(8,128)(2,1)} %wk_ref.1, ...), custom_call_target="tpu_custom_call" | custom-call | flops 4697620480 | bytes 9437184 | tf_op jit(solution)/shard_map/project/pallas_call | solution.py:105
  16.1 1.6 %collective-permute-start.1 = (s32[8,32]{1,0:T(8,128)S(1)}, s32[8,32]{1,0:T(8,128)S(1)}, u32[]{:S(2)}, u32[]{:S(2)}) collective-permute-start(s32[8,32]{1,0:T(8,128)S(1)} %fusion.58), channel_id=1, source_target_pairs={{0,8},{4,12},{8,0},{12,4},{16,24},{20,28},{24,16},{28,20},{1,9},{5... | collective-permute-start | bytes 3080 | tf_op jit(solution)/shard_map/ppermute | solution.py:308
  18.1 1.6 %collective-permute-done.1 = s32[8,32]{1,0:T(8,128)S(1)} collective-permute-done((s32[8,32]{1,0:T(8,128)S(1)}, s32[8,32]{1,0:T(8,128)S(1)}, u32[]{:S(2)}, u32[]{:S(2)}) %collective-permute-start.1) | collective-permute-done | bytes 1056 | tf_op jit(solution)/shard_map/ppermute | solution.py:308
  19.8 2.6 %collective-permute-start.2 = (s32[8,32]{1,0:T(8,128)S(1)}, s32[8,32]{1,0:T(8,128)S(1)}, u32[]{:S(2)}, u32[]{:S(2)}) collective-permute-start(s32[8,32]{1,0:T(8,128)S(1)} %fusion.61), channel_id=1, source_target_pairs={{0,16},{4,20},{8,24},{12,28},{16,0},{20,4},{24,8},{28,12},{1,17},{... | collective-permute-start | bytes 3080 | tf_op jit(solution)/shard_map/ppermute | solution.py:308
  22.8 1.5 %collective-permute-done.2 = s32[8,32]{1,0:T(8,128)S(1)} collective-permute-done((s32[8,32]{1,0:T(8,128)S(1)}, s32[8,32]{1,0:T(8,128)S(1)}, u32[]{:S(2)}, u32[]{:S(2)}) %collective-permute-start.2) | collective-permute-done | bytes 1056 | tf_op jit(solution)/shard_map/ppermute | solution.py:308
  24.9 1.9 %select_blocks.1 = (bf16[2,160,128]{2,1,0:T(8,128)(2,1)}, bf16[2,160,128]{2,1,0:T(8,128)(2,1)}, bf16[2,160,128]{2,1,0:T(8,128)(2,1)}, bf16[2,160,128]{2,1,0:T(8,...) custom-call(s32[1]{0:T(128)} %bitcast.1.own_ref.refs_1_, ...), custom_call_target="tpu_custom_call" | custom-call | tf_op jit(solution)/shard_map/select_blocks/pallas_call | solution.py:160
  26.8 2.1 %collective-permute-start.3 = (bf16[2,160,128]{2,1,0:T(8,128)(2,1)}, bf16[2,160,128]{2,1,0:T(8,128)(2,1)S(1)}, u32[]{:S(2)}, u32[]{:S(2)}) collective-permute-start(bf16[2,160,128]{2,1,0:T(8,128)(2,1)} %get-tuple-element.22), channel_id=1, source_target_pairs={{0,4},{4,8},{8,12},{12,16},{16,20},{20,24},{24,28},{1,5},{5,9},{9,... | collective-permute-start | bytes 245768 | tf_op jit(solution)/shard_map/ppermute | solution.py:324
  28.9 3.8 %collective-permute-start.4 = (bf16[2,160,128]{2,1,0:T(8,128)(2,1)}, bf16[2,160,128]{2,1,0:T(8,128)(2,1)S(1)}, u32[]{:S(2)}, u32[]{:S(2)}) collective-permute-start(bf16[2,160,128]{2,1,0:T(8,128)(2,1)} %get-tuple-element.23), channel_id=1, source_target_pairs={{0,8},{4,12},{8,16},{12,20},{16,24},{20,28},{1,9},{5,13},{9,17},{1... | collective-permute-start | bytes 245768 | tf_op jit(solution)/shard_map/ppermute | solution.py:324
  33.1 5.5 %collective-permute-start.5 = (bf16[2,160,128]{2,1,0:T(8,128)(2,1)}, bf16[2,160,128]{2,1,0:T(8,128)(2,1)S(1)}, u32[]{:S(2)}, u32[]{:S(2)}) collective-permute-start(bf16[2,160,128]{2,1,0:T(8,128)(2,1)} %get-tuple-element.24), channel_id=1, source_target_pairs={{0,12},{4,16},{8,20},{12,24},{16,28},{1,13},{5,17},{9,21},{13,25},... | collective-permute-start | bytes 245768 | tf_op jit(solution)/shard_map/ppermute | solution.py:324
  38.6 1.3 %collective-permute-start.6 = (bf16[2,160,128]{2,1,0:T(8,128)(2,1)}, bf16[2,160,128]{2,1,0:T(8,128)(2,1)S(1)}, u32[]{:S(2)}, u32[]{:S(2)}) collective-permute-start(bf16[2,160,128]{2,1,0:T(8,128)(2,1)} %get-tuple-element.25), channel_id=1, source_target_pairs={{0,16},{4,20},{8,24},{12,28},{1,17},{5,21},{9,25},{13,29},{2,18},{... | collective-permute-start | bytes 245768 | tf_op jit(solution)/shard_map/ppermute | solution.py:324
  39.9 1.3 %collective-permute-start.7 = (bf16[2,160,128]{2,1,0:T(8,128)(2,1)}, bf16[2,160,128]{2,1,0:T(8,128)(2,1)S(1)}, u32[]{:S(2)}, u32[]{:S(2)}) collective-permute-start(bf16[2,160,128]{2,1,0:T(8,128)(2,1)} %get-tuple-element.26), channel_id=1, source_target_pairs={{0,20},{4,24},{8,28},{1,21},{5,25},{9,29},{2,22},{6,26},{10,30},{3... | collective-permute-start | bytes 245768 | tf_op jit(solution)/shard_map/ppermute | solution.py:324
  42.5 1.5 %collective-permute-start.9 = (bf16[2,160,128]{2,1,0:T(8,128)(2,1)}, bf16[2,160,128]{2,1,0:T(8,128)(2,1)S(1)}, u32[]{:S(2)}, u32[]{:S(2)}) collective-permute-start(bf16[2,160,128]{2,1,0:T(8,128)(2,1)} %get-tuple-element.28), channel_id=1, source_target_pairs={{0,28},{1,29},{2,30},{3,31}} | collective-permute-start | bytes 245768 | tf_op jit(solution)/shard_map/ppermute | solution.py:324
  44.9 1.3 %collective-permute-done.9.refs_13_ = bf16[2,160,128]{2,1,0:T(8,128)(2,1)S(1)} collective-permute-done((bf16[2,160,128]{2,1,0:T(8,128)(2,1)}, bf16[2,160,128]{2,1,0:T(8,128)(2,1)S(1)}, u32[]{:S(2)}, u32[]{:S(2)}) %collective-permute-start.9) | collective-permute-done | bytes 81952 | tf_op jit(solution)/shard_map/ppermute | solution.py:324
  46.8 13.1 %attend.3 = bf16[320,512]{1,0:T(8,128)(2,1)} custom-call(s32[1]{0:T(128)} %bitcast.8.refs_0_, s32[1]{0:T(128)} %bitcast.1.own_ref.refs_1_, s32[10,32]{1,0:T(8,128)} %select_n.67.refs_2_, bf16[8,640,128]{2,1,0:T(8,128)(2,1)} %get-tuple-element.18.refs_3_, f32[640,16]{1,0:T(8,128)} %get-tuple-element.19.refs_4_, ...), custom_call_target="tpu_custom_call" | custom-call | flops 1677721600 | bytes 655360 | tf_op jit(solution)/shard_map/attend/pallas_call | solution.py:256
  59.9 1.3 %convolution_convert_fusion.7 = bf16[160,1024]{1,0:T(8,128)(2,1)S(1)} fusion(bf16[512,4096]{1,0:T(8,128)(2,1)S(1)} %copy-done, bf16[320,512]{1,0:T(8,128)(2,1)} %attend.3, s32[]{:T(128)S(6)} %select_n.69), kind=kOutput, calls=%fused_computation.10 | convolution fusion | flops 167936000 | bytes 1540100 | tf_op jit(solution)/shard_map/dot_general | solution.py:353
  63.4 12.6 %attend.2 = bf16[320,512]{1,0:T(8,128)(2,1)} custom-call(s32[1]{0:T(128)} %bitcast.refs_0_, s32[1]{0:T(128)} %bitcast.1.own_ref.refs_1_, s32[10,32]{1,0:T(8,128)} %select_n.67.refs_2_, bf16[8,640,128]{2,1,0:T(8,128)(2,1)} %get-tuple-element.18.refs_3_, f32[640,16]{1,0:T(8,128)} %get-tuple-element.19.refs_4_, ...), custom_call_target="tpu_custom_call" | custom-call | flops 1677721600 | bytes 655360 | tf_op jit(solution)/shard_map/attend/pallas_call | solution.py:256
  76.1 1.8 %convolution_convert_fusion.1 = bf16[160,4096]{1,0:T(8,128)(2,1)S(1)} fusion(bf16[512,4096]{1,0:T(8,128)(2,1)S(1)} %copy-done, bf16[320,512]{1,0:T(8,128)(2,1)} %attend.2, s32[]{:T(128)S(6)} %select_n.69), kind=kOutput, calls=%fused_computation.2 | convolution fusion | flops 671744000 | bytes 5668868 | tf_op jit(solution)/shard_map/dot_general | solution.py:353
  79.3 1.6 %collective-permute-start.12 = (bf16[160,1024]{1,0:T(8,128)(2,1)S(1)}, bf16[160,1024]{1,0:T(8,128)(2,1)S(1)}, u32[]{:S(2)}, u32[]{:S(2)}) collective-permute-start(bf16[160,1024]{1,0:T(8,128)(2,1)S(1)} %add_convert_fusion.3), channel_id=1, source_target_pairs={{0,2},{1,3},{2,0},{3,1},{4,6},{5,7},{6,4},{7,5},{8,10},{9,11},{10,... | collective-permute-start | bytes 983048 | tf_op jit(solution)/shard_map/ppermute | solution.py:370
  82.2 1.6 %collective-permute-start.16 = (bf16[160,1024]{1,0:T(8,128)(2,1)S(1)}, bf16[160,1024]{1,0:T(8,128)(2,1)S(1)}, u32[]{:S(2)}, u32[]{:S(2)}) collective-permute-start(bf16[160,1024]{1,0:T(8,128)(2,1)S(1)} %add_convert_fusion.1), channel_id=1, source_target_pairs={{0,2},{1,3},{2,0},{3,1},{4,6},{5,7},{6,4},{7,5},{8,10},{9,11},{10,... | collective-permute-start | bytes 983048 | tf_op jit(solution)/shard_map/ppermute | solution.py:370
  85.6 4.4 %collective-permute-done.12 = bf16[160,1024]{1,0:T(8,128)(2,1)S(1)} collective-permute-done((bf16[160,1024]{1,0:T(8,128)(2,1)S(1)}, bf16[160,1024]{1,0:T(8,128)(2,1)S(1)}, u32[]{:S(2)}, u32[]{:S(2)}) %collective-permute-start.12) | collective-permute-done | bytes 327712 | tf_op jit(solution)/shard_map/ppermute | solution.py:370
  89.9 7.0 %collective-permute-done.18 = bf16[160,1024]{1,0:T(8,128)(2,1)S(1)} collective-permute-done((bf16[160,1024]{1,0:T(8,128)(2,1)S(1)}, bf16[160,1024]{1,0:T(8,128)(2,1)S(1)}, u32[]{:S(2)}, u32[]{:S(2)}) %collective-permute-start.18) | collective-permute-done | bytes 327712 | tf_op jit(solution)/shard_map/ppermute | solution.py:370
  97.0 7.0 %collective-permute-done.16 = bf16[160,1024]{1,0:T(8,128)(2,1)S(1)} collective-permute-done((bf16[160,1024]{1,0:T(8,128)(2,1)S(1)}, bf16[160,1024]{1,0:T(8,128)(2,1)S(1)}, u32[]{:S(2)}, u32[]{:S(2)}) %collective-permute-start.16) | collective-permute-done | bytes 327712 | tf_op jit(solution)/shard_map/ppermute | solution.py:370
  104.0 6.5 %collective-permute-done.14 = bf16[160,1024]{1,0:T(8,128)(2,1)S(1)} collective-permute-done((bf16[160,1024]{1,0:T(8,128)(2,1)S(1)}, bf16[160,1024]{1,0:T(8,128)(2,1)S(1)}, u32[]{:S(2)}, u32[]{:S(2)}) %collective-permute-start.14) | collective-permute-done | bytes 327712 | tf_op jit(solution)/shard_map/ppermute | solution.py:370
  (73 shorter events, 15.1 us)
Async XLA Ops:
  1.2 14.1 %collective-permute-start = (s32[8,32]{1,0:T(8,128)S(1)}, s32[8,32]{1,0:T(8,128)S(1)}, u32[]{:S(2)}, u32[]{:S(2)}) collective-permute-start(s32[8,32]{1,0:T(8,128)S(1)} %broadcast_select_fusion.1), channel_id=1, source_target_pairs={{0,4},{4,0},{8,12},{12,8},{16,20},{20,16},{24,28},{28,24},{1,5},{5... | collective-permute-start | bytes 3080 | tf_op jit(solution)/shard_map/ppermute | solution.py:308
  4.2 11.1 %copy-start.2 = (s32[10,2,16]{2,1,0:T(2,128)S(1)}, s32[10,2,16]{2,1,0:T(2,128)}, u32[]{:S(2)}) copy-start(s32[10,2,16]{2,1,0:T(2,128)} %param.19) | copy-start | bytes 3844
  16.1 3.6 %collective-permute-start.1 = (s32[8,32]{1,0:T(8,128)S(1)}, s32[8,32]{1,0:T(8,128)S(1)}, u32[]{:S(2)}, u32[]{:S(2)}) collective-permute-start(s32[8,32]{1,0:T(8,128)S(1)} %fusion.58), channel_id=1, source_target_pairs={{0,8},{4,12},{8,0},{12,4},{16,24},{20,28},{24,16},{28,20},{1,9},{5... | collective-permute-start | bytes 3080 | tf_op jit(solution)/shard_map/ppermute | solution.py:308
  19.8 4.5 %collective-permute-start.2 = (s32[8,32]{1,0:T(8,128)S(1)}, s32[8,32]{1,0:T(8,128)S(1)}, u32[]{:S(2)}, u32[]{:S(2)}) collective-permute-start(s32[8,32]{1,0:T(8,128)S(1)} %fusion.61), channel_id=1, source_target_pairs={{0,16},{4,20},{8,24},{12,28},{16,0},{20,4},{24,8},{28,12},{1,17},{... | collective-permute-start | bytes 3080 | tf_op jit(solution)/shard_map/ppermute | solution.py:308
  26.8 14.4 %collective-permute-start.3 = (bf16[2,160,128]{2,1,0:T(8,128)(2,1)}, bf16[2,160,128]{2,1,0:T(8,128)(2,1)S(1)}, u32[]{:S(2)}, u32[]{:S(2)}) collective-permute-start(bf16[2,160,128]{2,1,0:T(8,128)(2,1)} %get-tuple-element.22), channel_id=1, source_target_pairs={{0,4},{4,8},{8,12},{12,16},{16,20},{20,24},{24,28},{1,5},{5,9},{9,... | collective-permute-start | bytes 245768 | tf_op jit(solution)/shard_map/ppermute | solution.py:324
  28.9 13.7 %collective-permute-start.4 = (bf16[2,160,128]{2,1,0:T(8,128)(2,1)}, bf16[2,160,128]{2,1,0:T(8,128)(2,1)S(1)}, u32[]{:S(2)}, u32[]{:S(2)}) collective-permute-start(bf16[2,160,128]{2,1,0:T(8,128)(2,1)} %get-tuple-element.23), channel_id=1, source_target_pairs={{0,8},{4,12},{8,16},{12,20},{16,24},{20,28},{1,9},{5,13},{9,17},{1... | collective-permute-start | bytes 245768 | tf_op jit(solution)/shard_map/ppermute | solution.py:324
  33.1 11.6 %collective-permute-start.5 = (bf16[2,160,128]{2,1,0:T(8,128)(2,1)}, bf16[2,160,128]{2,1,0:T(8,128)(2,1)S(1)}, u32[]{:S(2)}, u32[]{:S(2)}) collective-permute-start(bf16[2,160,128]{2,1,0:T(8,128)(2,1)} %get-tuple-element.24), channel_id=1, source_target_pairs={{0,12},{4,16},{8,20},{12,24},{16,28},{1,13},{5,17},{9,21},{13,25},... | collective-permute-start | bytes 245768 | tf_op jit(solution)/shard_map/ppermute | solution.py:324
  38.6 6.1 %collective-permute-start.6 = (bf16[2,160,128]{2,1,0:T(8,128)(2,1)}, bf16[2,160,128]{2,1,0:T(8,128)(2,1)S(1)}, u32[]{:S(2)}, u32[]{:S(2)}) collective-permute-start(bf16[2,160,128]{2,1,0:T(8,128)(2,1)} %get-tuple-element.25), channel_id=1, source_target_pairs={{0,16},{4,20},{8,24},{12,28},{1,17},{5,21},{9,25},{13,29},{2,18},{... | collective-permute-start | bytes 245768 | tf_op jit(solution)/shard_map/ppermute | solution.py:324
  39.9 4.8 %collective-permute-start.7 = (bf16[2,160,128]{2,1,0:T(8,128)(2,1)}, bf16[2,160,128]{2,1,0:T(8,128)(2,1)S(1)}, u32[]{:S(2)}, u32[]{:S(2)}) collective-permute-start(bf16[2,160,128]{2,1,0:T(8,128)(2,1)} %get-tuple-element.26), channel_id=1, source_target_pairs={{0,20},{4,24},{8,28},{1,21},{5,25},{9,29},{2,22},{6,26},{10,30},{3... | collective-permute-start | bytes 245768 | tf_op jit(solution)/shard_map/ppermute | solution.py:324
  41.2 5.0 %copy-start.3 = (bf16[2,160,128]{2,1,0:T(8,128)(2,1)}, bf16[2,160,128]{2,1,0:T(8,128)(2,1)S(1)}, u32[]{:S(2)}) copy-start(bf16[2,160,128]{2,1,0:T(8,128)(2,1)S(1)} %collective-permute-done.3.refs_7_) | copy-start | bytes 245764
  41.2 3.7 %collective-permute-start.8 = (bf16[2,160,128]{2,1,0:T(8,128)(2,1)}, bf16[2,160,128]{2,1,0:T(8,128)(2,1)S(1)}, u32[]{:S(2)}, u32[]{:S(2)}) collective-permute-start(bf16[2,160,128]{2,1,0:T(8,128)(2,1)} %get-tuple-element.27), channel_id=1, source_target_pairs={{0,24},{4,28},{1,25},{5,29},{2,26},{6,30},{3,27},{7,31}} | collective-permute-start | bytes 245768 | tf_op jit(solution)/shard_map/ppermute | solution.py:324
  42.5 3.7 %copy-start.4 = (bf16[2,160,128]{2,1,0:T(8,128)(2,1)}, bf16[2,160,128]{2,1,0:T(8,128)(2,1)S(1)}, u32[]{:S(2)}) copy-start(bf16[2,160,128]{2,1,0:T(8,128)(2,1)S(1)} %collective-permute-done.4.refs_8_) | copy-start | bytes 245764
  42.5 3.7 %collective-permute-start.9 = (bf16[2,160,128]{2,1,0:T(8,128)(2,1)}, bf16[2,160,128]{2,1,0:T(8,128)(2,1)S(1)}, u32[]{:S(2)}, u32[]{:S(2)}) collective-permute-start(bf16[2,160,128]{2,1,0:T(8,128)(2,1)} %get-tuple-element.28), channel_id=1, source_target_pairs={{0,28},{1,29},{2,30},{3,31}} | collective-permute-start | bytes 245768 | tf_op jit(solution)/shard_map/ppermute | solution.py:324
  46.8 13.1 %copy-start = (bf16[512,4096]{1,0:T(8,128)(2,1)S(1)}, bf16[512,4096]{1,0:T(8,128)(2,1)}, u32[]{:S(2)}) copy-start(bf16[512,4096]{1,0:T(8,128)(2,1)} %param.18) | copy-start | bytes 12582916
  62.9 16.1 %collective-permute-start.11 = (bf16[160,1024]{1,0:T(8,128)(2,1)S(1)}, bf16[160,1024]{1,0:T(8,128)(2,1)S(1)}, u32[]{:S(2)}, u32[]{:S(2)}) collective-permute-start(bf16[160,1024]{1,0:T(8,128)(2,1)S(1)} %convolution_convert_fusion.9), channel_id=1, source_target_pairs={{0,1},{1,0},{2,3},{3,2},{4,5},{5,4},{6,7},{7,6},{8,9},{9,8},{10,11... | collective-permute-start | bytes 983048 | tf_op jit(solution)/shard_map/ppermute | solution.py:367
  62.9 17.9 %collective-permute-start.17 = (bf16[160,1024]{1,0:T(8,128)(2,1)S(1)}, bf16[160,1024]{1,0:T(8,128)(2,1)S(1)}, u32[]{:S(2)}, u32[]{:S(2)}) collective-permute-start(bf16[160,1024]{1,0:T(8,128)(2,1)S(1)} %convolution_convert_fusion.3), channel_id=1, source_target_pairs={{0,1},{1,0},{2,3},{3,2},{4,5},{5,4},{6,7},{7,6},{8,9},{9,8},{10,11... | collective-permute-start | bytes 983048 | tf_op jit(solution)/shard_map/ppermute | solution.py:367
  77.9 6.8 %collective-permute-start.10 = (bf16[160,4096]{1,0:T(8,128)(2,1)S(1)}, bf16[160,4096]{1,0:T(8,128)(2,1)S(1)}, u32[]{:S(2)}, u32[]{:S(2)}) collective-permute-start(bf16[160,4096]{1,0:T(8,128)(2,1)S(1)} %convolution_convert_fusion.1), channel_id=1, source_target_pairs={{0,1},{1,0},{2,3},{3,2},{4,5},{5,4},{6,7},{7,6},{8,9},{9,8},{10,11... | collective-permute-start | bytes 3932168 | tf_op jit(solution)/shard_map/ppermute | solution.py:372
  78.3 3.5 %collective-permute-start.15 = (bf16[160,1024]{1,0:T(8,128)(2,1)S(1)}, bf16[160,1024]{1,0:T(8,128)(2,1)S(1)}, u32[]{:S(2)}, u32[]{:S(2)}) collective-permute-start(bf16[160,1024]{1,0:T(8,128)(2,1)S(1)} %convolution_convert_fusion.5), channel_id=1, source_target_pairs={{0,1},{1,0},{2,3},{3,2},{4,5},{5,4},{6,7},{7,6},{8,9},{9,8},{10,11... | collective-permute-start | bytes 983048 | tf_op jit(solution)/shard_map/ppermute | solution.py:367
  78.8 4.9 %collective-permute-start.13 = (bf16[160,1024]{1,0:T(8,128)(2,1)S(1)}, bf16[160,1024]{1,0:T(8,128)(2,1)S(1)}, u32[]{:S(2)}, u32[]{:S(2)}) collective-permute-start(bf16[160,1024]{1,0:T(8,128)(2,1)S(1)} %convolution_convert_fusion.7), channel_id=1, source_target_pairs={{0,1},{1,0},{2,3},{3,2},{4,5},{5,4},{6,7},{7,6},{8,9},{9,8},{10,11... | collective-permute-start | bytes 983048 | tf_op jit(solution)/shard_map/ppermute | solution.py:367
  79.3 5.4 %copy-start.1 = (bf16[320,512]{1,0:T(8,128)(2,1)S(1)}, bf16[320,512]{1,0:T(8,128)(2,1)}, u32[]{:S(2)}) copy-start(bf16[320,512]{1,0:T(8,128)(2,1)} %attend.2) | copy-start | bytes 983044
  79.3 10.6 %collective-permute-start.12 = (bf16[160,1024]{1,0:T(8,128)(2,1)S(1)}, bf16[160,1024]{1,0:T(8,128)(2,1)S(1)}, u32[]{:S(2)}, u32[]{:S(2)}) collective-permute-start(bf16[160,1024]{1,0:T(8,128)(2,1)S(1)} %add_convert_fusion.3), channel_id=1, source_target_pairs={{0,2},{1,3},{2,0},{3,1},{4,6},{5,7},{6,4},{7,5},{8,10},{9,11},{10,... | collective-permute-start | bytes 983048 | tf_op jit(solution)/shard_map/ppermute | solution.py:370
  81.2 15.8 %collective-permute-start.18 = (bf16[160,1024]{1,0:T(8,128)(2,1)S(1)}, bf16[160,1024]{1,0:T(8,128)(2,1)S(1)}, u32[]{:S(2)}, u32[]{:S(2)}) collective-permute-start(bf16[160,1024]{1,0:T(8,128)(2,1)S(1)} %add_convert_fusion), channel_id=1, source_target_pairs={{0,2},{1,3},{2,0},{3,1},{4,6},{5,7},{6,4},{7,5},{8,10},{9,11},{10,... | collective-permute-start | bytes 983048 | tf_op jit(solution)/shard_map/ppermute | solution.py:370
  82.2 21.8 %collective-permute-start.16 = (bf16[160,1024]{1,0:T(8,128)(2,1)S(1)}, bf16[160,1024]{1,0:T(8,128)(2,1)S(1)}, u32[]{:S(2)}, u32[]{:S(2)}) collective-permute-start(bf16[160,1024]{1,0:T(8,128)(2,1)S(1)} %add_convert_fusion.1), channel_id=1, source_target_pairs={{0,2},{1,3},{2,0},{3,1},{4,6},{5,7},{6,4},{7,5},{8,10},{9,11},{10,... | collective-permute-start | bytes 983048 | tf_op jit(solution)/shard_map/ppermute | solution.py:370
  84.1 26.4 %collective-permute-start.14 = (bf16[160,1024]{1,0:T(8,128)(2,1)S(1)}, bf16[160,1024]{1,0:T(8,128)(2,1)S(1)}, u32[]{:S(2)}, u32[]{:S(2)}) collective-permute-start(bf16[160,1024]{1,0:T(8,128)(2,1)S(1)} %add_convert_fusion.2), channel_id=1, source_target_pairs={{0,2},{1,3},{2,0},{3,1},{4,6},{5,7},{6,4},{7,5},{8,10},{9,11},{10,... | collective-permute-start | bytes 983048 | tf_op jit(solution)/shard_map/ppermute | solution.py:370
  (6 other events, 9.0 us)

commit v2 on v1

--- a/solution.py
+++ b/solution.py
@@ -14,7 +14,7 @@
 N_SEL = 16
 LANES = 2 * HD
 SPAN_PAD = 32
-CHUNKS = 4
+SLOT_STEPS = (8, 12)
 LOW = -1e30
 FLOOR = -1e29
 EXP_SCALE = HD ** (-0.5) * 1.4426950408889634
@@ -170,7 +170,7 @@
 def attn_kernel(count, *refs):
     base_ref, own_ref, table_ref, q_ref, gate_ref, kv_ref, sm_ref = refs[:7]
     recv_refs = refs[7 : 7 + count - 1]
-    out_ref, poolk, poolv, sumk, sumv, kbuf, vbuf = refs[7 + count - 1 :]
+    out_ref, poolk, pool, sumk, sumv, kbuf, vbuf = refs[7 + count - 1 :]
     step = pl.program_id(0)
     own = own_ref[0]
     block = base_ref[0] + step
@@ -189,15 +189,15 @@
         for g in range(heads):
             for j in range(own_blocks):
                 piece = kv_ref[g, j * SB : (j + 1) * SB, :]
+                pool[g, j] = piece
                 poolk[g, j] = piece * keep
-                poolv[g, j] = piece * other + keep
             for k, recv in enumerate(recv_refs):
                 for j in range(2):
                     piece = recv[g, j * SB : (j + 1) * SB, :]
+                    pool[g, own_blocks + 2 * k + j] = piece
                     poolk[g, own_blocks + 2 * k + j] = piece * keep
-                    poolv[g, own_blocks + 2 * k + j] = piece * other + keep
+            pool[g, total_blocks] = jnp.zeros((SB, LANES), BF16)
             poolk[g, total_blocks] = jnp.where(lane == HD, LOW, 0.0).astype(BF16)
-            poolv[g, total_blocks] = jnp.zeros((SB, LANES), BF16)
             for k in range(count):
                 piece = sm_ref[g] if k == 0 else recv_refs[k - 1][g, 2 * SB :, :]
                 sumv[g, k * SPAN_PAD : (k + 1) * SPAN_PAD] = piece * other[:SPAN_PAD] + keep[:SPAN_PAD]
@@ -215,44 +215,59 @@
     contract = (((1,), (1,)), ((), ()))
     low_half = lane < HD
     for g in range(heads):
-        for s in range(N_SEL):
-            place = table_ref[block, g * N_SEL + s]
-            piece = poolk[g, place]
-            if s == 0:
-                piece = piece + diagonal
-            kbuf[g, s * SB : (s + 1) * SB, :] = piece
-            vbuf[g, s * SB : (s + 1) * SB, :] = poolv[g, place]
         sumk[g, 0:SPAN_PAD] = sm_ref[g] * keep[:SPAN_PAD] + bias
-        q = q_ref[g * group : (g + 1) * group].reshape(group * SB, LANES)
-        score = lax.dot_general(q, kbuf[g], contract, preferred_element_type=F32)
-        top = jnp.max(score, axis=1, keepdims=True)
-        weight = jnp.exp2((score - top) * EXP_SCALE).astype(BF16)
-        picked = jnp.dot(weight, vbuf[g], preferred_element_type=F32)
-        score = lax.dot_general(q, sumk[g], contract, preferred_element_type=F32)
-        top = jnp.maximum(jnp.max(score, axis=1, keepdims=True), FLOOR)
-        weight = jnp.exp2((score - top) * EXP_SCALE).astype(BF16)
-        summed = jnp.dot(weight, sumv[g], preferred_element_type=F32)
-        for pair in range(group // 2):
-            mixed = []
-            for r in (2 * pair, 2 * pair + 1):
-                h = g * group + r
-                a = summed[r * SB : (r + 1) * SB]
-                c = picked[r * SB : (r + 1) * SB]
-                ca = gate_ref[:, 2 * h : 2 * h + 1] / jnp.maximum(a, 1e-30)
-                cc = gate_ref[:, 2 * h + 1 : 2 * h + 2] / c
-                if r % 2 == 0:
-                    mixed.append(pltpu.roll(a, HD, 1) * ca + pltpu.roll(c, HD, 1) * cc)
+
+    def one(slots):
+        for g in range(heads):
+            for s in range(slots):
+                place = table_ref[block, g * N_SEL + s]
+                piece = pool[g, place]
+                if s == 0:
+                    kbuf[g, s * SB : (s + 1) * SB, :] = piece * keep + diagonal
                 else:
-                    mixed.append(a * pltpu.roll(ca, HD, 1) + c * pltpu.roll(cc, HD, 1))
-            both = jnp.where(low_half, mixed[0], mixed[1]).astype(BF16)
-            at = (g * group) // 2 + pair
-            out_ref[:, at * LANES : (at + 1) * LANES] = both
+                    kbuf[g, s * SB : (s + 1) * SB, :] = poolk[g, place]
+                vbuf[g, s * SB : (s + 1) * SB, :] = piece * other + keep
+            q = q_ref[g * group : (g + 1) * group].reshape(group * SB, LANES)
+            score = lax.dot_general(q, kbuf[g, : slots * SB], contract, preferred_element_type=F32)
+            top = jnp.max(score, axis=1, keepdims=True)
+            weight = jnp.exp2((score - top) * EXP_SCALE).astype(BF16)
+            picked = jnp.dot(weight, vbuf[g, : slots * SB], preferred_element_type=F32)
+            score = lax.dot_general(q, sumk[g], contract, preferred_element_type=F32)
+            top = jnp.maximum(jnp.max(score, axis=1, keepdims=True), FLOOR)
+            weight = jnp.exp2((score - top) * EXP_SCALE).astype(BF16)
+            summed = jnp.dot(weight, sumv[g], preferred_element_type=F32)
+            for pair in range(group // 2):
+                mixed = []
+                for r in (2 * pair, 2 * pair + 1):
+                    h = g * group + r
+                    a = summed[r * SB : (r + 1) * SB]
+                    c = picked[r * SB : (r + 1) * SB]
+                    ca = gate_ref[:, 2 * h : 2 * h + 1] / jnp.maximum(a, 1e-30)
+                    cc = gate_ref[:, 2 * h + 1 : 2 * h + 2] / c
+                    if r % 2 == 0:
+                        mixed.append(pltpu.roll(a, HD, 1) * ca + pltpu.roll(c, HD, 1) * cc)
+                    else:
+                        mixed.append(a * pltpu.roll(ca, HD, 1) + c * pltpu.roll(cc, HD, 1))
+                both = jnp.where(low_half, mixed[0], mixed[1]).astype(BF16)
+                at = (g * group) // 2 + pair
+                out_ref[:, at * LANES : (at + 1) * LANES] = both
+
+    def past(slots):
+        named = [table_ref[block, g * N_SEL + slots] != total_blocks for g in range(heads)]
+        return functools.reduce(jnp.logical_or, named)
+
+    sizes = [slots for slots in SLOT_STEPS if slots < N_SEL] + [N_SEL]
+    for k, slots in enumerate(sizes):
+        taken = past(sizes[k - 1]) if k else None
+        if slots < N_SEL:
+            short = jnp.logical_not(past(slots))
+            taken = short if taken is None else jnp.logical_and(taken, short)
+        pl.when(taken)(functools.partial(one, slots))
 
 
 def attend(count, blocks, base, own, table, q, gates, kv, summaries, received):
     heads, rows = kv.shape[0], kv.shape[1]
     total = rows // SB + 2 * (count - 1)
-    full = lambda shape: pl.BlockSpec(shape, lambda i, *s: (0,) * len(shape))
     return pl.pallas_call(
         functools.partial(attn_kernel, count),
         grid_spec=pltpu.PrefetchScalarGridSpec(
@@ -261,9 +276,7 @@
             in_specs=[
                 pl.BlockSpec((q.shape[0], SB, LANES), lambda i, base, *s: (0, base[0] + i, 0)),
                 pl.BlockSpec((SB, gates.shape[1]), lambda i, base, *s: (base[0] + i, 0)),
-                full(kv.shape),
-                full(summaries.shape),
-                *[full(r.shape) for r in received],
+                *[pl.BlockSpec(memory_space=pltpu.VMEM)] * (2 + len(received)),
             ],
             out_specs=pl.BlockSpec((SB, q.shape[0] * HD), lambda i, *s: (i, 0)),
             scratch_shapes=[
@@ -357,28 +370,30 @@
 
     swap = [(i, i ^ 1) for i in range(parts)]
     cross = [(i, i ^ 2) for i in range(parts)]
-    width = out_weight.shape[1] // CHUNKS
+    width = out_weight.shape[1]
+    moved = width // 2
+    left, right = out_weight[:, :moved], out_weight[:, moved:]
+    other_left = lax.ppermute(left, "tp", cross)
     far = halves(1 - half)
-    far_keep, far_send = rows_of(far, core), rows_of(far, 1 - core)
-    crossed = []
-    for c in range(CHUNKS):
-        columns = out_weight[:, c * width : (c + 1) * width]
-        piece = product(far_send, columns)
-        got = lax.ppermute(piece, "tp", swap)
-        kept = product(far_keep, columns)
-        both = (got.astype(F32) + kept.astype(F32)).astype(BF16)
-        crossed.append(lax.ppermute(both, "tp", cross))
+    other_near = lax.ppermute(far, "tp", cross)
+    piece = product(rows_of(far, 1 - core), right)
+    got = lax.ppermute(piece, "tp", swap)
+    both = (got.astype(F32) + product(rows_of(far, core), right).astype(F32)).astype(BF16)
+    crossed = lax.ppermute(both, "tp", cross)
     near = halves(half)
-    got = lax.ppermute(product(rows_of(near, 1 - core), out_weight), "tp", swap)
-    kept = product(rows_of(near, core), out_weight)
-    base = got.astype(F32) + kept.astype(F32)
-    return jnp.concatenate(
-        [
-            (base[:, c * width : (c + 1) * width] + crossed[c].astype(F32)).astype(BF16)
-            for c in range(CHUNKS)
-        ],
-        axis=1,
-    )
+
+    def near_product(which):
+        mine, its = rows_of(near, which), rows_of(other_near, which)
+        total = jnp.dot(mine, left, preferred_element_type=F32) + jnp.dot(its, other_left, preferred_element_type=F32)
+        return total.astype(BF16), product(mine, right)
+
+    send_left, send_right = near_product(1 - core)
+    got_left = lax.ppermute(send_left, "tp", swap)
+    got_right = lax.ppermute(send_right, "tp", swap)
+    keep_left, keep_right = near_product(core)
+    out_left = (got_left.astype(F32) + keep_left.astype(F32)).astype(BF16)
+    out_right = (got_right.astype(F32) + keep_right.astype(F32) + crossed.astype(F32)).astype(BF16)
+    return jnp.concatenate([out_left, out_right], axis=1)
 
 
 def solution(mesh):

time: 113 us -> 101 us (0.89)
  waiting for transfers between devices: 29.4 us -> 18.1 us
  local copies, waits for them, and re-layouts: 1.49 us -> 4.66 us
  Pallas kernels: 38.6 us -> 36.3 us
  matrix products: 7.3 us -> 6.16 us
    ppermute x5, waiting for transfers between devices: 24.9 us -> 13.6 us  [the longest x1 13.6 us: local(): crossed = lax.ppermute(both, 'tp', cross)]
    dot_general x10 -> x4, matrix products: 7.3 us -> 3.99 us  [product(): return jnp.dot(att, columns, preferred_element_type=F32).astype(BF16)]
    slice x0 -> x1, local copies, waits for them, and re-layouts: none -> 3.17 us  [local(): left, right = (out_weight[:, :moved], out_weight[:, moved:])]
    dot_general x0 -> x4, matrix products: none -> 2.17 us  [the longest x2 1.15 us: near_product(): jnp.dot(mine, left, preferred_element_type=F32)]
    pallas_call x2, Pallas kernels: 25.7 us -> 23.5 us  [attend(): pl.pallas_call(functools.partial(attn_kernel, count), grid_spec=pltpu.Pre...]
  transfers between devices with their start and end apart: 19 -> 16, of which waited for: 8 -> 4; matrix products, arithmetic and copies ran while one was open for 6% -> 13% of each run, Pallas kernels for 21% -> 36%
where the time goes in v2:
time: 101 us; the launch traced here: 99.7 us
  Pallas kernels  36.3 us (36%)
  starting transfers between devices  28.8 us (29%)
  waiting for transfers between devices  18.1 us (18%)
  matrix products  6.16 us (6%)
  other arithmetic  5.19 us (5%)
  local copies, waits for them, and re-layouts  4.66 us (5%)
    pallas_call x2, Pallas kernels, attend(): pl.pallas_call(functools.partial(attn_kernel, count), grid_spec=pltpu.Pre...  23.5 us
    ppermute x7, starting transfers between devices, local(): lax.ppermute(pieces[k - 1], 'kv', [(i, i + k) for i in range(count - k)])  17.5 us
    ppermute x1, waiting for transfers between devices, local(): crossed = lax.ppermute(both, 'tp', cross)  13.6 us
    pallas_call x1, Pallas kernels, project(): pl.pallas_call(proj_kernel, grid_spec=pltpu.PrefetchScalarGridSpec(num_sc...  10.9 us
    ppermute x3, starting transfers between devices, local(): got = lax.ppermute(everyone, 'kv', [(i, i ^ bit) for i in range(count)])  7.17 us
    dot_general x4, matrix products, product(): return jnp.dot(att, columns, preferred_element_type=F32).astype(BF16)  3.99 us
    slice x1, local copies, waits for them, and re-layouts, local(): left, right = (out_weight[:, :moved], out_weight[:, moved:])  3.17 us
    ppermute x3, waiting for transfers between devices, local(): got = lax.ppermute(everyone, 'kv', [(i, i ^ bit) for i in range(count)])  3.08 us
  transfers between devices with their start and end apart: 16, of which 4 were waited for; matrix products, arithmetic and copies ran while one was open for 13% of the time, Pallas kernels for 36%

profile of v2, /device:TPU:0, one launch (start us, length us, event | category | flops | bytes accessed | tf_op | source)
XLA Modules:
  0.0 99.7 jit_solution(14350964015989840479)
XLA Ops:
  1.2 3.0 %collective-permute-start = (s32[8,32]{1,0:T(8,128)S(1)}, s32[8,32]{1,0:T(8,128)S(1)}, u32[]{:S(2)}, u32[]{:S(2)}) collective-permute-start(s32[8,32]{1,0:T(8,128)S(1)} %broadcast_select_fusion.1), channel_id=1, source_target_pairs={{0,4},{4,0},{8,12},{12,8},{16,20},{20,16},{24,28},{28,24},{1,5},{5... | collective-permute-start | bytes 3080 | tf_op jit(solution)/shard_map/ppermute | solution.py:321
  4.2 3.2 %slice.6 = bf16[512,2048]{1,0:T(8,128)(2,1)} slice(bf16[512,4096]{1,0:T(8,128)(2,1)} %param.18), slice={[0:512], [0:2048]} | slice | bytes 4194304 | tf_op jit(solution)/shard_map/slice | solution.py:375
  7.4 1.5 %collective-permute-start.11 = (bf16[512,2048]{1,0:T(8,128)(2,1)}, bf16[512,2048]{1,0:T(8,128)(2,1)S(1)}, u32[]{:S(2)}, u32[]{:S(2)}) collective-permute-start(bf16[512,2048]{1,0:T(8,128)(2,1)} %slice.6), channel_id=1, source_target_pairs={{0,2},{1,3},{2,0},{3,1},{4,6},{5,7},{6,4},{7,5},{8,10},{9,11},{10,... | collective-permute-start | bytes 6291464 | tf_op jit(solution)/shard_map/ppermute | solution.py:376
  8.9 10.9 %project.1 = (bf16[8,640,128]{2,1,0:T(8,128)(2,1)}, f32[640,16]{1,0:T(8,128)}, bf16[2,640,128]{2,1,0:T(8,128)(2,1)}, bf16[2,32,128]{2,1,0:T(8,128)(2,1)}) custom-call(s32[1]{0:T(128)} %bitcast.4.part_ref, bf16[640,4096]{1,0:T(8,128)(2,1)} %tok_ref.1, bf16[4096,512]{1,0:T(8,128)(2,1)} %wq_ref.1, bf16[4096,128]{1,0:T(8,128)(2,1)} %wk_ref.1, ...), custom_call_target="tpu_custom_call" | custom-call | flops 4697620480 | bytes 9437184 | tf_op jit(solution)/shard_map/project/pallas_call | solution.py:105
  20.6 1.6 %collective-permute-start.1 = (s32[8,32]{1,0:T(8,128)S(1)}, s32[8,32]{1,0:T(8,128)S(1)}, u32[]{:S(2)}, u32[]{:S(2)}) collective-permute-start(s32[8,32]{1,0:T(8,128)S(1)} %fusion.36), channel_id=1, source_target_pairs={{0,8},{4,12},{8,0},{12,4},{16,24},{20,28},{24,16},{28,20},{1,9},{5... | collective-permute-start | bytes 3080 | tf_op jit(solution)/shard_map/ppermute | solution.py:321
  22.6 1.6 %collective-permute-done.1 = s32[8,32]{1,0:T(8,128)S(1)} collective-permute-done((s32[8,32]{1,0:T(8,128)S(1)}, s32[8,32]{1,0:T(8,128)S(1)}, u32[]{:S(2)}, u32[]{:S(2)}) %collective-permute-start.1) | collective-permute-done | bytes 1056 | tf_op jit(solution)/shard_map/ppermute | solution.py:321
  24.3 2.6 %collective-permute-start.2 = (s32[8,32]{1,0:T(8,128)S(1)}, s32[8,32]{1,0:T(8,128)S(1)}, u32[]{:S(2)}, u32[]{:S(2)}) collective-permute-start(s32[8,32]{1,0:T(8,128)S(1)} %fusion.41), channel_id=1, source_target_pairs={{0,16},{4,20},{8,24},{12,28},{16,0},{20,4},{24,8},{28,12},{1,17},{... | collective-permute-start | bytes 3080 | tf_op jit(solution)/shard_map/ppermute | solution.py:321
  27.3 1.5 %collective-permute-done.2 = s32[8,32]{1,0:T(8,128)S(1)} collective-permute-done((s32[8,32]{1,0:T(8,128)S(1)}, s32[8,32]{1,0:T(8,128)S(1)}, u32[]{:S(2)}, u32[]{:S(2)}) %collective-permute-start.2) | collective-permute-done | bytes 1056 | tf_op jit(solution)/shard_map/ppermute | solution.py:321
  29.4 1.9 %select_blocks.1 = (bf16[2,160,128]{2,1,0:T(8,128)(2,1)}, bf16[2,160,128]{2,1,0:T(8,128)(2,1)}, bf16[2,160,128]{2,1,0:T(8,128)(2,1)}, bf16[2,160,128]{2,1,0:T(8,...) custom-call(s32[1]{0:T(128)} %bitcast.1.own_ref.refs_1_, ...), custom_call_target="tpu_custom_call" | custom-call | tf_op jit(solution)/shard_map/select_blocks/pallas_call | solution.py:160
  31.3 2.4 %collective-permute-start.3 = (bf16[2,160,128]{2,1,0:T(8,128)(2,1)}, bf16[2,160,128]{2,1,0:T(8,128)(2,1)S(1)}, u32[]{:S(2)}, u32[]{:S(2)}) collective-permute-start(bf16[2,160,128]{2,1,0:T(8,128)(2,1)} %get-tuple-element.22), channel_id=1, source_target_pairs={{0,4},{4,8},{8,12},{12,16},{16,20},{20,24},{24,28},{1,5},{5,9},{9,... | collective-permute-start | bytes 245768 | tf_op jit(solution)/shard_map/ppermute | solution.py:337
  33.7 3.5 %collective-permute-start.4 = (bf16[2,160,128]{2,1,0:T(8,128)(2,1)}, bf16[2,160,128]{2,1,0:T(8,128)(2,1)S(1)}, u32[]{:S(2)}, u32[]{:S(2)}) collective-permute-start(bf16[2,160,128]{2,1,0:T(8,128)(2,1)} %get-tuple-element.23), channel_id=1, source_target_pairs={{0,8},{4,12},{8,16},{12,20},{16,24},{20,28},{1,9},{5,13},{9,17},{1... | collective-permute-start | bytes 245768 | tf_op jit(solution)/shard_map/ppermute | solution.py:337
  37.2 5.5 %collective-permute-start.5 = (bf16[2,160,128]{2,1,0:T(8,128)(2,1)}, bf16[2,160,128]{2,1,0:T(8,128)(2,1)S(1)}, u32[]{:S(2)}, u32[]{:S(2)}) collective-permute-start(bf16[2,160,128]{2,1,0:T(8,128)(2,1)} %get-tuple-element.24), channel_id=1, source_target_pairs={{0,12},{4,16},{8,20},{12,24},{16,28},{1,13},{5,17},{9,21},{13,25},... | collective-permute-start | bytes 245768 | tf_op jit(solution)/shard_map/ppermute | solution.py:337
  43.1 1.3 %collective-permute-start.6 = (bf16[2,160,128]{2,1,0:T(8,128)(2,1)}, bf16[2,160,128]{2,1,0:T(8,128)(2,1)S(1)}, u32[]{:S(2)}, u32[]{:S(2)}) collective-permute-start(bf16[2,160,128]{2,1,0:T(8,128)(2,1)} %get-tuple-element.25), channel_id=1, source_target_pairs={{0,16},{4,20},{8,24},{12,28},{1,17},{5,21},{9,25},{13,29},{2,18},{... | collective-permute-start | bytes 245768 | tf_op jit(solution)/shard_map/ppermute | solution.py:337
  44.4 1.3 %collective-permute-start.7 = (bf16[2,160,128]{2,1,0:T(8,128)(2,1)}, bf16[2,160,128]{2,1,0:T(8,128)(2,1)S(1)}, u32[]{:S(2)}, u32[]{:S(2)}) collective-permute-start(bf16[2,160,128]{2,1,0:T(8,128)(2,1)} %get-tuple-element.26), channel_id=1, source_target_pairs={{0,20},{4,24},{8,28},{1,21},{5,25},{9,29},{2,22},{6,26},{10,30},{3... | collective-permute-start | bytes 245768 | tf_op jit(solution)/shard_map/ppermute | solution.py:337
  45.7 1.3 %collective-permute-start.8 = (bf16[2,160,128]{2,1,0:T(8,128)(2,1)}, bf16[2,160,128]{2,1,0:T(8,128)(2,1)S(1)}, u32[]{:S(2)}, u32[]{:S(2)}) collective-permute-start(bf16[2,160,128]{2,1,0:T(8,128)(2,1)} %get-tuple-element.27), channel_id=1, source_target_pairs={{0,24},{4,28},{1,25},{5,29},{2,26},{6,30},{3,27},{7,31}} | collective-permute-start | bytes 245768 | tf_op jit(solution)/shard_map/ppermute | solution.py:337
  47.1 2.2 %collective-permute-start.9 = (bf16[2,160,128]{2,1,0:T(8,128)(2,1)}, bf16[2,160,128]{2,1,0:T(8,128)(2,1)S(1)}, u32[]{:S(2)}, u32[]{:S(2)}) collective-permute-start(bf16[2,160,128]{2,1,0:T(8,128)(2,1)} %get-tuple-element.28), channel_id=1, source_target_pairs={{0,28},{1,29},{2,30},{3,31}} | collective-permute-start | bytes 245768 | tf_op jit(solution)/shard_map/ppermute | solution.py:337
  50.1 1.4 %collective-permute-done.9.refs_13_ = bf16[2,160,128]{2,1,0:T(8,128)(2,1)S(1)} collective-permute-done((bf16[2,160,128]{2,1,0:T(8,128)(2,1)}, bf16[2,160,128]{2,1,0:T(8,128)(2,1)S(1)}, u32[]{:S(2)}, u32[]{:S(2)}) %collective-permute-start.9) | collective-permute-done | bytes 81952 | tf_op jit(solution)/shard_map/ppermute | solution.py:337
  52.1 11.8 %attend.3 = bf16[320,512]{1,0:T(8,128)(2,1)} custom-call(s32[1]{0:T(128)} %bitcast.8.refs_0_, s32[1]{0:T(128)} %bitcast.1.own_ref.refs_1_, s32[10,32]{1,0:T(8,128)} %select_n.69.refs_2_, bf16[8,640,128]{2,1,0:T(8,128)(2,1)} %get-tuple-element.18.refs_3_, f32[640,16]{1,0:T(8,128)} %get-tuple-element.19.refs_4_, ...), custom_call_target="tpu_custom_call" | custom-call | flops 1677721600 | bytes 655360 | tf_op jit(solution)/shard_map/attend/pallas_call | solution.py:271
  63.9 1.4 %convolution_convert_fusion.1 = bf16[160,2048]{1,0:T(8,128)(2,1)S(1)} fusion(bf16[512,4096]{1,0:T(8,128)(2,1)S(1)} %copy-done, bf16[320,512]{1,0:T(8,128)(2,1)} %attend.3, s32[]{:T(128)S(6)} %select_n.71), kind=kOutput, calls=%fused_computation.7 | convolution fusion | flops 335872000 | bytes 2916356 | tf_op jit(solution)/shard_map/dot_general | solution.py:366
  66.0 11.8 %attend.2 = bf16[320,512]{1,0:T(8,128)(2,1)} custom-call(s32[1]{0:T(128)} %bitcast.refs_0_, s32[1]{0:T(128)} %bitcast.1.own_ref.refs_1_, s32[10,32]{1,0:T(8,128)} %select_n.69.refs_2_, bf16[8,640,128]{2,1,0:T(8,128)(2,1)} %get-tuple-element.18.refs_3_, f32[640,16]{1,0:T(8,128)} %get-tuple-element.19.refs_4_, ...), custom_call_target="tpu_custom_call" | custom-call | flops 1677721600 | bytes 655360 | tf_op jit(solution)/shard_map/attend/pallas_call | solution.py:271
  77.8 1.5 %convolution_convert_fusion.3 = bf16[160,2048]{1,0:T(8,128)(2,1)S(1)} fusion(bf16[512,4096]{1,0:T(8,128)(2,1)S(1)} %copy-done.1, bf16[320,512]{1,0:T(8,128)(2,1)} %attend.2, s32[]{:T(128)S(6)} %select_n.71), kind=kOutput, calls=%fused_computation.10 | convolution fusion | flops 335872000 | bytes 2916356 | tf_op jit(solution)/shard_map/dot_general | solution.py:366
  80.1 1.6 %collective-permute-start.15 = (bf16[160,2048]{1,0:T(8,128)(2,1)S(1)}, bf16[160,2048]{1,0:T(8,128)(2,1)S(1)}, u32[]{:S(2)}, u32[]{:S(2)}) collective-permute-start(bf16[160,2048]{1,0:T(8,128)(2,1)S(1)} %add_convert_fusion.1), channel_id=1, source_target_pairs={{0,2},{1,3},{2,0},{3,1},{4,6},{5,7},{6,4},{7,5},{8,10},{9,11},{10,... | collective-permute-start | bytes 1966088 | tf_op jit(solution)/shard_map/ppermute | solution.py:382
  83.5 13.6 %collective-permute-done.15 = bf16[160,2048]{1,0:T(8,128)(2,1)S(1)} collective-permute-done((bf16[160,2048]{1,0:T(8,128)(2,1)S(1)}, bf16[160,2048]{1,0:T(8,128)(2,1)S(1)}, u32[]{:S(2)}, u32[]{:S(2)}) %collective-permute-start.15) | collective-permute-done | bytes 655392 | tf_op jit(solution)/shard_map/ppermute | solution.py:382
  98.5 1.1 %pad_maximum_fusion = bf16[160,4096]{1,0:T(8,128)(2,1)} fusion(bf16[160,2048]{1,0:T(8,128)(2,1)S(1)} %add_convert_fusion, bf16[160,2048]{1,0:T(8,128)(2,1)S(1)} %add_convert_fusion.2), kind=kLoop, calls=%fused_computation.15 | loop fusion | flops 2621440 | bytes 2621440 | tf_op jit(solution)/shard_map/concatenate | solution.py:396
  (68 shorter events, 9.9 us)
Async XLA Ops:
  1.2 18.6 %collective-permute-start = (s32[8,32]{1,0:T(8,128)S(1)}, s32[8,32]{1,0:T(8,128)S(1)}, u32[]{:S(2)}, u32[]{:S(2)}) collective-permute-start(s32[8,32]{1,0:T(8,128)S(1)} %broadcast_select_fusion.1), channel_id=1, source_target_pairs={{0,4},{4,0},{8,12},{12,8},{16,20},{20,16},{24,28},{28,24},{1,5},{5... | collective-permute-start | bytes 3080 | tf_op jit(solution)/shard_map/ppermute | solution.py:321
  7.4 74.8 %collective-permute-start.11 = (bf16[512,2048]{1,0:T(8,128)(2,1)}, bf16[512,2048]{1,0:T(8,128)(2,1)S(1)}, u32[]{:S(2)}, u32[]{:S(2)}) collective-permute-start(bf16[512,2048]{1,0:T(8,128)(2,1)} %slice.6), channel_id=1, source_target_pairs={{0,2},{1,3},{2,0},{3,1},{4,6},{5,7},{6,4},{7,5},{8,10},{9,11},{10,... | collective-permute-start | bytes 6291464 | tf_op jit(solution)/shard_map/ppermute | solution.py:376
  8.9 10.9 %copy-start.3 = (s32[10,2,16]{2,1,0:T(2,128)S(1)}, s32[10,2,16]{2,1,0:T(2,128)}, u32[]{:S(2)}) copy-start(s32[10,2,16]{2,1,0:T(2,128)} %param.19) | copy-start | bytes 3844
  20.6 3.6 %collective-permute-start.1 = (s32[8,32]{1,0:T(8,128)S(1)}, s32[8,32]{1,0:T(8,128)S(1)}, u32[]{:S(2)}, u32[]{:S(2)}) collective-permute-start(s32[8,32]{1,0:T(8,128)S(1)} %fusion.36), channel_id=1, source_target_pairs={{0,8},{4,12},{8,0},{12,4},{16,24},{20,28},{24,16},{28,20},{1,9},{5... | collective-permute-start | bytes 3080 | tf_op jit(solution)/shard_map/ppermute | solution.py:321
  24.3 4.5 %collective-permute-start.2 = (s32[8,32]{1,0:T(8,128)S(1)}, s32[8,32]{1,0:T(8,128)S(1)}, u32[]{:S(2)}, u32[]{:S(2)}) collective-permute-start(s32[8,32]{1,0:T(8,128)S(1)} %fusion.41), channel_id=1, source_target_pairs={{0,16},{4,20},{8,24},{12,28},{16,0},{20,4},{24,8},{28,12},{1,17},{... | collective-permute-start | bytes 3080 | tf_op jit(solution)/shard_map/ppermute | solution.py:321
  31.3 13.1 %collective-permute-start.3 = (bf16[2,160,128]{2,1,0:T(8,128)(2,1)}, bf16[2,160,128]{2,1,0:T(8,128)(2,1)S(1)}, u32[]{:S(2)}, u32[]{:S(2)}) collective-permute-start(bf16[2,160,128]{2,1,0:T(8,128)(2,1)} %get-tuple-element.22), channel_id=1, source_target_pairs={{0,4},{4,8},{8,12},{12,16},{16,20},{20,24},{24,28},{1,5},{5,9},{9,... | collective-permute-start | bytes 245768 | tf_op jit(solution)/shard_map/ppermute | solution.py:337
  33.7 12.0 %collective-permute-start.4 = (bf16[2,160,128]{2,1,0:T(8,128)(2,1)}, bf16[2,160,128]{2,1,0:T(8,128)(2,1)S(1)}, u32[]{:S(2)}, u32[]{:S(2)}) collective-permute-start(bf16[2,160,128]{2,1,0:T(8,128)(2,1)} %get-tuple-element.23), channel_id=1, source_target_pairs={{0,8},{4,12},{8,16},{12,20},{16,24},{20,28},{1,9},{5,13},{9,17},{1... | collective-permute-start | bytes 245768 | tf_op jit(solution)/shard_map/ppermute | solution.py:337
  37.2 9.9 %collective-permute-start.5 = (bf16[2,160,128]{2,1,0:T(8,128)(2,1)}, bf16[2,160,128]{2,1,0:T(8,128)(2,1)S(1)}, u32[]{:S(2)}, u32[]{:S(2)}) collective-permute-start(bf16[2,160,128]{2,1,0:T(8,128)(2,1)} %get-tuple-element.24), channel_id=1, source_target_pairs={{0,12},{4,16},{8,20},{12,24},{16,28},{1,13},{5,17},{9,21},{13,25},... | collective-permute-start | bytes 245768 | tf_op jit(solution)/shard_map/ppermute | solution.py:337
  43.1 6.9 %collective-permute-start.6 = (bf16[2,160,128]{2,1,0:T(8,128)(2,1)}, bf16[2,160,128]{2,1,0:T(8,128)(2,1)S(1)}, u32[]{:S(2)}, u32[]{:S(2)}) collective-permute-start(bf16[2,160,128]{2,1,0:T(8,128)(2,1)} %get-tuple-element.25), channel_id=1, source_target_pairs={{0,16},{4,20},{8,24},{12,28},{1,17},{5,21},{9,25},{13,29},{2,18},{... | collective-permute-start | bytes 245768 | tf_op jit(solution)/shard_map/ppermute | solution.py:337
  44.4 7.1 %copy-start.5 = (bf16[2,160,128]{2,1,0:T(8,128)(2,1)}, bf16[2,160,128]{2,1,0:T(8,128)(2,1)S(1)}, u32[]{:S(2)}) copy-start(bf16[2,160,128]{2,1,0:T(8,128)(2,1)S(1)} %collective-permute-done.3.refs_7_) | copy-start | bytes 245764
  44.4 5.6 %collective-permute-start.7 = (bf16[2,160,128]{2,1,0:T(8,128)(2,1)}, bf16[2,160,128]{2,1,0:T(8,128)(2,1)S(1)}, u32[]{:S(2)}, u32[]{:S(2)}) collective-permute-start(bf16[2,160,128]{2,1,0:T(8,128)(2,1)} %get-tuple-element.26), channel_id=1, source_target_pairs={{0,20},{4,24},{8,28},{1,21},{5,25},{9,29},{2,22},{6,26},{10,30},{3... | collective-permute-start | bytes 245768 | tf_op jit(solution)/shard_map/ppermute | solution.py:337
  45.7 5.8 %copy-start.6 = (bf16[2,160,128]{2,1,0:T(8,128)(2,1)}, bf16[2,160,128]{2,1,0:T(8,128)(2,1)S(1)}, u32[]{:S(2)}) copy-start(bf16[2,160,128]{2,1,0:T(8,128)(2,1)S(1)} %collective-permute-done.4.refs_8_) | copy-start | bytes 245764
  45.7 4.3 %collective-permute-start.8 = (bf16[2,160,128]{2,1,0:T(8,128)(2,1)}, bf16[2,160,128]{2,1,0:T(8,128)(2,1)S(1)}, u32[]{:S(2)}, u32[]{:S(2)}) collective-permute-start(bf16[2,160,128]{2,1,0:T(8,128)(2,1)} %get-tuple-element.27), channel_id=1, source_target_pairs={{0,24},{4,28},{1,25},{5,29},{2,26},{6,30},{3,27},{7,31}} | collective-permute-start | bytes 245768 | tf_op jit(solution)/shard_map/ppermute | solution.py:337
  47.1 4.4 %copy-start.7 = (bf16[2,160,128]{2,1,0:T(8,128)(2,1)}, bf16[2,160,128]{2,1,0:T(8,128)(2,1)S(1)}, u32[]{:S(2)}) copy-start(bf16[2,160,128]{2,1,0:T(8,128)(2,1)S(1)} %collective-permute-done.5.refs_9_) | copy-start | bytes 245764
  47.1 4.4 %collective-permute-start.9 = (bf16[2,160,128]{2,1,0:T(8,128)(2,1)}, bf16[2,160,128]{2,1,0:T(8,128)(2,1)S(1)}, u32[]{:S(2)}, u32[]{:S(2)}) collective-permute-start(bf16[2,160,128]{2,1,0:T(8,128)(2,1)} %get-tuple-element.28), channel_id=1, source_target_pairs={{0,28},{1,29},{2,30},{3,31}} | collective-permute-start | bytes 245768 | tf_op jit(solution)/shard_map/ppermute | solution.py:337
  52.1 11.8 %copy-start = (bf16[512,4096]{1,0:T(8,128)(2,1)S(1)}, bf16[512,4096]{1,0:T(8,128)(2,1)}, u32[]{:S(2)}) copy-start(bf16[512,4096]{1,0:T(8,128)(2,1)} %param.18) | copy-start | bytes 12582916
  65.3 14.2 %collective-permute-start.14 = (bf16[160,2048]{1,0:T(8,128)(2,1)S(1)}, bf16[160,2048]{1,0:T(8,128)(2,1)S(1)}, u32[]{:S(2)}, u32[]{:S(2)}) collective-permute-start(bf16[160,2048]{1,0:T(8,128)(2,1)S(1)} %convolution_convert_fusion.1), channel_id=1, source_target_pairs={{0,1},{1,0},{2,3},{3,2},{4,5},{5,4},{6,7},{7,6},{8,9},{9,8},{10,11... | collective-permute-start | bytes 1966088 | tf_op jit(solution)/shard_map/ppermute | solution.py:380
  65.4 16.8 %collective-permute-start.10 = (bf16[320,512]{1,0:T(8,128)(2,1)}, bf16[320,512]{1,0:T(8,128)(2,1)S(1)}, u32[]{:S(2)}, u32[]{:S(2)}) collective-permute-start(bf16[320,512]{1,0:T(8,128)(2,1)} %attend.3), channel_id=1, source_target_pairs={{0,2},{1,3},{2,0},{3,1},{4,6},{5,7},{6,4},{7,5},{8,10},{9,11},{10,... | collective-permute-start | bytes 983048 | tf_op jit(solution)/shard_map/ppermute | solution.py:378
  66.0 11.8 %copy-start.1 = (bf16[512,4096]{1,0:T(8,128)(2,1)S(1)}, bf16[512,4096]{1,0:T(8,128)(2,1)}, u32[]{:S(2)}) copy-start(bf16[512,4096]{1,0:T(8,128)(2,1)} %param.18) | copy-start | bytes 12582916
  77.8 1.7 %copy-start.4 = (bf16[320,512]{1,0:T(8,128)(2,1)S(1)}, bf16[320,512]{1,0:T(8,128)(2,1)}, u32[]{:S(2)}) copy-start(bf16[320,512]{1,0:T(8,128)(2,1)} %attend.3) | copy-start | bytes 983044
  79.3 2.3 %copy-start.2 = (bf16[320,512]{1,0:T(8,128)(2,1)S(1)}, bf16[320,512]{1,0:T(8,128)(2,1)}, u32[]{:S(2)}) copy-start(bf16[320,512]{1,0:T(8,128)(2,1)} %attend.2) | copy-start | bytes 983044
  79.3 4.2 %collective-permute-start.13 = (bf16[160,2048]{1,0:T(8,128)(2,1)S(1)}, bf16[160,2048]{1,0:T(8,128)(2,1)S(1)}, u32[]{:S(2)}, u32[]{:S(2)}) collective-permute-start(bf16[160,2048]{1,0:T(8,128)(2,1)S(1)} %convolution_convert_fusion.3), channel_id=1, source_target_pairs={{0,1},{1,0},{2,3},{3,2},{4,5},{5,4},{6,7},{7,6},{8,9},{9,8},{10,11... | collective-permute-start | bytes 1966088 | tf_op jit(solution)/shard_map/ppermute | solution.py:392
  80.1 17.1 %collective-permute-start.15 = (bf16[160,2048]{1,0:T(8,128)(2,1)S(1)}, bf16[160,2048]{1,0:T(8,128)(2,1)S(1)}, u32[]{:S(2)}, u32[]{:S(2)}) collective-permute-start(bf16[160,2048]{1,0:T(8,128)(2,1)S(1)} %add_convert_fusion.1), channel_id=1, source_target_pairs={{0,2},{1,3},{2,0},{3,1},{4,6},{5,7},{6,4},{7,5},{8,10},{9,11},{10,... | collective-permute-start | bytes 1966088 | tf_op jit(solution)/shard_map/ppermute | solution.py:382
  83.3 14.6 %collective-permute-start.12 = (bf16[160,2048]{1,0:T(8,128)(2,1)S(1)}, bf16[160,2048]{1,0:T(8,128)(2,1)S(1)}, u32[]{:S(2)}, u32[]{:S(2)}) collective-permute-start(bf16[160,2048]{1,0:T(8,128)(2,1)S(1)} %fusion), channel_id=1, source_target_pairs={{0,1},{1,0},{2,3},{3,2},{4,5},{5,4},{6,7},{7,6},{8,9},{9,8},{10,11... | collective-permute-start | bytes 1966088 | tf_op jit(solution)/shard_map/ppermute | solution.py:391
  (4 other events, 5.1 us)

commit v3 on v1

v3 whole, which is shorter than its diff:
```python
import functools

import jax
import jax.numpy as jnp
from jax import lax
from jax.experimental import pallas as pl
from jax.experimental.pallas import tpu as pltpu
from jax.sharding import PartitionSpec as P


HD = 64
CMP = 32
SB = 64
N_SEL = 16
LANES = 2 * HD
SPAN_PAD = 32
UNITS = 16
FIRST_UNITS, MORE_UNITS = 3, 6
LOW = -1e30
FLOOR = -1e29
EXP_SCALE = HD ** (-0.5) * 1.4426950408889634
VMEM_LIMIT = 60 * 1024 * 1024
ATTEND_LIMIT = 24 * 1024 * 1024
PROD_LIMIT = 16 * 1024 * 1024


F32 = jnp.float32
BF16 = jnp.bfloat16


def lane_iota(rows):
    return lax.broadcasted_iota(jnp.int32, (rows, LANES), 1)


def row_iota(rows):
    return lax.broadcasted_iota(jnp.int32, (rows, LANES), 0)


def proj_kernel(part_ref, tok_ref, wq_ref, wk_ref, wv_ref, gw_ref, pos_ref, km_ref, vm_ref, wo_ref, q_ref,
                gate_ref, kv_ref, sm_ref, more_ref, tok, weight, gate_rows, acc_ref, gacc_ref, held, sems, wide_sems):
    heads, rows = q_ref.shape[0], q_ref.shape[1]
    key_heads = kv_ref.shape[0]
    gates = gate_ref.shape[1]
    steps, chunk = weight.shape[0], weight.shape[1]
    at_k, at_v = heads * HD, heads * HD + key_heads * HD
    copies = []
    for i in range(steps):
        depth = slice(i * chunk, (i + 1) * chunk)
        copies.append(
            [
                pltpu.make_async_copy(tok_ref.at[:, depth], tok.at[i], sems.at[i, 0]),
                pltpu.make_async_copy(wq_ref.at[depth, :], weight.at[i, :, :at_k], sems.at[i, 1]),
                pltpu.make_async_copy(wk_ref.at[depth, :], weight.at[i, :, at_k:at_v], sems.at[i, 2]),
                pltpu.make_async_copy(wv_ref.at[depth, :], weight.at[i, :, at_v:], sems.at[i, 3]),
            ]
        )
    start = pl.multiple_of(part_ref[0] * gates, gates)
    gate_copy = pltpu.make_async_copy(gw_ref.at[pl.ds(start, gates), :], gate_rows, wide_sems.at[0])
    ahead = 2
    for i in range(ahead):
        for copy in copies[i]:
            copy.start()
        if i == 0:
            gate_copy.start()
    unit = wo_ref.shape[1] // UNITS
    more = slice(FIRST_UNITS * unit, (FIRST_UNITS + MORE_UNITS) * unit)
    fetch = pltpu.make_async_copy(wo_ref.at[:, more], held, wide_sems.at[1])
    put = pltpu.make_async_copy(held, more_ref, wide_sems.at[2])
    for i, group in enumerate(copies):
        for copy in group:
            copy.wait()
        if i == 0:
            gate_copy.wait()
        if i + ahead < steps:
            for copy in copies[i + ahead]:
                copy.start()
        elif i + ahead == steps:
            fetch.start()
        piece = jnp.dot(tok[i], weight[i], preferred_element_type=F32)
        gpiece = lax.dot_general(
            tok[i], gate_rows[:, i * chunk : (i + 1) * chunk], (((1,), (1,)), ((), ())), preferred_element_type=F32
        )
        if i == 0:
            acc_ref[...] = piece
            gacc_ref[...] = gpiece
        else:
            acc_ref[...] += piece
            gacc_ref[...] += gpiece
    fetch.wait()
    put.start()

    lane, inner = lane_iota(rows), lax.rem(row_iota(rows), SB)
    low_half = lane < HD
    ext = jnp.where((lane == HD) | (lane - HD > inner), 1.0, 0.0)
    for h in range(heads):
        slab = acc_ref[:, (h // 2) * LANES : (h // 2 + 1) * LANES]
        if h % 2:
            slab = pltpu.roll(slab, HD, 1)
        q_ref[h] = jnp.where(low_half, slab, ext).astype(BF16)
    gate_ref[...] = jax.nn.sigmoid(gacc_ref[...])

    spans = rows // CMP
    pos = pos_ref[...].astype(F32)
    pos = jnp.concatenate([pos, pos], axis=1)
    line = lax.broadcasted_iota(jnp.int32, km_ref.shape, 0)
    eye = lax.broadcasted_iota(jnp.int32, (CMP, CMP), 0) == lax.broadcasted_iota(jnp.int32, (CMP, CMP), 1)

    def column(ref, head):
        kept = jnp.sum(jnp.where(line == head, ref[...].astype(F32), 0.0), axis=0, keepdims=True)
        return jnp.sum(jnp.where(eye, kept, 0.0), axis=1, keepdims=True)

    for g in range(key_heads):
        k = acc_ref[:, at_k + (g // 2) * LANES : at_k + (g // 2 + 1) * LANES]
        v = acc_ref[:, at_v + (g // 2) * LANES : at_v + (g // 2 + 1) * LANES]
        if g % 2 == 0:
            both = jnp.where(low_half, k, pltpu.roll(v, HD, 1))
        else:
            both = jnp.where(low_half, pltpu.roll(k, HD, 1), v)
        both = both.astype(BF16)
        kv_ref[g] = both
        head = part_ref[0] * key_heads + g
        mix = jnp.where(lane_iota(CMP) < HD, column(km_ref, head), column(vm_ref, head))
        windows = both.astype(F32).reshape(spans, CMP, LANES) + pos[None]
        total = jnp.sum(windows * mix[None], axis=1)
        pad = jnp.zeros((SPAN_PAD - spans, LANES), F32)
        sm_ref[g] = jnp.concatenate([total, pad], axis=0).astype(BF16)
    put.wait()


def project(part, tokens, query_weight, key_weight, value_weight, gate_rows, pos, kmix, vmix, out_weight):
    rows, depth = tokens.shape
    qwidth, width = query_weight.shape[1], key_weight.shape[1]
    heads, key_heads = qwidth // HD, width // HD
    steps = 4
    chunk = depth // steps
    inner, wide = out_weight.shape
    hbm = pl.BlockSpec(memory_space=pl.ANY)
    smem = pl.BlockSpec(memory_space=pltpu.SMEM)
    full = lambda shape: pl.BlockSpec(shape, lambda i: (0,) * len(shape))
    return pl.pallas_call(
        proj_kernel,
        grid=(1,),
        in_specs=[smem, hbm, hbm, hbm, hbm, hbm, full(pos.shape), full(kmix.shape), full(vmix.shape), hbm],
        out_specs=[
            full((heads, rows, LANES)),
            full((rows, 2 * heads)),
            full((key_heads, rows, LANES)),
            full((key_heads, SPAN_PAD, LANES)),
            hbm,
        ],
        scratch_shapes=[
            pltpu.VMEM((steps, rows, chunk), BF16),
            pltpu.VMEM((steps, chunk, qwidth + 2 * width), BF16),
            pltpu.VMEM((2 * heads, depth), BF16),
            pltpu.VMEM((rows, qwidth + 2 * width), F32),
            pltpu.VMEM((rows, 2 * heads), F32),
            pltpu.VMEM((inner, MORE_UNITS * wide // UNITS), BF16),
            pltpu.SemaphoreType.DMA((steps, 4)),
            pltpu.SemaphoreType.DMA((3,)),
        ],
        out_shape=[
            jax.ShapeDtypeStruct((heads, rows, LANES), BF16),
            jax.ShapeDtypeStruct((rows, 2 * heads), F32),
            jax.ShapeDtypeStruct((key_heads, rows, LANES), BF16),
            jax.ShapeDtypeStruct((key_heads, SPAN_PAD, LANES), BF16),
            jax.ShapeDtypeStruct((inner, MORE_UNITS * wide // UNITS), BF16),
        ],
        cost_estimate=pl.CostEstimate(
            flops=2 * rows * depth * (qwidth + 3 * width), transcendentals=0, bytes_accessed=2 * depth * (rows + qwidth)
        ),
        compiler_params=pltpu.CompilerParams(vmem_limit_bytes=VMEM_LIMIT),
        name="project",
    )(part, tokens, query_weight, key_weight, value_weight, gate_rows, pos, kmix, vmix, out_weight)


def copy_kernel(from_ref, to_ref):
    to_ref[...] = from_ref[...]


def first_piece(out_weight):
    inner, wide = out_weight.shape
    width = FIRST_UNITS * wide // UNITS
    spec = pl.BlockSpec((inner // 2, width), lambda i: (i, 0))
    return pl.pallas_call(
        copy_kernel,
        grid=(2,),
        in_specs=[spec],
        out_specs=spec,
        out_shape=jax.ShapeDtypeStruct((inner, width), BF16),
        compiler_params=pltpu.CompilerParams(vmem_limit_bytes=VMEM_LIMIT),
        name="first_piece",
    )(out_weight)


def select_kernel(count, own_ref, req_ref, kv_ref, sm_ref, *out_refs):
    heads = kv_ref.shape[0]
    own = own_ref[0]
    for shift in range(1, count):
        taker = jnp.minimum(own + shift, count - 1)
        out_ref = out_refs[shift - 1]
        for g in range(heads):
            for j in range(2):
                block = req_ref[taker, own * (2 * heads) + 2 * g + j]
                out_ref[g, j * SB : (j + 1) * SB, :] = kv_ref[g, pl.ds(pl.multiple_of(block * SB, SB), SB), :]
            out_ref[g, 2 * SB :, :] = sm_ref[g]


def select_blocks(count, own, requests, kv, summaries):
    heads = kv.shape[0]
    piece = (heads, 2 * SB + SPAN_PAD, LANES)
    smem = pl.BlockSpec(memory_space=pltpu.SMEM)
    full = lambda shape: pl.BlockSpec(shape, lambda i: (0,) * len(shape))
    return pl.pallas_call(
        functools.partial(select_kernel, count),
        grid=(1,),
        in_specs=[smem, smem, full(kv.shape), full(summaries.shape)],
        out_specs=[full(piece)] * (count - 1),
        out_shape=[jax.ShapeDtypeStruct(piece, BF16)] * (count - 1),
        compiler_params=pltpu.CompilerParams(vmem_limit_bytes=VMEM_LIMIT),
        name="select_blocks",
    )(own, requests, kv, summaries)


def attn_kernel(count, blocks, *refs):
    half_ref, own_ref, core_ref, table_ref, q_ref, gate_ref, kv_ref, sm_ref = refs[:8]
    recv_refs = refs[8 : 8 + count - 1]
    out_ref, poolk, poolv, sumk, sumv, score0, score1, weight0, weight1 = refs[8 + count - 1 :]
    own, base = own_ref[0], half_ref[0] * blocks
    turn = (1 - core_ref[0]) * (blocks * SB // 2)
    heads, rows = kv_ref.shape[0], kv_ref.shape[1]
    group = q_ref.shape[0] // heads
    own_blocks = rows // SB
    spans = rows // CMP
    total_blocks = poolk.shape[1] - 1
    named = N_SEL * SB
    lane, row = lane_iota(SB), row_iota(SB)
    keep = jnp.where(lane < HD, 1.0, 0.0).astype(BF16)
    other = jnp.where(lane < HD, 0.0, 1.0).astype(BF16)
    span_lane, span_row = lane_iota(SPAN_PAD), row_iota(SPAN_PAD)
    low_half = lane < HD
    diagonal = jnp.where((lane - HD == row) & (row > 0), LOW, 0.0).astype(BF16)
    contract = (((1,), (1,)), ((), ()))

    def wide(piece):
        n = piece.shape[0]
        turned = pltpu.roll(piece.astype(F32), HD, 1).astype(BF16)
        return jnp.concatenate([piece * other[:n] + keep[:n], turned * keep[:n] + other[:n]], axis=1)

    for g in range(heads):
        for j in range(own_blocks):
            piece = kv_ref[g, j * SB : (j + 1) * SB, :]
            poolk[g, j] = piece * keep
            poolv[g, j] = wide(piece)
        for k, recv in enumerate(recv_refs):
            for j in range(2):
                piece = recv[g, j * SB : (j + 1) * SB, :]
                poolk[g, own_blocks + 2 * k + j] = piece * keep
                poolv[g, own_blocks + 2 * k + j] = wide(piece)
        poolk[g, total_blocks] = jnp.where(lane == HD, LOW, 0.0).astype(BF16)
        poolv[g, total_blocks] = jnp.zeros((SB, 2 * LANES), BF16)
        for k in range(count):
            piece = sm_ref[g] if k == 0 else recv_refs[k - 1][g, 2 * SB :, :]
            sumv[g, k * SPAN_PAD : (k + 1) * SPAN_PAD] = wide(piece)
            if k:
                hidden = (span_lane == HD) & ((span_row >= spans) | (own < k))
                bias = jnp.where(hidden, LOW, 0.0).astype(BF16)
                sumk[g, (k - 1) * SPAN_PAD : k * SPAN_PAD] = piece * keep[:SPAN_PAD] + bias

    def scores(j, g, score):
        block = base + j
        last = SB // CMP * block
        hidden = (span_lane == HD) & (span_row >= last + SB // CMP)
        for i in range(SB // CMP):
            hidden = hidden | ((span_row == last + i) & (span_lane == HD + (i + 1) * CMP - 1))
        bias = jnp.where(hidden, LOW, 0.0).astype(BF16)
        pieces = [poolk[g, table_ref[block, g * N_SEL + s]] for s in range(N_SEL)]
        pieces[0] = pieces[0] + diagonal
        keys = jnp.concatenate([*pieces, sm_ref[g] * keep[:SPAN_PAD] + bias, sumk[g]], axis=0)
        q = q_ref[g * group : (g + 1) * group, pl.ds(pl.multiple_of(j * SB, SB), SB), :]
        q = q.reshape(group * SB, LANES)
        score[...] = lax.dot_general(q, keys, contract, preferred_element_type=F32)

    def weights(score, weight):
        top = jnp.max(score[:, :named], axis=1, keepdims=True)
        weight[:, :named] = jnp.exp2((score[:, :named] - top) * EXP_SCALE).astype(BF16)
        top = jnp.maximum(jnp.max(score[:, named:], axis=1, keepdims=True), FLOOR)
        weight[:, named:] = jnp.exp2((score[:, named:] - top) * EXP_SCALE).astype(BF16)

    def mixed(j, g, weight):
        block = base + j
        values = jnp.concatenate([poolv[g, table_ref[block, g * N_SEL + s]] for s in range(N_SEL)], axis=0)
        picked = jnp.dot(weight[:, :named], values, preferred_element_type=F32)
        summed = jnp.dot(weight[:, named:], sumv[g], preferred_element_type=F32)
        gate = gate_ref[pl.ds(pl.multiple_of(j * SB, SB), SB), :]
        for pair in range(group // 2):
            h = g * group + 2 * pair
            even, odd = slice(2 * pair * SB, (2 * pair + 1) * SB), slice((2 * pair + 1) * SB, (2 * pair + 2) * SB)

            def branch(out, which):
                top = jnp.where(low_half, out[even, LANES:], out[odd, :LANES])
                total = jnp.where(low_half, out[even, :LANES], out[odd, LANES:])
                scale = jnp.where(low_half, gate[:, 2 * h + which : 2 * h + which + 1],
                                  gate[:, 2 * h + 2 + which : 2 * h + 3 + which])
                return top * (scale / jnp.maximum(total, 1e-30))

            both = (branch(summed, 0) + branch(picked, 1)).astype(BF16)
            at = (g * group) // 2 + pair
            for part in range(SB // CMP):
                place = lax.rem(j * SB + part * CMP + turn, blocks * SB)
                place = pl.ds(pl.multiple_of(place, CMP), CMP)
                out_ref[place, at * LANES : (at + 1) * LANES] = both[part * CMP : (part + 1) * CMP]

    slots = [(score0, weight0), (score1, weight1)]

    def stage(first, ahead, behind):
        if first is not None:
            scores(*first, slots[first[1] % 2][0])
        if ahead is not None:
            weights(*slots[ahead[1] % 2])
        if behind is not None:
            mixed(*behind, slots[behind[1] % 2][1])

    def unit(j, g):
        return (j + g // heads, g % heads) if g >= 0 else (j - 1, g + heads)

    stage(unit(0, 0), None, None)
    stage(unit(0, 1), unit(0, 0), None)

    def body(j, carry):
        for g in range(heads):
            stage(unit(j, g), unit(j, g - 1), unit(j, g - 2))
        return carry

    lax.fori_loop(1, blocks, body, 0)
    stage(None, unit(blocks - 1, 1), unit(blocks - 1, 0))
    stage(None, None, unit(blocks - 1, 1))


def attend(count, blocks, half, own, core, table, q, gates, kv, summaries, received):
    heads, rows = kv.shape[0], kv.shape[1]
    group = q.shape[0] // heads
    total = rows // SB + 2 * (count - 1)
    keys = N_SEL * SB + count * SPAN_PAD
    full = lambda shape: pl.BlockSpec(shape, lambda i, *s: (0,) * len(shape))
    return pl.pallas_call(
        functools.partial(attn_kernel, count, blocks),
        grid_spec=pltpu.PrefetchScalarGridSpec(
            num_scalar_prefetch=4,
            grid=(1,),
            in_specs=[
                pl.BlockSpec((q.shape[0], blocks * SB, LANES), lambda i, half, *s: (0, half[0], 0)),
                pl.BlockSpec((blocks * SB, gates.shape[1]), lambda i, half, *s: (half[0], 0)),
                full(kv.shape),
                full(summaries.shape),
                *[full(r.shape) for r in received],
            ],
            out_specs=full((blocks * SB, q.shape[0] * HD)),
        scratch_shapes=[
            pltpu.VMEM((heads, total + 1, SB, LANES), BF16),
            pltpu.VMEM((heads, total + 1, SB, 2 * LANES), BF16),
            pltpu.VMEM((heads, (count - 1) * SPAN_PAD, LANES), BF16),
            pltpu.VMEM((heads, count * SPAN_PAD, 2 * LANES), BF16),
            pltpu.VMEM((group * SB, keys), F32),
            pltpu.VMEM((group * SB, keys), F32),
            pltpu.VMEM((group * SB, keys), BF16),
            pltpu.VMEM((group * SB, keys), BF16),
        ]),
        out_shape=jax.ShapeDtypeStruct((blocks * SB, q.shape[0] * HD), BF16),
        cost_estimate=pl.CostEstimate(
            flops=blocks * q.shape[0] * SB * keys * LANES * 4,
            transcendentals=blocks * q.shape[0] * SB * keys,
            bytes_accessed=4 * kv.size,
        ),
        compiler_params=pltpu.CompilerParams(vmem_limit_bytes=ATTEND_LIMIT),
        name="attend",
    )(half, own, core, table, q, gates, kv, summaries, *received)


def product_kernel(starts, near_ref, own_ref, *refs):
    send_ref, keep_ref = refs[-2:]
    rows = send_ref.shape[0]
    step = pl.program_id(0)
    total = jnp.dot(near_ref[...], own_ref[...], preferred_element_type=F32)
    if not starts:
        send_ref[...] = total[:rows].astype(BF16)
        keep_ref[...] = total[rows:].astype(BF16)
        return
    its_ref, piece_refs = refs[0], refs[1:-2]

    def one(piece_ref):
        both = total + jnp.dot(its_ref[...], piece_ref[...], preferred_element_type=F32)
        send_ref[...] = both[:rows].astype(BF16)
        keep_ref[...] = both[rows:].astype(BF16)

    for k, piece_ref in enumerate(piece_refs):
        inside = step >= starts[k]
        if k + 1 < len(piece_refs):
            inside = inside & (step < starts[k + 1])
        pl.when(inside)(functools.partial(one, piece_ref))


def out_product(near, out_weight, first, units, its=None, pieces=()):
    depth, wide = out_weight.shape
    unit = wide // UNITS * 3 if units % 3 == 0 else wide // UNITS * units
    steps = units * (wide // UNITS) // unit
    offset = first * (wide // UNITS)
    sizes = [piece.shape[1] // unit for piece in pieces]
    starts = [sum(sizes[:k]) for k in range(len(sizes))]
    rows = near.shape[0] // 2
    full = lambda shape: pl.BlockSpec(shape, lambda i: (0,) * len(shape))

    def piece_spec(k):
        return pl.BlockSpec((depth, unit), lambda i: (0, jnp.clip(i - starts[k], 0, sizes[k] - 1)))

    out = pl.BlockSpec((rows, unit), lambda i: (0, i))
    args = [near, out_weight] + ([its, *pieces] if pieces else [])
    specs = [full(near.shape), pl.BlockSpec((pl.Element(depth), pl.Element(unit)), lambda i: (0, pl.multiple_of(offset + i * unit, 2 * LANES)))]
    if pieces:
        specs += [full(its.shape), *[piece_spec(k) for k in range(len(pieces))]]
    return pl.pallas_call(
        functools.partial(product_kernel, starts),
        grid=(steps,),
        in_specs=specs,
        out_specs=[out, out],
        out_shape=[jax.ShapeDtypeStruct((rows, steps * unit), BF16)] * 2,
        cost_estimate=pl.CostEstimate(
            flops=8 * rows * depth * steps * unit, transcendentals=0, bytes_accessed=4 * depth * steps * unit
        ),
        compiler_params=pltpu.CompilerParams(vmem_limit_bytes=PROD_LIMIT),
        name="out_product",
    )(*args)


def final_kernel(first, *refs):
    out_ref, total, sem = refs[-3:]
    width = total.shape[1]
    value = refs[0][...].astype(F32) + refs[1][...].astype(F32)
    if len(refs) > 6:
        value += refs[2][...].astype(F32)
    total[...] = value.astype(BF16)
    copy = pltpu.make_async_copy(total, out_ref.at[:, first : first + width], sem)
    copy.start()
    copy.wait()


def final_sum(wide, first, *parts, into=None):
    rows, width = parts[0].shape
    full = pl.BlockSpec((rows, width), lambda i: (0, 0))
    hbm = pl.BlockSpec(memory_space=pl.ANY)
    more = [] if into is None else [into]
    return pl.pallas_call(
        functools.partial(final_kernel, first),
        grid=(1,),
        in_specs=[full] * len(parts) + [hbm] * len(more),
        out_specs=hbm,
        out_shape=jax.ShapeDtypeStruct((rows, wide), BF16),
        scratch_shapes=[pltpu.VMEM((rows, width), BF16), pltpu.SemaphoreType.DMA],
        input_output_aliases={} if into is None else {len(parts): 0},
        compiler_params=pltpu.CompilerParams(vmem_limit_bytes=PROD_LIMIT),
        name="final_sum",
    )(*parts, *more)


def local(count, parts, tokens, query_weight, key_weight, value_weight, gate_weight, summary_pos, key_mixing,
          value_mixing, out_weight, chosen):
    rows = tokens.shape[0]
    own = lax.axis_index("kv").astype(jnp.int32)
    part = lax.axis_index("tp").astype(jnp.int32)
    own_blocks = rows // SB
    heads = key_weight.shape[1] // HD
    own1, part1 = own.reshape(1), part.reshape(1)

    source = chosen // own_blocks
    place = chosen - source * own_blocks
    match = source[None] == jnp.arange(count, dtype=jnp.int32)[:, None, None, None]
    lowest = jnp.min(jnp.where(match, place[None], own_blocks - 1), axis=(1, 3))
    highest = jnp.max(jnp.where(match, place[None], 0), axis=(1, 3))
    request = jnp.stack([lowest, highest], axis=-1).reshape(1, count * heads * 2)
    everyone = jnp.where(jnp.arange(count, dtype=jnp.int32)[:, None] == own, request, 0)
    if count & (count - 1) == 0:
        bit, stage = 1, 0
        while bit < count:
            got = lax.ppermute(everyone, "kv", [(i, i ^ bit) for i in range(count)])
            everyone = everyone + got
            if stage == 0:
                chosen = lax.optimization_barrier((chosen, got))[0]
            bit, stage = 2 * bit, stage + 1
    else:
        everyone = lax.all_gather(request, "kv", axis=0, tiled=True)

    cross = [(i, i ^ 2) for i in range(parts)]
    swap = [(i, i ^ 1) for i in range(parts)]
    piece_a = lax.ppermute(first_piece(out_weight), "tp", cross)
    q, gates, kv, summaries, more = project(
        part1, tokens, query_weight, key_weight, value_weight, gate_weight.T, summary_pos, key_mixing.T,
        value_mixing.T, out_weight,
    )
    piece_b = lax.ppermute(more, "tp", cross)

    pieces = select_blocks(count, own1, everyone, kv, summaries)
    received = []
    for k in range(1, count):
        received.append(lax.ppermute(pieces[k - 1], "kv", [(i, i + k) for i in range(count - k)]))

    source = chosen // own_blocks
    place = chosen - source * own_blocks
    match = source[None] == jnp.arange(count, dtype=jnp.int32)[:, None, None, None]

    high_at = jnp.sum(jnp.where(match, highest[:, None, :, None], 0), axis=0)
    away = own_blocks + 2 * (own - source - 1) + (place == high_at).astype(jnp.int32)
    index = jnp.where(source == own, place, away)
    slots = jnp.arange(N_SEL, dtype=jnp.int32)
    earlier = slots[None, :] < slots[:, None]
    repeated = jnp.any((chosen[..., :, None] == chosen[..., None, :]) & earlier, axis=-1)
    first = jnp.logical_not(repeated)
    rank = jnp.sum((first[..., None, :] & earlier).astype(jnp.int32), axis=-1)
    at = (rank[..., None, :] == slots[:, None]) & first[..., None, :]
    fill = own_blocks + 2 * (count - 1)
    table = jnp.where(jnp.any(at, axis=-1), jnp.sum(jnp.where(at, index[..., None, :], 0), axis=-1), fill)
    table = table.reshape(own_blocks, heads * N_SEL)

    half_blocks = own_blocks // 2
    half = part // 2
    core1 = (part % 2).reshape(1)

    def halves(which):
        return attend(count, half_blocks, which.reshape(1), own1, core1, table, q, gates, kv, summaries,
                      received)

    left = FIRST_UNITS + MORE_UNITS
    right = UNITS - left
    wide = out_weight.shape[1]
    far = halves(1 - half)
    its = lax.ppermute(far, "tp", cross)
    send, keep = out_product(far, out_weight, left, right)
    got = lax.ppermute(send, "tp", swap)
    crossed = lax.ppermute((got.astype(F32) + keep.astype(F32)).astype(BF16), "tp", cross)
    near = halves(half)
    send, keep = out_product(near, out_weight, 0, left, its, [piece_a, piece_b])
    got = lax.ppermute(send, "tp", swap)
    late_send, late_keep = out_product(near, out_weight, left, right)
    late_got = lax.ppermute(late_send, "tp", swap)
    out = final_sum(wide, 0, got, keep)
    return final_sum(wide, left * wide // UNITS, late_got, late_keep, crossed, into=out)


def solution(mesh):
    placed = (
        P("kv", None),
        P(None, "tp"),
        P(None, "tp"),
        P(None, "tp"),
        P(),
        P(),
        P(),
        P(),
        P("tp", None),
        P("kv", "tp", None),
    )
    count = mesh.shape["kv"]

    def body(*args):
        return local(count, mesh.shape["tp"], *args)

    return jax.shard_map(
        body, mesh=mesh, in_specs=placed, out_specs=P(("kv", "tp"), None), check_vma=False
    )
```

time: 113 us -> 96.7 us (0.86)
  waiting for transfers between devices: 29.4 us -> 20 us
  matrix products: 7.3 us -> 0 us
  starting transfers between devices: 29.5 us -> 34.6 us
  Pallas kernels: 38.6 us -> 34.7 us
  other arithmetic: 5.43 us -> 3.92 us
    ppermute x9 -> x7, waiting for transfers between devices: 24.9 us -> 15.6 us  [the longest x1 12.3 us: local(): lax.ppermute((got.astype(F32) + keep.astype(F32)).astype(BF16), 'tp', cross)]
    dot_general x10 -> x0, matrix products: 7.3 us -> none  [product(): return jnp.dot(att, columns, preferred_element_type=F32).astype(BF16)]
    ppermute x7, starting transfers between devices: 16.7 us -> 23.2 us  [local(): lax.ppermute(pieces[k - 1], 'kv', [(i, i + k) for i in range(count - k)])]
    pallas_call x4 -> x10, Pallas kernels: 38.6 us -> 34.7 us  [the longest x2 12.2 us: attend(): pl.pallas_call(functools.partial(attn_kernel, count, blocks), grid_spec=p...]
    unnamed x22 -> x14, local copies, waits for them, and re-layouts: 0.63 us -> 2.31 us
    ppermute x9 -> x7, starting transfers between devices: 5.6 us -> 4.27 us  [the longest x1 1.55 us: local(): piece_b = lax.ppermute(more, 'tp', cross)]
    concatenate x1 -> x0, other arithmetic: 1.15 us -> none  [local(): jnp.concatenate([(base[:, c * width:(c + 1) * width] + crossed[c].astype(...]
  transfers between devices with their start and end apart: 19 -> 17, of which waited for: 8 -> 7; matrix products, arithmetic and copies ran while one was open for 6% -> 3% of each run, Pallas kernels for 21% -> 35%
where the time goes in v3:
time: 96.7 us; the launch traced here: 96.3 us
  Pallas kernels  34.7 us (36%)
  starting transfers between devices  34.6 us (36%)
  waiting for transfers between devices  20 us (21%)
  other arithmetic  3.92 us (4%)
  local copies, waits for them, and re-layouts  2.57 us (3%)
    ppermute x7, starting transfers between devices, local(): lax.ppermute(pieces[k - 1], 'kv', [(i, i + k) for i in range(count - k)])  23.2 us
    ppermute x1, waiting for transfers between devices, local(): lax.ppermute((got.astype(F32) + keep.astype(F32)).astype(BF16), 'tp', cross)  12.3 us
    pallas_call x2, Pallas kernels, attend(): pl.pallas_call(functools.partial(attn_kernel, count, blocks), grid_spec=p...  12.2 us
    pallas_call x1, Pallas kernels, project(): pl.pallas_call(proj_kernel, grid=(1,), in_specs=[smem, hbm, hbm, hbm, hbm...  12 us
    ppermute x3, starting transfers between devices, local(): got = lax.ppermute(everyone, 'kv', [(i, i ^ bit) for i in range(count)])  7.17 us
    pallas_call x3, Pallas kernels, out_product(): pl.pallas_call(functools.partial(product_kernel, starts), grid=(steps,),...  4.56 us
    ppermute x1, waiting for transfers between devices, local(): its = lax.ppermute(far, 'tp', cross)  2.64 us
    ppermute x3, waiting for transfers between devices, local(): got = lax.ppermute(everyone, 'kv', [(i, i ^ bit) for i in range(count)])  2.32 us
  transfers between devices with their start and end apart: 17, of which 7 were waited for; matrix products, arithmetic and copies ran while one was open for 3% of the time, Pallas kernels for 35%

profile of v3, /device:TPU:0, one launch (start us, length us, event | category | flops | bytes accessed | tf_op | source)
XLA Modules:
  0.0 96.3 jit_solution(7655303863124458327)
XLA Ops:
  1.2 3.0 %collective-permute-start = (s32[8,32]{1,0:T(8,128)S(1)}, s32[8,32]{1,0:T(8,128)S(1)}, u32[]{:S(2)}, u32[]{:S(2)}) collective-permute-start(s32[8,32]{1,0:T(8,128)S(1)} %broadcast_select_fusion.1), channel_id=1, source_target_pairs={{0,4},{4,0},{8,12},{12,8},{16,20},{20,16},{24,28},{28,24},{1,5},{5... | collective-permute-start | bytes 3080 | tf_op jit(solution)/shard_map/ppermute | solution.py:483
  4.2 12.0 %project.1 = (bf16[8,640,128]{2,1,0:T(8,128)(2,1)}, f32[640,16]{1,0:T(8,128)}, bf16[2,640,128]{2,1,0:T(8,128)(2,1)}, bf16[2,32,128]{2,1,0:T(8,128)(2,1)}, bf16[512,1536]{1,0:T(8,128)(2,1)}) custom-call(s32[1]{0:T(128)} %bitcast.5.part_ref, bf16[640,4096]{1,0:T(8,128)(2,1)} %tok_ref.1, bf16[4096,512]{1,0:T(8,128)(2,1)} %wq_ref.1, bf16[4096,128]{1,0:T(8,128)(2,1)} %wk_ref.1, ...), custom_call_target="tpu_custom_call" | custom-call | flops 4697620480 | bytes 9437184 | tf_op jit(solution)/shard_map/project/pallas_call | solution.py:140
  16.2 1.6 %collective-permute-start.15 = (bf16[512,1536]{1,0:T(8,128)(2,1)}, bf16[512,1536]{1,0:T(8,128)(2,1)S(1)}, u32[]{:S(2)}, u32[]{:S(2)}) collective-permute-start(bf16[512,1536]{1,0:T(8,128)(2,1)} %get-tuple-element.40), channel_id=1, source_target_pairs={{0,2},{1,3},{2,0},{3,1},{4,6},{5,7},{6,4},{7,5},{8,10},{9,11},{10,... | collective-permute-start | bytes 4718600 | tf_op jit(solution)/shard_map/ppermute | solution.py:498
  17.8 1.9 %first_piece.1 = bf16[512,768]{1,0:T(8,128)(2,1)} custom-call(bf16[512,4096]{1,0:T(8,128)(2,1)} %own_ref.5), custom_call_target="tpu_custom_call" | custom-call | tf_op jit(solution)/shard_map/first_piece/pallas_call | solution.py:184
  19.8 1.6 %collective-permute-start.1 = (s32[8,32]{1,0:T(8,128)S(1)}, s32[8,32]{1,0:T(8,128)S(1)}, u32[]{:S(2)}, u32[]{:S(2)}) collective-permute-start(s32[8,32]{1,0:T(8,128)S(1)} %fusion.3), channel_id=1, source_target_pairs={{0,8},{4,12},{8,0},{12,4},{16,24},{20,28},{24,16},{28,20},{1,9},{5... | collective-permute-start | bytes 3080 | tf_op jit(solution)/shard_map/ppermute | solution.py:483
  23.5 2.6 %collective-permute-start.2 = (s32[8,32]{1,0:T(8,128)S(1)}, s32[8,32]{1,0:T(8,128)S(1)}, u32[]{:S(2)}, u32[]{:S(2)}) collective-permute-start(s32[8,32]{1,0:T(8,128)S(1)} %fusion.4), channel_id=1, source_target_pairs={{0,16},{4,20},{8,24},{12,28},{16,0},{20,4},{24,8},{28,12},{1,17},{... | collective-permute-start | bytes 3080 | tf_op jit(solution)/shard_map/ppermute | solution.py:483
  26.5 1.5 %collective-permute-done.2 = s32[8,32]{1,0:T(8,128)S(1)} collective-permute-done((s32[8,32]{1,0:T(8,128)S(1)}, s32[8,32]{1,0:T(8,128)S(1)}, u32[]{:S(2)}, u32[]{:S(2)}) %collective-permute-start.2) | collective-permute-done | bytes 1056 | tf_op jit(solution)/shard_map/ppermute | solution.py:483
  28.6 1.9 %select_blocks.1 = (bf16[2,160,128]{2,1,0:T(8,128)(2,1)}, bf16[2,160,128]{2,1,0:T(8,128)(2,1)}, bf16[2,160,128]{2,1,0:T(8,128)(2,1)}, bf16[2,160,128]{2,1,0:T(8,...) custom-call(s32[1]{0:T(128)} %bitcast.1.own_ref.refs_1_, ...), custom_call_target="tpu_custom_call" | custom-call | tf_op jit(solution)/shard_map/select_blocks/pallas_call | solution.py:213
  30.5 2.4 %collective-permute-start.3 = (bf16[2,160,128]{2,1,0:T(8,128)(2,1)}, bf16[2,160,128]{2,1,0:T(8,128)(2,1)S(1)}, u32[]{:S(2)}, u32[]{:S(2)}) collective-permute-start(bf16[2,160,128]{2,1,0:T(8,128)(2,1)} %get-tuple-element.29), channel_id=1, source_target_pairs={{0,4},{4,8},{8,12},{12,16},{16,20},{20,24},{24,28},{1,5},{5,9},{9,... | collective-permute-start | bytes 245768 | tf_op jit(solution)/shard_map/ppermute | solution.py:503
  32.9 3.5 %collective-permute-start.4 = (bf16[2,160,128]{2,1,0:T(8,128)(2,1)}, bf16[2,160,128]{2,1,0:T(8,128)(2,1)S(1)}, u32[]{:S(2)}, u32[]{:S(2)}) collective-permute-start(bf16[2,160,128]{2,1,0:T(8,128)(2,1)} %get-tuple-element.30), channel_id=1, source_target_pairs={{0,8},{4,12},{8,16},{12,20},{16,24},{20,28},{1,9},{5,13},{9,17},{1... | collective-permute-start | bytes 245768 | tf_op jit(solution)/shard_map/ppermute | solution.py:503
  36.4 5.5 %collective-permute-start.5 = (bf16[2,160,128]{2,1,0:T(8,128)(2,1)}, bf16[2,160,128]{2,1,0:T(8,128)(2,1)S(1)}, u32[]{:S(2)}, u32[]{:S(2)}) collective-permute-start(bf16[2,160,128]{2,1,0:T(8,128)(2,1)} %get-tuple-element.31), channel_id=1, source_target_pairs={{0,12},{4,16},{8,20},{12,24},{16,28},{1,13},{5,17},{9,21},{13,25},... | collective-permute-start | bytes 245768 | tf_op jit(solution)/shard_map/ppermute | solution.py:503
  41.8 1.3 %collective-permute-start.6 = (bf16[2,160,128]{2,1,0:T(8,128)(2,1)}, bf16[2,160,128]{2,1,0:T(8,128)(2,1)S(1)}, u32[]{:S(2)}, u32[]{:S(2)}) collective-permute-start(bf16[2,160,128]{2,1,0:T(8,128)(2,1)} %get-tuple-element.32), channel_id=1, source_target_pairs={{0,16},{4,20},{8,24},{12,28},{1,17},{5,21},{9,25},{13,29},{2,18},{... | collective-permute-start | bytes 245768 | tf_op jit(solution)/shard_map/ppermute | solution.py:503
  44.2 3.4 %collective-permute-start.7 = (bf16[2,160,128]{2,1,0:T(8,128)(2,1)}, bf16[2,160,128]{2,1,0:T(8,128)(2,1)S(1)}, u32[]{:S(2)}, u32[]{:S(2)}) collective-permute-start(bf16[2,160,128]{2,1,0:T(8,128)(2,1)} %get-tuple-element.33), channel_id=1, source_target_pairs={{0,20},{4,24},{8,28},{1,21},{5,25},{9,29},{2,22},{6,26},{10,30},{3... | collective-permute-start | bytes 245768 | tf_op jit(solution)/shard_map/ppermute | solution.py:503
  47.6 5.3 %collective-permute-start.8 = (bf16[2,160,128]{2,1,0:T(8,128)(2,1)}, bf16[2,160,128]{2,1,0:T(8,128)(2,1)S(1)}, u32[]{:S(2)}, u32[]{:S(2)}) collective-permute-start(bf16[2,160,128]{2,1,0:T(8,128)(2,1)} %get-tuple-element.34), channel_id=1, source_target_pairs={{0,24},{4,28},{1,25},{5,29},{2,26},{6,30},{3,27},{7,31}} | collective-permute-start | bytes 245768 | tf_op jit(solution)/shard_map/ppermute | solution.py:503
  52.9 1.9 %collective-permute-start.9 = (bf16[2,160,128]{2,1,0:T(8,128)(2,1)}, bf16[2,160,128]{2,1,0:T(8,128)(2,1)S(1)}, u32[]{:S(2)}, u32[]{:S(2)}) collective-permute-start(bf16[2,160,128]{2,1,0:T(8,128)(2,1)} %get-tuple-element.35), channel_id=1, source_target_pairs={{0,28},{1,29},{2,30},{3,31}} | collective-permute-start | bytes 245768 | tf_op jit(solution)/shard_map/ppermute | solution.py:503
  55.2 1.8 %collective-permute-done.9.refs_14_ = bf16[2,160,128]{2,1,0:T(8,128)(2,1)S(1)} collective-permute-done((bf16[2,160,128]{2,1,0:T(8,128)(2,1)}, bf16[2,160,128]{2,1,0:T(8,128)(2,1)S(1)}, u32[]{:S(2)}, u32[]{:S(2)}) %collective-permute-start.9) | collective-permute-done | bytes 81952 | tf_op jit(solution)/shard_map/ppermute | solution.py:503
  57.0 1.3 %copy-done.3 = bf16[8,640,128]{2,1,0:T(8,128)(2,1)S(1)} copy-done((bf16[8,640,128]{2,1,0:T(8,128)(2,1)S(1)}, bf16[8,640,128]{2,1,0:T(8,128)(2,1)}, u32[]{:S(2)}) %copy-start.3) | copy-done | bytes 1310744
  59.3 6.1 %attend.3.near_ref = bf16[320,512]{1,0:T(8,128)(2,1)S(1)} custom-call(s32[1]{0:T(128)} %bitcast.9.refs_0_, s32[1]{0:T(128)} %bitcast.1.own_ref.refs_1_, s32[1]{0:T(128)} %bitcast.2.refs_2_, s32[10,32]{1,0:T(8,128)S(1)} %select_n.60.refs_3_, bf16[8,640,128]{2,1,0:T(8,128)(2,1)S(1)} %copy-done.3, f32[640,16]{1,0:T(8,128)S(1)} %copy-done.4, ...), custom_call_target="tpu_custom_call" | custom-call | flops 1677721600 | bytes 655360 | tf_op jit(solution)/shard_map/attend/pallas_call | solution.py:345
  66.4 6.1 %attend.2.near_ref = bf16[320,512]{1,0:T(8,128)(2,1)S(1)} custom-call(s32[1]{0:T(128)} %bitcast.refs_0_, s32[1]{0:T(128)} %bitcast.1.own_ref.refs_1_, s32[1]{0:T(128)} %bitcast.2.refs_2_, s32[10,32]{1,0:T(8,128)S(1)} %select_n.60.refs_3_, bf16[8,640,128]{2,1,0:T(8,128)(2,1)S(1)} %copy-done.3, f32[640,16]{1,0:T(8,128)S(1)} %copy-done.5, ...), custom_call_target="tpu_custom_call" | custom-call | flops 1677721600 | bytes 655360 | tf_op jit(solution)/shard_map/attend/pallas_call | solution.py:345
  73.7 2.6 %collective-permute-done.13.refs_0_ = bf16[320,512]{1,0:T(8,128)(2,1)S(1)} collective-permute-done((bf16[320,512]{1,0:T(8,128)(2,1)S(1)}, bf16[320,512]{1,0:T(8,128)(2,1)S(1)}, u32[]{:S(2)}, u32[]{:S(2)}) %collective-permute-start.13) | collective-permute-done | bytes 327712 | tf_op jit(solution)/shard_map/ppermute | solution.py:534
  76.4 3.0 %out_product.5 = (bf16[160,2304]{1,0:T(8,128)(2,1)S(1)}, bf16[160,2304]{1,0:T(8,128)(2,1)S(1)}) custom-call(bf16[320,512]{1,0:T(8,128)(2,1)S(1)} %attend.2.near_ref, bf16[512,4096]{1,0:T(8,128)(2,1)S(1)} %copy-done, bf16[320,512]{1,0:T(8,128)(2,1)S(1)} %collective-permute-done.13.refs_0_, bf16[512,768]{1,0:T(8,128)(2,1)S(1)} %collective-permute-done.14.refs_1_, ...), custom_call_target="tpu_custom_call" | custom-call | flops 1509949440 | bytes 4718592 | tf_op jit(solution)/shard_map/out_product/pallas_call | solution.py:420
  79.6 1.4 %collective-permute-start.12 = (bf16[160,1792]{1,0:T(8,128)(2,1)S(1)}, bf16[160,1792]{1,0:T(8,128)(2,1)S(1)}, u32[]{:S(2)}, u32[]{:S(2)}) collective-permute-start(bf16[160,1792]{1,0:T(8,128)(2,1)S(1)} %add_convert_fusion), channel_id=1, source_target_pairs={{0,2},{1,3},{2,0},{3,1},{4,6},{5,7},{6,4},{7,5},{8,10},{9,11},{10,... | collective-permute-start | bytes 1720328 | tf_op jit(solution)/shard_map/ppermute | solution.py:537
  81.7 1.0 %final_sum.2.refs_3_ = bf16[160,4096]{1,0:T(8,128)(2,1)} custom-call(bf16[160,2304]{1,0:T(8,128)(2,1)S(1)} %collective-permute-done.16.refs_0_, bf16[160,2304]{1,0:T(8,128)(2,1)S(1)} %get-tuple-element.42.refs_1_), custom_call_target="tpu_custom_call" | custom-call | tf_op jit(solution)/shard_map/final_sum/pallas_call | solution.py:451
  82.8 12.3 %collective-permute-done.12.refs_2_ = bf16[160,1792]{1,0:T(8,128)(2,1)S(1)} collective-permute-done((bf16[160,1792]{1,0:T(8,128)(2,1)S(1)}, bf16[160,1792]{1,0:T(8,128)(2,1)S(1)}, u32[]{:S(2)}, u32[]{:S(2)}) %collective-permute-start.12) | collective-permute-done | bytes 573472 | tf_op jit(solution)/shard_map/ppermute | solution.py:537
  (56 shorter events, 10.9 us)
Async XLA Ops:
  1.2 18.5 %collective-permute-start = (s32[8,32]{1,0:T(8,128)S(1)}, s32[8,32]{1,0:T(8,128)S(1)}, u32[]{:S(2)}, u32[]{:S(2)}) collective-permute-start(s32[8,32]{1,0:T(8,128)S(1)} %broadcast_select_fusion.1), channel_id=1, source_target_pairs={{0,4},{4,0},{8,12},{12,8},{16,20},{20,16},{24,28},{28,24},{1,5},{5... | collective-permute-start | bytes 3080 | tf_op jit(solution)/shard_map/ppermute | solution.py:483
  16.2 60.2 %collective-permute-start.15 = (bf16[512,1536]{1,0:T(8,128)(2,1)}, bf16[512,1536]{1,0:T(8,128)(2,1)S(1)}, u32[]{:S(2)}, u32[]{:S(2)}) collective-permute-start(bf16[512,1536]{1,0:T(8,128)(2,1)} %get-tuple-element.40), channel_id=1, source_target_pairs={{0,2},{1,3},{2,0},{3,1},{4,6},{5,7},{6,4},{7,5},{8,10},{9,11},{10,... | collective-permute-start | bytes 4718600 | tf_op jit(solution)/shard_map/ppermute | solution.py:498
  17.8 3.6 %copy-start.6 = (s32[10,2,16]{2,1,0:T(2,128)S(1)}, s32[10,2,16]{2,1,0:T(2,128)}, u32[]{:S(2)}) copy-start(s32[10,2,16]{2,1,0:T(2,128)} %param.19) | copy-start | bytes 3844
  17.8 39.2 %copy-start.1 = (bf16[2,640,128]{2,1,0:T(8,128)(2,1)S(1)}, bf16[2,640,128]{2,1,0:T(8,128)(2,1)}, u32[]{:S(2)}) copy-start(bf16[2,640,128]{2,1,0:T(8,128)(2,1)} %get-tuple-element.27.kv_ref.refs_6_) | copy-start | bytes 983044
  17.8 39.2 %copy-start.2 = (bf16[2,32,128]{2,1,0:T(8,128)(2,1)S(1)}, bf16[2,32,128]{2,1,0:T(8,128)(2,1)}, u32[]{:S(2)}) copy-start(bf16[2,32,128]{2,1,0:T(8,128)(2,1)} %get-tuple-element.28.sm_ref.refs_7_) | copy-start | bytes 49156
  19.8 3.6 %collective-permute-start.1 = (s32[8,32]{1,0:T(8,128)S(1)}, s32[8,32]{1,0:T(8,128)S(1)}, u32[]{:S(2)}, u32[]{:S(2)}) collective-permute-start(s32[8,32]{1,0:T(8,128)S(1)} %fusion.3), channel_id=1, source_target_pairs={{0,8},{4,12},{8,0},{12,4},{16,24},{20,28},{24,16},{28,20},{1,9},{5... | collective-permute-start | bytes 3080 | tf_op jit(solution)/shard_map/ppermute | solution.py:483
  23.5 4.5 %collective-permute-start.2 = (s32[8,32]{1,0:T(8,128)S(1)}, s32[8,32]{1,0:T(8,128)S(1)}, u32[]{:S(2)}, u32[]{:S(2)}) collective-permute-start(s32[8,32]{1,0:T(8,128)S(1)} %fusion.4), channel_id=1, source_target_pairs={{0,16},{4,20},{8,24},{12,28},{16,0},{20,4},{24,8},{28,12},{1,17},{... | collective-permute-start | bytes 3080 | tf_op jit(solution)/shard_map/ppermute | solution.py:483
  30.5 13.1 %collective-permute-start.3 = (bf16[2,160,128]{2,1,0:T(8,128)(2,1)}, bf16[2,160,128]{2,1,0:T(8,128)(2,1)S(1)}, u32[]{:S(2)}, u32[]{:S(2)}) collective-permute-start(bf16[2,160,128]{2,1,0:T(8,128)(2,1)} %get-tuple-element.29), channel_id=1, source_target_pairs={{0,4},{4,8},{8,12},{12,16},{16,20},{20,24},{24,28},{1,5},{5,9},{9,... | collective-permute-start | bytes 245768 | tf_op jit(solution)/shard_map/ppermute | solution.py:503
  32.9 11.3 %collective-permute-start.4 = (bf16[2,160,128]{2,1,0:T(8,128)(2,1)}, bf16[2,160,128]{2,1,0:T(8,128)(2,1)S(1)}, u32[]{:S(2)}, u32[]{:S(2)}) collective-permute-start(bf16[2,160,128]{2,1,0:T(8,128)(2,1)} %get-tuple-element.30), channel_id=1, source_target_pairs={{0,8},{4,12},{8,16},{12,20},{16,24},{20,28},{1,9},{5,13},{9,17},{1... | collective-permute-start | bytes 245768 | tf_op jit(solution)/shard_map/ppermute | solution.py:503
  36.4 11.2 %collective-permute-start.5 = (bf16[2,160,128]{2,1,0:T(8,128)(2,1)}, bf16[2,160,128]{2,1,0:T(8,128)(2,1)S(1)}, u32[]{:S(2)}, u32[]{:S(2)}) collective-permute-start(bf16[2,160,128]{2,1,0:T(8,128)(2,1)} %get-tuple-element.31), channel_id=1, source_target_pairs={{0,12},{4,16},{8,20},{12,24},{16,28},{1,13},{5,17},{9,21},{13,25},... | collective-permute-start | bytes 245768 | tf_op jit(solution)/shard_map/ppermute | solution.py:503
  41.8 11.0 %collective-permute-start.6 = (bf16[2,160,128]{2,1,0:T(8,128)(2,1)}, bf16[2,160,128]{2,1,0:T(8,128)(2,1)S(1)}, u32[]{:S(2)}, u32[]{:S(2)}) collective-permute-start(bf16[2,160,128]{2,1,0:T(8,128)(2,1)} %get-tuple-element.32), channel_id=1, source_target_pairs={{0,16},{4,20},{8,24},{12,28},{1,17},{5,21},{9,25},{13,29},{2,18},{... | collective-permute-start | bytes 245768 | tf_op jit(solution)/shard_map/ppermute | solution.py:503
  43.6 32.8 %collective-permute-start.14 = (bf16[512,768]{1,0:T(8,128)(2,1)}, bf16[512,768]{1,0:T(8,128)(2,1)S(1)}, u32[]{:S(2)}, u32[]{:S(2)}) collective-permute-start(bf16[512,768]{1,0:T(8,128)(2,1)} %first_piece.1), channel_id=1, source_target_pairs={{0,2},{1,3},{2,0},{3,1},{4,6},{5,7},{6,4},{7,5},{8,10},{9,11},{10,... | collective-permute-start | bytes 2359304 | tf_op jit(solution)/shard_map/ppermute | solution.py:493
  44.2 10.7 %collective-permute-start.7 = (bf16[2,160,128]{2,1,0:T(8,128)(2,1)}, bf16[2,160,128]{2,1,0:T(8,128)(2,1)S(1)}, u32[]{:S(2)}, u32[]{:S(2)}) collective-permute-start(bf16[2,160,128]{2,1,0:T(8,128)(2,1)} %get-tuple-element.33), channel_id=1, source_target_pairs={{0,20},{4,24},{8,28},{1,21},{5,25},{9,29},{2,22},{6,26},{10,30},{3... | collective-permute-start | bytes 245768 | tf_op jit(solution)/shard_map/ppermute | solution.py:503
  47.6 7.6 %collective-permute-start.8 = (bf16[2,160,128]{2,1,0:T(8,128)(2,1)}, bf16[2,160,128]{2,1,0:T(8,128)(2,1)S(1)}, u32[]{:S(2)}, u32[]{:S(2)}) collective-permute-start(bf16[2,160,128]{2,1,0:T(8,128)(2,1)} %get-tuple-element.34), channel_id=1, source_target_pairs={{0,24},{4,28},{1,25},{5,29},{2,26},{6,30},{3,27},{7,31}} | collective-permute-start | bytes 245768 | tf_op jit(solution)/shard_map/ppermute | solution.py:503
  52.9 4.1 %collective-permute-start.9 = (bf16[2,160,128]{2,1,0:T(8,128)(2,1)}, bf16[2,160,128]{2,1,0:T(8,128)(2,1)S(1)}, u32[]{:S(2)}, u32[]{:S(2)}) collective-permute-start(bf16[2,160,128]{2,1,0:T(8,128)(2,1)} %get-tuple-element.35), channel_id=1, source_target_pairs={{0,28},{1,29},{2,30},{3,31}} | collective-permute-start | bytes 245768 | tf_op jit(solution)/shard_map/ppermute | solution.py:503
  57.0 1.3 %copy-start.3 = (bf16[8,640,128]{2,1,0:T(8,128)(2,1)S(1)}, bf16[8,640,128]{2,1,0:T(8,128)(2,1)}, u32[]{:S(2)}) copy-start(bf16[8,640,128]{2,1,0:T(8,128)(2,1)} %get-tuple-element.25.refs_4_) | copy-start | bytes 3932164
  58.3 1.0 %copy-start.4 = (f32[640,16]{1,0:T(8,128)S(1)}, f32[640,16]{1,0:T(8,128)}, u32[]{:S(2)}) copy-start(f32[640,16]{1,0:T(8,128)} %get-tuple-element.26.refs_5_) | copy-start | bytes 122884
  59.3 6.1 %copy-start = (bf16[512,4096]{1,0:T(8,128)(2,1)S(1)}, bf16[512,4096]{1,0:T(8,128)(2,1)}, u32[]{:S(2)}) copy-start(bf16[512,4096]{1,0:T(8,128)(2,1)} %own_ref.5) | copy-start | bytes 12582916
  65.4 1.0 %copy-start.5 = (f32[640,16]{1,0:T(8,128)S(1)}, f32[640,16]{1,0:T(8,128)}, u32[]{:S(2)}) copy-start(f32[640,16]{1,0:T(8,128)} %get-tuple-element.26.refs_5_) | copy-start | bytes 122884
  66.2 13.3 %collective-permute-start.11 = (bf16[160,1792]{1,0:T(8,128)(2,1)S(1)}, bf16[160,1792]{1,0:T(8,128)(2,1)S(1)}, u32[]{:S(2)}, u32[]{:S(2)}) collective-permute-start(bf16[160,1792]{1,0:T(8,128)(2,1)S(1)} %get-tuple-element.38), channel_id=1, source_target_pairs={{0,1},{1,0},{2,3},{3,2},{4,5},{5,4},{6,7},{7,6},{8,9},{9,8},{10,11... | collective-permute-start | bytes 1720328 | tf_op jit(solution)/shard_map/ppermute | solution.py:536
  66.3 10.1 %collective-permute-start.13 = (bf16[320,512]{1,0:T(8,128)(2,1)S(1)}, bf16[320,512]{1,0:T(8,128)(2,1)S(1)}, u32[]{:S(2)}, u32[]{:S(2)}) collective-permute-start(bf16[320,512]{1,0:T(8,128)(2,1)S(1)} %attend.3.near_ref), channel_id=1, source_target_pairs={{0,2},{1,3},{2,0},{3,1},{4,6},{5,7},{6,4},{7,5},{8,10},{9,11},{10,... | collective-permute-start | bytes 983048 | tf_op jit(solution)/shard_map/ppermute | solution.py:534
  73.3 9.4 %collective-permute-start.10 = (bf16[160,1792]{1,0:T(8,128)(2,1)S(1)}, bf16[160,1792]{1,0:T(8,128)(2,1)S(1)}, u32[]{:S(2)}, u32[]{:S(2)}) collective-permute-start(bf16[160,1792]{1,0:T(8,128)(2,1)S(1)} %get-tuple-element.36), channel_id=1, source_target_pairs={{0,1},{1,0},{2,3},{3,2},{4,5},{5,4},{6,7},{7,6},{8,9},{9,8},{10,11... | collective-permute-start | bytes 1720328 | tf_op jit(solution)/shard_map/ppermute | solution.py:542
  79.4 2.3 %collective-permute-start.16 = (bf16[160,2304]{1,0:T(8,128)(2,1)S(1)}, bf16[160,2304]{1,0:T(8,128)(2,1)S(1)}, u32[]{:S(2)}, u32[]{:S(2)}) collective-permute-start(bf16[160,2304]{1,0:T(8,128)(2,1)S(1)} %get-tuple-element.41), channel_id=1, source_target_pairs={{0,1},{1,0},{2,3},{3,2},{4,5},{5,4},{6,7},{7,6},{8,9},{9,8},{10,11... | collective-permute-start | bytes 2211848 | tf_op jit(solution)/shard_map/ppermute | solution.py:540
  79.6 15.4 %collective-permute-start.12 = (bf16[160,1792]{1,0:T(8,128)(2,1)S(1)}, bf16[160,1792]{1,0:T(8,128)(2,1)S(1)}, u32[]{:S(2)}, u32[]{:S(2)}) collective-permute-start(bf16[160,1792]{1,0:T(8,128)(2,1)S(1)} %add_convert_fusion), channel_id=1, source_target_pairs={{0,2},{1,3},{2,0},{3,1},{4,6},{5,7},{6,4},{7,5},{8,10},{9,11},{10,... | collective-permute-start | bytes 1720328 | tf_op jit(solution)/shard_map/ppermute | solution.py:537

commit v4 on v3

--- a/solution.py
+++ b/solution.py
@@ -15,12 +15,15 @@
 LANES = 2 * HD
 SPAN_PAD = 32
 UNITS = 16
-FIRST_UNITS, MORE_UNITS = 3, 6
+BLOCK = 512
+FIRST_UNITS, MORE_UNITS = 2, 7
 LOW = -1e30
 FLOOR = -1e29
 EXP_SCALE = HD ** (-0.5) * 1.4426950408889634
 VMEM_LIMIT = 60 * 1024 * 1024
+SELECT_LIMIT = 8 * 1024 * 1024
 ATTEND_LIMIT = 24 * 1024 * 1024
+PROJ_LIMIT = 57 * 1024 * 1024
 PROD_LIMIT = 16 * 1024 * 1024
 
 
@@ -36,69 +39,50 @@
     return lax.broadcasted_iota(jnp.int32, (rows, LANES), 0)
 
 
-def proj_kernel(part_ref, tok_ref, wq_ref, wk_ref, wv_ref, gw_ref, pos_ref, km_ref, vm_ref, wo_ref, q_ref,
-                gate_ref, kv_ref, sm_ref, more_ref, tok, weight, gate_rows, acc_ref, gacc_ref, held, sems, wide_sems):
-    heads, rows = q_ref.shape[0], q_ref.shape[1]
-    key_heads = kv_ref.shape[0]
-    gates = gate_ref.shape[1]
+def staged(copies, ahead, step):
+    for group in copies[:ahead]:
+        for copy in group:
+            copy.start()
+    for i, group in enumerate(copies):
+        for copy in group:
+            copy.wait()
+        if i + ahead < len(copies):
+            for copy in copies[i + ahead]:
+                copy.start()
+        step(i)
+
+
+def kv_kernel(part_ref, tok_ref, wk_ref, wv_ref, pos_ref, km_ref, vm_ref, wo_ref, kv_ref, sm_ref, more_ref, tok, weight,
+              acc_ref, held, sems, wide_sems):
+    key_heads, rows = kv_ref.shape[0], kv_ref.shape[1]
     steps, chunk = weight.shape[0], weight.shape[1]
-    at_k, at_v = heads * HD, heads * HD + key_heads * HD
+    at_v = key_heads * HD
     copies = []
     for i in range(steps):
         depth = slice(i * chunk, (i + 1) * chunk)
         copies.append(
             [
                 pltpu.make_async_copy(tok_ref.at[:, depth], tok.at[i], sems.at[i, 0]),
-                pltpu.make_async_copy(wq_ref.at[depth, :], weight.at[i, :, :at_k], sems.at[i, 1]),
-                pltpu.make_async_copy(wk_ref.at[depth, :], weight.at[i, :, at_k:at_v], sems.at[i, 2]),
-                pltpu.make_async_copy(wv_ref.at[depth, :], weight.at[i, :, at_v:], sems.at[i, 3]),
+                pltpu.make_async_copy(wk_ref.at[depth, :], weight.at[i, :, :at_v], sems.at[i, 1]),
+                pltpu.make_async_copy(wv_ref.at[depth, :], weight.at[i, :, at_v:], sems.at[i, 2]),
             ]
         )
-    start = pl.multiple_of(part_ref[0] * gates, gates)
-    gate_copy = pltpu.make_async_copy(gw_ref.at[pl.ds(start, gates), :], gate_rows, wide_sems.at[0])
-    ahead = 2
-    for i in range(ahead):
-        for copy in copies[i]:
-            copy.start()
-        if i == 0:
-            gate_copy.start()
+
     unit = wo_ref.shape[1] // UNITS
     more = slice(FIRST_UNITS * unit, (FIRST_UNITS + MORE_UNITS) * unit)
-    fetch = pltpu.make_async_copy(wo_ref.at[:, more], held, wide_sems.at[1])
-    put = pltpu.make_async_copy(held, more_ref, wide_sems.at[2])
-    for i, group in enumerate(copies):
-        for copy in group:
-            copy.wait()
-        if i == 0:
-            gate_copy.wait()
-        if i + ahead < steps:
-            for copy in copies[i + ahead]:
-                copy.start()
-        elif i + ahead == steps:
+    fetch = pltpu.make_async_copy(wo_ref.at[:, more], held, wide_sems.at[0])
+    put = pltpu.make_async_copy(held, more_ref, wide_sems.at[1])
+
+    def step(i):
+        if i == steps - 2:
             fetch.start()
         piece = jnp.dot(tok[i], weight[i], preferred_element_type=F32)
-        gpiece = lax.dot_general(
-            tok[i], gate_rows[:, i * chunk : (i + 1) * chunk], (((1,), (1,)), ((), ())), preferred_element_type=F32
-        )
-        if i == 0:
-            acc_ref[...] = piece
-            gacc_ref[...] = gpiece
-        else:
-            acc_ref[...] += piece
-            gacc_ref[...] += gpiece
+        acc_ref[...] = piece if i == 0 else acc_ref[...] + piece
+
+    staged(copies, 2, step)
     fetch.wait()
     put.start()
-
-    lane, inner = lane_iota(rows), lax.rem(row_iota(rows), SB)
-    low_half = lane < HD
-    ext = jnp.where((lane == HD) | (lane - HD > inner), 1.0, 0.0)
-    for h in range(heads):
-        slab = acc_ref[:, (h // 2) * LANES : (h // 2 + 1) * LANES]
-        if h % 2:
-            slab = pltpu.roll(slab, HD, 1)
-        q_ref[h] = jnp.where(low_half, slab, ext).astype(BF16)
-    gate_ref[...] = jax.nn.sigmoid(gacc_ref[...])
-
+    low_half = lane_iota(rows) < HD
     spans = rows // CMP
     pos = pos_ref[...].astype(F32)
     pos = jnp.concatenate([pos, pos], axis=1)
@@ -110,7 +94,7 @@
         return jnp.sum(jnp.where(eye, kept, 0.0), axis=1, keepdims=True)
 
     for g in range(key_heads):
-        k = acc_ref[:, at_k + (g // 2) * LANES : at_k + (g // 2 + 1) * LANES]
+        k = acc_ref[:, (g // 2) * LANES : (g // 2 + 1) * LANES]
         v = acc_ref[:, at_v + (g // 2) * LANES : at_v + (g // 2 + 1) * LANES]
         if g % 2 == 0:
             both = jnp.where(low_half, k, pltpu.roll(v, HD, 1))
@@ -127,50 +111,108 @@
     put.wait()
 
 
-def project(part, tokens, query_weight, key_weight, value_weight, gate_rows, pos, kmix, vmix, out_weight):
+def project_kv(part, tokens, key_weight, value_weight, pos, kmix, vmix, out_weight):
     rows, depth = tokens.shape
-    qwidth, width = query_weight.shape[1], key_weight.shape[1]
-    heads, key_heads = qwidth // HD, width // HD
+    inner, wide = out_weight.shape
+    width = key_weight.shape[1]
+    key_heads = width // HD
     steps = 4
     chunk = depth // steps
-    inner, wide = out_weight.shape
     hbm = pl.BlockSpec(memory_space=pl.ANY)
     smem = pl.BlockSpec(memory_space=pltpu.SMEM)
     full = lambda shape: pl.BlockSpec(shape, lambda i: (0,) * len(shape))
     return pl.pallas_call(
-        proj_kernel,
+        kv_kernel,
         grid=(1,),
-        in_specs=[smem, hbm, hbm, hbm, hbm, hbm, full(pos.shape), full(kmix.shape), full(vmix.shape), hbm],
-        out_specs=[
-            full((heads, rows, LANES)),
-            full((rows, 2 * heads)),
-            full((key_heads, rows, LANES)),
-            full((key_heads, SPAN_PAD, LANES)),
-            hbm,
-        ],
+        in_specs=[smem, hbm, hbm, hbm, full(pos.shape), full(kmix.shape), full(vmix.shape), hbm],
+        out_specs=[full((key_heads, rows, LANES)), full((key_heads, SPAN_PAD, LANES)), hbm],
         scratch_shapes=[
             pltpu.VMEM((steps, rows, chunk), BF16),
-            pltpu.VMEM((steps, chunk, qwidth + 2 * width), BF16),
-            pltpu.VMEM((2 * heads, depth), BF16),
-            pltpu.VMEM((rows, qwidth + 2 * width), F32),
-            pltpu.VMEM((rows, 2 * heads), F32),
+            pltpu.VMEM((steps, chunk, 2 * width), BF16),
+            pltpu.VMEM((rows, 2 * width), F32),
             pltpu.VMEM((inner, MORE_UNITS * wide // UNITS), BF16),
-            pltpu.SemaphoreType.DMA((steps, 4)),
-            pltpu.SemaphoreType.DMA((3,)),
+            pltpu.SemaphoreType.DMA((steps, 3)),
+            pltpu.SemaphoreType.DMA((2,)),
         ],
         out_shape=[
-            jax.ShapeDtypeStruct((heads, rows, LANES), BF16),
-            jax.ShapeDtypeStruct((rows, 2 * heads), F32),
             jax.ShapeDtypeStruct((key_heads, rows, LANES), BF16),
             jax.ShapeDtypeStruct((key_heads, SPAN_PAD, LANES), BF16),
             jax.ShapeDtypeStruct((inner, MORE_UNITS * wide // UNITS), BF16),
         ],
         cost_estimate=pl.CostEstimate(
-            flops=2 * rows * depth * (qwidth + 3 * width), transcendentals=0, bytes_accessed=2 * depth * (rows + qwidth)
+            flops=4 * rows * depth * width, transcendentals=0, bytes_accessed=2 * depth * (rows + 2 * width)
         ),
         compiler_params=pltpu.CompilerParams(vmem_limit_bytes=VMEM_LIMIT),
-        name="project",
-    )(part, tokens, query_weight, key_weight, value_weight, gate_rows, pos, kmix, vmix, out_weight)
+        name="project_kv",
+    )(part, tokens, key_weight, value_weight, pos, kmix, vmix, out_weight)
+
+
+def q_kernel(part_ref, tok_ref, wq_ref, gw_ref, q_ref, gate_ref, tok, weight, gate_rows, acc_ref, gacc_ref, sems):
+    heads, rows = q_ref.shape[0], q_ref.shape[1]
+    gates = gate_ref.shape[1]
+    steps, chunk = weight.shape[0], weight.shape[1]
+    start = pl.multiple_of(part_ref[0] * gates, gates)
+    copies = []
+    for i in range(steps):
+        depth = slice(i * chunk, (i + 1) * chunk)
+        copies.append(
+            [
+                pltpu.make_async_copy(tok_ref.at[:, depth], tok.at[i], sems.at[i, 0]),
+                pltpu.make_async_copy(wq_ref.at[depth, :], weight.at[i], sems.at[i, 1]),
+                pltpu.make_async_copy(gw_ref.at[pl.ds(start, gates), depth], gate_rows.at[i], sems.at[i, 2]),
+            ]
+        )
+
+    def step(i):
+        piece = jnp.dot(tok[i], weight[i], preferred_element_type=F32)
+        gpiece = lax.dot_general(tok[i], gate_rows[i], (((1,), (1,)), ((), ())), preferred_element_type=F32)
+        acc_ref[...] = piece if i == 0 else acc_ref[...] + piece
+        gacc_ref[...] = gpiece if i == 0 else gacc_ref[...] + gpiece
+
+    staged(copies, 2, step)
+    lane, inner = lane_iota(rows), lax.rem(row_iota(rows), SB)
+    low_half = lane < HD
+    ext = jnp.where((lane == HD) | (lane - HD > inner), 1.0, 0.0)
+    for h in range(heads):
+        slab = acc_ref[:, (h // 2) * LANES : (h // 2 + 1) * LANES]
+        if h % 2:
+            slab = pltpu.roll(slab, HD, 1)
+        q_ref[h] = jnp.where(low_half, slab, ext).astype(BF16)
+    gate_ref[...] = jax.nn.sigmoid(gacc_ref[...])
+
+
+def project_q(part, tokens, query_weight, gate_rows):
+    rows, depth = tokens.shape
+    qwidth = query_weight.shape[1]
+    heads = qwidth // HD
+    steps = 4
+    chunk = depth // steps
+    hbm = pl.BlockSpec(memory_space=pl.ANY)
+    smem = pl.BlockSpec(memory_space=pltpu.SMEM)
+    full = lambda shape: pl.BlockSpec(shape, lambda i: (0,) * len(shape))
+    return pl.pallas_call(
+        q_kernel,
+        grid=(1,),
+        in_specs=[smem, hbm, hbm, hbm],
+        out_specs=[full((heads, rows, LANES)), full((rows, 2 * heads))],
+        scratch_shapes=[
+            pltpu.VMEM((steps, rows, chunk), BF16),
+            pltpu.VMEM((steps, chunk, qwidth), BF16),
+            pltpu.VMEM((steps, 2 * heads, chunk), BF16),
+            pltpu.VMEM((rows, qwidth), F32),
+            pltpu.VMEM((rows, 2 * heads), F32),
+            pltpu.SemaphoreType.DMA((steps, 3)),
+        ],
+        out_shape=[
+            jax.ShapeDtypeStruct((heads, rows, LANES), BF16),
+            jax.ShapeDtypeStruct((rows, 2 * heads), F32),
+        ],
+        cost_estimate=pl.CostEstimate(
+            flops=3 * rows * depth * qwidth, transcendentals=0, bytes_accessed=2 * depth * (rows + qwidth)
+        ),
+        compiler_params=pltpu.CompilerParams(vmem_limit_bytes=PROJ_LIMIT),
+        name="project_q",
+    )(part, tokens, query_weight, gate_rows)
 
 
 def copy_kernel(from_ref, to_ref):
@@ -216,9 +258,31 @@
         in_specs=[smem, smem, full(kv.shape), full(summaries.shape)],
         out_specs=[full(piece)] * (count - 1),
         out_shape=[jax.ShapeDtypeStruct(piece, BF16)] * (count - 1),
-        compiler_params=pltpu.CompilerParams(vmem_limit_bytes=VMEM_LIMIT),
+        compiler_params=pltpu.CompilerParams(vmem_limit_bytes=SELECT_LIMIT),
         name="select_blocks",
     )(own, requests, kv, summaries)
+
+
+def stage_kernel(q_ref, gate_ref, q_out, gate_out, sems):
+    copies = [pltpu.make_async_copy(q_ref, q_out, sems.at[0]), pltpu.make_async_copy(gate_ref, gate_out, sems.at[1])]
+    for copy in copies:
+        copy.start()
+    for copy in copies:
+        copy.wait()
+
+
+def bring(q, gates):
+    hbm = pl.BlockSpec(memory_space=pl.ANY)
+    vmem = pl.BlockSpec(memory_space=pltpu.VMEM)
+    return pl.pallas_call(
+        stage_kernel,
+        in_specs=[hbm, hbm],
+        out_specs=[vmem, vmem],
+        out_shape=[jax.ShapeDtypeStruct(q.shape, BF16), jax.ShapeDtypeStruct(gates.shape, F32)],
+        scratch_shapes=[pltpu.SemaphoreType.DMA((2,))],
+        compiler_params=pltpu.CompilerParams(vmem_limit_bytes=SELECT_LIMIT),
+        name="stage",
+    )(q, gates)
 
 
 def attn_kernel(count, blocks, *refs):
@@ -376,59 +440,64 @@
     )(half, own, core, table, q, gates, kv, summaries, *received)
 
 
-def product_kernel(starts, near_ref, own_ref, *refs):
-    send_ref, keep_ref = refs[-2:]
-    rows = send_ref.shape[0]
-    step = pl.program_id(0)
-    total = jnp.dot(near_ref[...], own_ref[...], preferred_element_type=F32)
-    if not starts:
-        send_ref[...] = total[:rows].astype(BF16)
-        keep_ref[...] = total[rows:].astype(BF16)
-        return
-    its_ref, piece_refs = refs[0], refs[1:-2]
-
-    def one(piece_ref):
-        both = total + jnp.dot(its_ref[...], piece_ref[...], preferred_element_type=F32)
-        send_ref[...] = both[:rows].astype(BF16)
-        keep_ref[...] = both[rows:].astype(BF16)
-
-    for k, piece_ref in enumerate(piece_refs):
-        inside = step >= starts[k]
-        if k + 1 < len(piece_refs):
-            inside = inside & (step < starts[k + 1])
-        pl.when(inside)(functools.partial(one, piece_ref))
+def product_kernel(first, near_ref, own_ref, send_ref, keep_ref):
+    rows, width = send_ref.shape
+    for at in range(0, width, BLOCK):
+        size = min(BLOCK, width - at)
+        total = jnp.dot(near_ref[...], own_ref[:, first + at : first + at + size], preferred_element_type=F32)
+        send_ref[:, at : at + size] = total[:rows].astype(BF16)
+        keep_ref[:, at : at + size] = total[rows:].astype(BF16)
+
+
+def joint_kernel(near_ref, its_ref, own_ref, a_ref, b_ref, send_ref, keep_ref, other, sems):
+    rows, width = send_ref.shape
+    start = a_ref.shape[1]
+    first = pltpu.make_async_copy(a_ref, other.at[:, :start], sems.at[0])
+    more = pltpu.make_async_copy(b_ref, other.at[:, start:], sems.at[1])
+    first.start()
+    more.start()
+    for at in range(0, width, BLOCK):
+        size = min(BLOCK, width - at)
+        columns = slice(at, at + size)
+        total = jnp.dot(near_ref[...], own_ref[:, columns], preferred_element_type=F32)
+        if at == 0:
+            first.wait()
+        if at == start // BLOCK * BLOCK:
+            more.wait()
+        total += jnp.dot(its_ref[...], other[:, columns], preferred_element_type=F32)
+        send_ref[:, columns] = total[:rows].astype(BF16)
+        keep_ref[:, columns] = total[rows:].astype(BF16)
 
 
 def out_product(near, out_weight, first, units, its=None, pieces=()):
     depth, wide = out_weight.shape
-    unit = wide // UNITS * 3 if units % 3 == 0 else wide // UNITS * units
-    steps = units * (wide // UNITS) // unit
-    offset = first * (wide // UNITS)
-    sizes = [piece.shape[1] // unit for piece in pieces]
-    starts = [sum(sizes[:k]) for k in range(len(sizes))]
+    unit = wide // UNITS
     rows = near.shape[0] // 2
+    width = units * unit
     full = lambda shape: pl.BlockSpec(shape, lambda i: (0,) * len(shape))
-
-    def piece_spec(k):
-        return pl.BlockSpec((depth, unit), lambda i: (0, jnp.clip(i - starts[k], 0, sizes[k] - 1)))
-
-    out = pl.BlockSpec((rows, unit), lambda i: (0, i))
-    args = [near, out_weight] + ([its, *pieces] if pieces else [])
-    specs = [full(near.shape), pl.BlockSpec((pl.Element(depth), pl.Element(unit)), lambda i: (0, pl.multiple_of(offset + i * unit, 2 * LANES)))]
-    if pieces:
-        specs += [full(its.shape), *[piece_spec(k) for k in range(len(pieces))]]
-    return pl.pallas_call(
-        functools.partial(product_kernel, starts),
-        grid=(steps,),
-        in_specs=specs,
-        out_specs=[out, out],
-        out_shape=[jax.ShapeDtypeStruct((rows, steps * unit), BF16)] * 2,
-        cost_estimate=pl.CostEstimate(
-            flops=8 * rows * depth * steps * unit, transcendentals=0, bytes_accessed=4 * depth * steps * unit
-        ),
+    hbm = pl.BlockSpec(memory_space=pl.ANY)
+    vmem = pl.BlockSpec(memory_space=pltpu.VMEM)
+    common = dict(
+        grid=(1,),
+        out_specs=[full((rows, width))] * 2,
+        out_shape=[jax.ShapeDtypeStruct((rows, width), BF16)] * 2,
+        cost_estimate=pl.CostEstimate(flops=8 * rows * depth * width, transcendentals=0, bytes_accessed=4 * depth * width),
         compiler_params=pltpu.CompilerParams(vmem_limit_bytes=PROD_LIMIT),
-        name="out_product",
-    )(*args)
+    )
+    if not pieces:
+        return pl.pallas_call(
+            functools.partial(product_kernel, first * unit),
+            in_specs=[full(near.shape), vmem],
+            name="out_product",
+            **common,
+        )(near, out_weight)
+    return pl.pallas_call(
+        joint_kernel,
+        in_specs=[full(near.shape), full(its.shape), vmem, hbm, hbm],
+        scratch_shapes=[pltpu.VMEM((depth, width), BF16), pltpu.SemaphoreType.DMA((2,))],
+        name="joint_product",
+        **common,
+    )(near, its, out_weight, *pieces)
 
 
 def final_kernel(first, *refs):
@@ -478,23 +547,23 @@
     request = jnp.stack([lowest, highest], axis=-1).reshape(1, count * heads * 2)
     everyone = jnp.where(jnp.arange(count, dtype=jnp.int32)[:, None] == own, request, 0)
     if count & (count - 1) == 0:
-        bit, stage = 1, 0
+        bit = 1
         while bit < count:
             got = lax.ppermute(everyone, "kv", [(i, i ^ bit) for i in range(count)])
             everyone = everyone + got
-            if stage == 0:
+            if 4 * bit == count:
                 chosen = lax.optimization_barrier((chosen, got))[0]
-            bit, stage = 2 * bit, stage + 1
+            bit = 2 * bit
     else:
         everyone = lax.all_gather(request, "kv", axis=0, tiled=True)
 
     cross = [(i, i ^ 2) for i in range(parts)]
     swap = [(i, i ^ 1) for i in range(parts)]
     piece_a = lax.ppermute(first_piece(out_weight), "tp", cross)
-    q, gates, kv, summaries, more = project(
-        part1, tokens, query_weight, key_weight, value_weight, gate_weight.T, summary_pos, key_mixing.T,
-        value_mixing.T, out_weight,
+    kv, summaries, more = project_kv(
+        part1, tokens, key_weight, value_weight, summary_pos, key_mixing.T, value_mixing.T, out_weight
     )
+    q, gates = project_q(part1, tokens, query_weight, gate_weight.T)
     piece_b = lax.ppermute(more, "tp", cross)
 
     pieces = select_blocks(count, own1, everyone, kv, summaries)
@@ -505,6 +574,8 @@
     source = chosen // own_blocks
     place = chosen - source * own_blocks
     match = source[None] == jnp.arange(count, dtype=jnp.int32)[:, None, None, None]
+
+    q, gates = bring(q, gates)
 
     high_at = jnp.sum(jnp.where(match, highest[:, None, :, None], 0), axis=0)
     away = own_blocks + 2 * (own - source - 1) + (place == high_at).astype(jnp.int32)

time: 96.7 us -> 92.1 us (0.952)
  starting transfers between devices: 34.6 us -> 27.8 us
  local copies, waits for them, and re-layouts: 2.57 us -> 6.89 us
  waiting for transfers between devices: 20 us -> 16.3 us
  Pallas kernels: 34.7 us -> 36.6 us
    ppermute x7, starting transfers between devices: 23.2 us -> 16.5 us  [local(): lax.ppermute(pieces[k - 1], 'kv', [(i, i + k) for i in range(count - k)])]
    unnamed x14 -> x26, local copies, waits for them, and re-layouts: 2.31 us -> 6.63 us
    pallas_call x4 -> x6, Pallas kernels: 16.6 us -> 19.8 us  [the longest x1 8.08 us: project_q(): pl.pallas_call(q_kernel, grid=(1,), in_specs=[smem, hbm, hbm, hbm], out_s...]
    ppermute x3, waiting for transfers between devices: 2.32 us -> 0.29 us  [local(): got = lax.ppermute(everyone, 'kv', [(i, i ^ bit) for i in range(count)])]
    pallas_call x1, Pallas kernels: 1.86 us -> 0.69 us  [select_blocks(): pl.pallas_call(functools.partial(select_kernel, count), grid=(1,), in_spe...]
    ppermute x1, waiting for transfers between devices: 2.64 us -> 1.53 us  [local(): its = lax.ppermute(far, 'tp', cross)]
  transfers between devices with their start and end apart: 17 -> 17, of which waited for: 7 -> 5; matrix products, arithmetic and copies ran while one was open for 3% -> 3% of each run, Pallas kernels for 35% -> 39%
where the time goes in v4:
time: 92.1 us; the launch traced here: 91.5 us
  Pallas kernels  36.6 us (40%)
  starting transfers between devices  27.8 us (30%)
  waiting for transfers between devices  16.3 us (18%)
  local copies, waits for them, and re-layouts  6.89 us (7%)
  other arithmetic  3.33 us (4%)
    ppermute x7, starting transfers between devices, local(): lax.ppermute(pieces[k - 1], 'kv', [(i, i + k) for i in range(count - k)])  16.5 us
    ppermute x1, waiting for transfers between devices, local(): lax.ppermute((got.astype(F32) + keep.astype(F32)).astype(BF16), 'tp', cross)  12.3 us
    pallas_call x2, Pallas kernels, attend(): pl.pallas_call(functools.partial(attn_kernel, count, blocks), grid_spec=p...  12.2 us
    pallas_call x1, Pallas kernels, project_q(): pl.pallas_call(q_kernel, grid=(1,), in_specs=[smem, hbm, hbm, hbm], out_s...  8.08 us
    pallas_call x1, Pallas kernels, project_kv(): pl.pallas_call(kv_kernel, grid=(1,), in_specs=[smem, hbm, hbm, hbm, full(...  7.46 us
    ppermute x3, starting transfers between devices, local(): got = lax.ppermute(everyone, 'kv', [(i, i ^ bit) for i in range(count)])  7.17 us
    unnamed x26, local copies, waits for them, and re-layouts  6.63 us
    pallas_call x1, Pallas kernels, out_product(): pl.pallas_call(joint_kernel, in_specs=[full(near.shape), full(its.shape),...  2.47 us
  transfers between devices with their start and end apart: 17, of which 5 were waited for; matrix products, arithmetic and copies ran while one was open for 3% of the time, Pallas kernels for 39%

profile of v4, /device:TPU:0, one launch (start us, length us, event | category | flops | bytes accessed | tf_op | source)
XLA Modules:
  0.0 91.5 jit_solution(4059953053344562881)
XLA Ops:
  1.2 3.0 %collective-permute-start = (s32[8,32]{1,0:T(8,128)S(1)}, s32[8,32]{1,0:T(8,128)S(1)}, u32[]{:S(2)}, u32[]{:S(2)}) collective-permute-start(s32[8,32]{1,0:T(8,128)S(1)} %broadcast_select_fusion.1), channel_id=1, source_target_pairs={{0,4},{4,0},{8,12},{12,8},{16,20},{20,16},{24,28},{28,24},{1,5},{5... | collective-permute-start | bytes 3080 | tf_op jit(solution)/shard_map/ppermute | solution.py:552
  4.2 7.5 %project_kv.1 = (bf16[2,640,128]{2,1,0:T(8,128)(2,1)}, bf16[2,32,128]{2,1,0:T(8,128)(2,1)}, bf16[512,1792]{1,0:T(8,128)(2,1)}) custom-call(s32[1]{0:T(128)} %bitcast.5.part_ref, bf16[640,4096]{1,0:T(8,128)(2,1)} %tok_ref.3, bf16[4096,128]{1,0:T(8,128)(2,1)} %wk_ref.1, bf16[4096,128]{1,0:T(8,128)(2,1)} %wv_ref.1, bf16[32,64]{1,0:T(8,128)(2,1)} %pos_ref.1, ...), custom_call_target="tpu_custom_call" | custom-call | flops 1342177280 | bytes 7340032 | tf_op jit(solution)/shard_map/project_kv/pallas_call | solution.py:124
  11.7 1.6 %collective-permute-start.15 = (bf16[512,1792]{1,0:T(8,128)(2,1)}, bf16[512,1792]{1,0:T(8,128)(2,1)S(1)}, u32[]{:S(2)}, u32[]{:S(2)}) collective-permute-start(bf16[512,1792]{1,0:T(8,128)(2,1)} %get-tuple-element.44), channel_id=1, source_target_pairs={{0,2},{1,3},{2,0},{3,1},{4,6},{5,7},{6,4},{7,5},{8,10},{9,11},{10,... | collective-permute-start | bytes 5505032 | tf_op jit(solution)/shard_map/ppermute | solution.py:567
  13.2 8.1 %project_q.1 = (bf16[8,640,128]{2,1,0:T(8,128)(2,1)}, f32[640,16]{1,0:T(8,128)}) custom-call(s32[1]{0:T(128)} %bitcast.5.part_ref, bf16[640,4096]{1,0:T(8,128)(2,1)} %tok_ref.3, bf16[4096,512]{1,0:T(8,128)(2,1)} %wq_ref.1, bf16[64,4096]{1,0:T(8,128)(2,1)} %bitcast.14), custom_call_target="tpu_custom_call" | custom-call | flops 4026531840 | bytes 9437184 | tf_op jit(solution)/shard_map/project_q/pallas_call | solution.py:193
  21.4 1.6 %collective-permute-start.1 = (s32[8,32]{1,0:T(8,128)S(1)}, s32[8,32]{1,0:T(8,128)S(1)}, u32[]{:S(2)}, u32[]{:S(2)}) collective-permute-start(s32[8,32]{1,0:T(8,128)S(1)} %fusion.3), channel_id=1, source_target_pairs={{0,8},{4,12},{8,0},{12,4},{16,24},{20,28},{24,16},{28,20},{1,9},{5... | collective-permute-start | bytes 3080 | tf_op jit(solution)/shard_map/ppermute | solution.py:552
  23.0 1.9 %first_piece.1 = bf16[512,512]{1,0:T(8,128)(2,1)} custom-call(bf16[512,4096]{1,0:T(8,128)(2,1)} %own_ref.5), custom_call_target="tpu_custom_call" | custom-call | tf_op jit(solution)/shard_map/first_piece/pallas_call | solution.py:226
  26.1 1.0 %copy-done.5 = bf16[8,640,128]{2,1,0:T(8,128)(2,1)} copy-done((bf16[8,640,128]{2,1,0:T(8,128)(2,1)}, bf16[8,640,128]{2,1,0:T(8,128)(2,1)S(1)}, u32[]{:S(2)}) %copy-start.5) | copy-done | bytes 1310744
  28.0 2.6 %collective-permute-start.2 = (s32[8,32]{1,0:T(8,128)S(1)}, s32[8,32]{1,0:T(8,128)S(1)}, u32[]{:S(2)}, u32[]{:S(2)}) collective-permute-start(s32[8,32]{1,0:T(8,128)S(1)} %fusion.4), channel_id=1, source_target_pairs={{0,16},{4,20},{8,24},{12,28},{16,0},{20,4},{24,8},{28,12},{1,17},{... | collective-permute-start | bytes 3080 | tf_op jit(solution)/shard_map/ppermute | solution.py:552
  33.2 2.4 %collective-permute-start.3 = (bf16[2,160,128]{2,1,0:T(8,128)(2,1)S(1)}, bf16[2,160,128]{2,1,0:T(8,128)(2,1)S(1)}, u32[]{:S(2)}, u32[]{:S(2)}) collective-permute-start(bf16[2,160,128]{2,1,0:T(8,128)(2,1)S(1)} %get-tuple-element.33), channel_id=1, source_target_pairs={{0,4},{4,8},{8,12},{12,16},{16,20},{20,24},{24,28},{1,5},{5,9},{9,... | collective-permute-start | bytes 245768 | tf_op jit(solution)/shard_map/ppermute | solution.py:572
  35.6 2.4 %collective-permute-start.4 = (bf16[2,160,128]{2,1,0:T(8,128)(2,1)S(1)}, bf16[2,160,128]{2,1,0:T(8,128)(2,1)S(1)}, u32[]{:S(2)}, u32[]{:S(2)}) collective-permute-start(bf16[2,160,128]{2,1,0:T(8,128)(2,1)S(1)} %get-tuple-element.34), channel_id=1, source_target_pairs={{0,8},{4,12},{8,16},{12,20},{16,24},{20,28},{1,9},{5,13},{9,17},{1... | collective-permute-start | bytes 245768 | tf_op jit(solution)/shard_map/ppermute | solution.py:572
  38.0 5.5 %collective-permute-start.5 = (bf16[2,160,128]{2,1,0:T(8,128)(2,1)S(1)}, bf16[2,160,128]{2,1,0:T(8,128)(2,1)S(1)}, u32[]{:S(2)}, u32[]{:S(2)}) collective-permute-start(bf16[2,160,128]{2,1,0:T(8,128)(2,1)S(1)} %get-tuple-element.35), channel_id=1, source_target_pairs={{0,12},{4,16},{8,20},{12,24},{16,28},{1,13},{5,17},{9,21},{13,25},... | collective-permute-start | bytes 245768 | tf_op jit(solution)/shard_map/ppermute | solution.py:572
  43.9 1.3 %collective-permute-start.6 = (bf16[2,160,128]{2,1,0:T(8,128)(2,1)S(1)}, bf16[2,160,128]{2,1,0:T(8,128)(2,1)S(1)}, u32[]{:S(2)}, u32[]{:S(2)}) collective-permute-start(bf16[2,160,128]{2,1,0:T(8,128)(2,1)S(1)} %get-tuple-element.36), channel_id=1, source_target_pairs={{0,16},{4,20},{8,24},{12,28},{1,17},{5,21},{9,25},{13,29},{2,18},{... | collective-permute-start | bytes 245768 | tf_op jit(solution)/shard_map/ppermute | solution.py:572
  45.2 1.3 %collective-permute-start.7 = (bf16[2,160,128]{2,1,0:T(8,128)(2,1)S(1)}, bf16[2,160,128]{2,1,0:T(8,128)(2,1)S(1)}, u32[]{:S(2)}, u32[]{:S(2)}) collective-permute-start(bf16[2,160,128]{2,1,0:T(8,128)(2,1)S(1)} %get-tuple-element.37), channel_id=1, source_target_pairs={{0,20},{4,24},{8,28},{1,21},{5,25},{9,29},{2,22},{6,26},{10,30},{3... | collective-permute-start | bytes 245768 | tf_op jit(solution)/shard_map/ppermute | solution.py:572
  46.5 1.3 %collective-permute-start.8 = (bf16[2,160,128]{2,1,0:T(8,128)(2,1)S(1)}, bf16[2,160,128]{2,1,0:T(8,128)(2,1)S(1)}, u32[]{:S(2)}, u32[]{:S(2)}) collective-permute-start(bf16[2,160,128]{2,1,0:T(8,128)(2,1)S(1)} %get-tuple-element.38), channel_id=1, source_target_pairs={{0,24},{4,28},{1,25},{5,29},{2,26},{6,30},{3,27},{7,31}} | collective-permute-start | bytes 245768 | tf_op jit(solution)/shard_map/ppermute | solution.py:572
  47.8 2.4 %collective-permute-start.9 = (bf16[2,160,128]{2,1,0:T(8,128)(2,1)S(1)}, bf16[2,160,128]{2,1,0:T(8,128)(2,1)S(1)}, u32[]{:S(2)}, u32[]{:S(2)}) collective-permute-start(bf16[2,160,128]{2,1,0:T(8,128)(2,1)S(1)} %get-tuple-element.39), channel_id=1, source_target_pairs={{0,28},{1,29},{2,30},{3,31}} | collective-permute-start | bytes 245768 | tf_op jit(solution)/shard_map/ppermute | solution.py:572
  50.9 1.2 %collective-permute-done.9.refs_14_ = bf16[2,160,128]{2,1,0:T(8,128)(2,1)S(1)} collective-permute-done((bf16[2,160,128]{2,1,0:T(8,128)(2,1)S(1)}, bf16[2,160,128]{2,1,0:T(8,128)(2,1)S(1)}, u32[]{:S(2)}, u32[]{:S(2)}) %collective-permute-start.9) | collective-permute-done | bytes 81952 | tf_op jit(solution)/shard_map/ppermute | solution.py:572
  52.1 1.3 %copy-done.6 = bf16[8,640,128]{2,1,0:T(8,128)(2,1)S(1)} copy-done((bf16[8,640,128]{2,1,0:T(8,128)(2,1)S(1)}, bf16[8,640,128]{2,1,0:T(8,128)(2,1)}, u32[]{:S(2)}) %copy-start.6) | copy-done | bytes 1310744
  54.4 6.1 %attend.3.near_ref = bf16[320,512]{1,0:T(8,128)(2,1)S(1)} custom-call(s32[1]{0:T(128)} %bitcast.9.refs_0_, s32[1]{0:T(128)} %bitcast.1.own_ref.refs_1_, s32[1]{0:T(128)} %bitcast.2.refs_2_, s32[10,32]{1,0:T(8,128)S(1)} %select_n.60.refs_3_, bf16[8,640,128]{2,1,0:T(8,128)(2,1)S(1)} %copy-done.6, f32[640,16]{1,0:T(8,128)S(1)} %copy-done.8, ...), custom_call_target="tpu_custom_call" | custom-call | flops 1677721600 | bytes 655360 | tf_op jit(solution)/shard_map/attend/pallas_call | solution.py:409
  63.5 6.1 %attend.2.near_ref = bf16[320,512]{1,0:T(8,128)(2,1)S(1)} custom-call(s32[1]{0:T(128)} %bitcast.refs_0_, s32[1]{0:T(128)} %bitcast.1.own_ref.refs_1_, s32[1]{0:T(128)} %bitcast.2.refs_2_, s32[10,32]{1,0:T(8,128)S(1)} %select_n.60.refs_3_, bf16[8,640,128]{2,1,0:T(8,128)(2,1)S(1)} %copy-done.6, f32[640,16]{1,0:T(8,128)S(1)} %copy-done.9, ...), custom_call_target="tpu_custom_call" | custom-call | flops 1677721600 | bytes 655360 | tf_op jit(solution)/shard_map/attend/pallas_call | solution.py:409
  70.6 1.5 %collective-permute-done.13.its_ref = bf16[320,512]{1,0:T(8,128)(2,1)S(1)} collective-permute-done((bf16[320,512]{1,0:T(8,128)(2,1)S(1)}, bf16[320,512]{1,0:T(8,128)(2,1)S(1)}, u32[]{:S(2)}, u32[]{:S(2)}) %collective-permute-start.13) | collective-permute-done | bytes 327712 | tf_op jit(solution)/shard_map/ppermute | solution.py:605
  72.1 2.5 %joint_product.1 = (bf16[160,2304]{1,0:T(8,128)(2,1)S(1)}, bf16[160,2304]{1,0:T(8,128)(2,1)S(1)}) custom-call(bf16[320,512]{1,0:T(8,128)(2,1)S(1)} %attend.2.near_ref, bf16[320,512]{1,0:T(8,128)(2,1)S(1)} %collective-permute-done.13.its_ref, bf16[512,4096]{1,0:T(8,128)(2,1)S(1)} %copy-done, bf16[512,512]{1,0:T(8,128)(2,1)S(1)} %collective-permute-done.14.a_ref, ...), custom_call_target="tpu_custom_call" | custom-call | flops 1509949440 | bytes 4718592 | tf_op jit(solution)/shard_map/joint_product/pallas_call | solution.py:494
  74.8 1.1 %collective-permute-start.12 = (bf16[160,1792]{1,0:T(8,128)(2,1)S(1)}, bf16[160,1792]{1,0:T(8,128)(2,1)S(1)}, u32[]{:S(2)}, u32[]{:S(2)}) collective-permute-start(bf16[160,1792]{1,0:T(8,128)(2,1)S(1)} %add_convert_fusion), channel_id=1, source_target_pairs={{0,2},{1,3},{2,0},{3,1},{4,6},{5,7},{6,4},{7,5},{8,10},{9,11},{10,... | collective-permute-start | bytes 1720328 | tf_op jit(solution)/shard_map/ppermute | solution.py:608
  76.9 1.0 %final_sum.2.refs_3_ = bf16[160,4096]{1,0:T(8,128)(2,1)} custom-call(bf16[160,2304]{1,0:T(8,128)(2,1)S(1)} %collective-permute-done.16.refs_0_, bf16[160,2304]{1,0:T(8,128)(2,1)S(1)} %get-tuple-element.46.refs_1_), custom_call_target="tpu_custom_call" | custom-call | tf_op jit(solution)/shard_map/final_sum/pallas_call | solution.py:520
  78.0 12.3 %collective-permute-done.12.refs_2_ = bf16[160,1792]{1,0:T(8,128)(2,1)S(1)} collective-permute-done((bf16[160,1792]{1,0:T(8,128)(2,1)S(1)}, bf16[160,1792]{1,0:T(8,128)(2,1)S(1)}, u32[]{:S(2)}, u32[]{:S(2)}) %collective-permute-start.12) | collective-permute-done | bytes 573472 | tf_op jit(solution)/shard_map/ppermute | solution.py:608
  (70 shorter events, 14.1 us)
Async XLA Ops:
  1.2 20.1 %collective-permute-start = (s32[8,32]{1,0:T(8,128)S(1)}, s32[8,32]{1,0:T(8,128)S(1)}, u32[]{:S(2)}, u32[]{:S(2)}) collective-permute-start(s32[8,32]{1,0:T(8,128)S(1)} %broadcast_select_fusion.1), channel_id=1, source_target_pairs={{0,4},{4,0},{8,12},{12,8},{16,20},{20,16},{24,28},{28,24},{1,5},{5... | collective-permute-start | bytes 3080 | tf_op jit(solution)/shard_map/ppermute | solution.py:552
  11.7 60.5 %collective-permute-start.15 = (bf16[512,1792]{1,0:T(8,128)(2,1)}, bf16[512,1792]{1,0:T(8,128)(2,1)S(1)}, u32[]{:S(2)}, u32[]{:S(2)}) collective-permute-start(bf16[512,1792]{1,0:T(8,128)(2,1)} %get-tuple-element.44), channel_id=1, source_target_pairs={{0,2},{1,3},{2,0},{3,1},{4,6},{5,7},{6,4},{7,5},{8,10},{9,11},{10,... | collective-permute-start | bytes 5505032 | tf_op jit(solution)/shard_map/ppermute | solution.py:567
  21.4 6.5 %collective-permute-start.1 = (s32[8,32]{1,0:T(8,128)S(1)}, s32[8,32]{1,0:T(8,128)S(1)}, u32[]{:S(2)}, u32[]{:S(2)}) collective-permute-start(s32[8,32]{1,0:T(8,128)S(1)} %fusion.3), channel_id=1, source_target_pairs={{0,8},{4,12},{8,0},{12,4},{16,24},{20,28},{24,16},{28,20},{1,9},{5... | collective-permute-start | bytes 3080 | tf_op jit(solution)/shard_map/ppermute | solution.py:552
  23.0 1.9 %copy-start.1 = (bf16[8,640,128]{2,1,0:T(8,128)(2,1)S(1)}, bf16[8,640,128]{2,1,0:T(8,128)(2,1)}, u32[]{:S(2)}) copy-start(bf16[8,640,128]{2,1,0:T(8,128)(2,1)} %get-tuple-element.27.q_ref) | copy-start | bytes 3932164
  23.0 7.6 %copy-start.12 = (s32[10,2,16]{2,1,0:T(2,128)S(1)}, s32[10,2,16]{2,1,0:T(2,128)}, u32[]{:S(2)}) copy-start(s32[10,2,16]{2,1,0:T(2,128)} %param.19) | copy-start | bytes 3844
  23.0 9.5 %copy-start.4 = (bf16[2,32,128]{2,1,0:T(8,128)(2,1)S(1)}, bf16[2,32,128]{2,1,0:T(8,128)(2,1)}, u32[]{:S(2)}) copy-start(bf16[2,32,128]{2,1,0:T(8,128)(2,1)} %get-tuple-element.32.sm_ref.refs_7_) | copy-start | bytes 49156
  24.9 7.6 %copy-start.2 = (bf16[2,640,128]{2,1,0:T(8,128)(2,1)S(1)}, bf16[2,640,128]{2,1,0:T(8,128)(2,1)}, u32[]{:S(2)}) copy-start(bf16[2,640,128]{2,1,0:T(8,128)(2,1)} %get-tuple-element.31.kv_ref.refs_6_) | copy-start | bytes 983044
  28.0 4.5 %collective-permute-start.2 = (s32[8,32]{1,0:T(8,128)S(1)}, s32[8,32]{1,0:T(8,128)S(1)}, u32[]{:S(2)}, u32[]{:S(2)}) collective-permute-start(s32[8,32]{1,0:T(8,128)S(1)} %fusion.4), channel_id=1, source_target_pairs={{0,16},{4,20},{8,24},{12,28},{16,0},{20,4},{24,8},{28,12},{1,17},{... | collective-permute-start | bytes 3080 | tf_op jit(solution)/shard_map/ppermute | solution.py:552
  33.2 12.0 %collective-permute-start.3 = (bf16[2,160,128]{2,1,0:T(8,128)(2,1)S(1)}, bf16[2,160,128]{2,1,0:T(8,128)(2,1)S(1)}, u32[]{:S(2)}, u32[]{:S(2)}) collective-permute-start(bf16[2,160,128]{2,1,0:T(8,128)(2,1)S(1)} %get-tuple-element.33), channel_id=1, source_target_pairs={{0,4},{4,8},{8,12},{12,16},{16,20},{20,24},{24,28},{1,5},{5,9},{9,... | collective-permute-start | bytes 245768 | tf_op jit(solution)/shard_map/ppermute | solution.py:572
  35.6 10.9 %collective-permute-start.4 = (bf16[2,160,128]{2,1,0:T(8,128)(2,1)S(1)}, bf16[2,160,128]{2,1,0:T(8,128)(2,1)S(1)}, u32[]{:S(2)}, u32[]{:S(2)}) collective-permute-start(bf16[2,160,128]{2,1,0:T(8,128)(2,1)S(1)} %get-tuple-element.34), channel_id=1, source_target_pairs={{0,8},{4,12},{8,16},{12,20},{16,24},{20,28},{1,9},{5,13},{9,17},{1... | collective-permute-start | bytes 245768 | tf_op jit(solution)/shard_map/ppermute | solution.py:572
  38.0 9.8 %collective-permute-start.5 = (bf16[2,160,128]{2,1,0:T(8,128)(2,1)S(1)}, bf16[2,160,128]{2,1,0:T(8,128)(2,1)S(1)}, u32[]{:S(2)}, u32[]{:S(2)}) collective-permute-start(bf16[2,160,128]{2,1,0:T(8,128)(2,1)S(1)} %get-tuple-element.35), channel_id=1, source_target_pairs={{0,12},{4,16},{8,20},{12,24},{16,28},{1,13},{5,17},{9,21},{13,25},... | collective-permute-start | bytes 245768 | tf_op jit(solution)/shard_map/ppermute | solution.py:572
  43.9 6.5 %collective-permute-start.6 = (bf16[2,160,128]{2,1,0:T(8,128)(2,1)S(1)}, bf16[2,160,128]{2,1,0:T(8,128)(2,1)S(1)}, u32[]{:S(2)}, u32[]{:S(2)}) collective-permute-start(bf16[2,160,128]{2,1,0:T(8,128)(2,1)S(1)} %get-tuple-element.36), channel_id=1, source_target_pairs={{0,16},{4,20},{8,24},{12,28},{1,17},{5,21},{9,25},{13,29},{2,18},{... | collective-permute-start | bytes 245768 | tf_op jit(solution)/shard_map/ppermute | solution.py:572
  45.2 5.7 %collective-permute-start.7 = (bf16[2,160,128]{2,1,0:T(8,128)(2,1)S(1)}, bf16[2,160,128]{2,1,0:T(8,128)(2,1)S(1)}, u32[]{:S(2)}, u32[]{:S(2)}) collective-permute-start(bf16[2,160,128]{2,1,0:T(8,128)(2,1)S(1)} %get-tuple-element.37), channel_id=1, source_target_pairs={{0,20},{4,24},{8,28},{1,21},{5,25},{9,29},{2,22},{6,26},{10,30},{3... | collective-permute-start | bytes 245768 | tf_op jit(solution)/shard_map/ppermute | solution.py:572
  46.5 4.4 %collective-permute-start.8 = (bf16[2,160,128]{2,1,0:T(8,128)(2,1)S(1)}, bf16[2,160,128]{2,1,0:T(8,128)(2,1)S(1)}, u32[]{:S(2)}, u32[]{:S(2)}) collective-permute-start(bf16[2,160,128]{2,1,0:T(8,128)(2,1)S(1)} %get-tuple-element.38), channel_id=1, source_target_pairs={{0,24},{4,28},{1,25},{5,29},{2,26},{6,30},{3,27},{7,31}} | collective-permute-start | bytes 245768 | tf_op jit(solution)/shard_map/ppermute | solution.py:572
  47.8 4.3 %collective-permute-start.9 = (bf16[2,160,128]{2,1,0:T(8,128)(2,1)S(1)}, bf16[2,160,128]{2,1,0:T(8,128)(2,1)S(1)}, u32[]{:S(2)}, u32[]{:S(2)}) collective-permute-start(bf16[2,160,128]{2,1,0:T(8,128)(2,1)S(1)} %get-tuple-element.39), channel_id=1, source_target_pairs={{0,28},{1,29},{2,30},{3,31}} | collective-permute-start | bytes 245768 | tf_op jit(solution)/shard_map/ppermute | solution.py:572
  50.3 21.8 %collective-permute-start.14 = (bf16[512,512]{1,0:T(8,128)(2,1)}, bf16[512,512]{1,0:T(8,128)(2,1)S(1)}, u32[]{:S(2)}, u32[]{:S(2)}) collective-permute-start(bf16[512,512]{1,0:T(8,128)(2,1)} %first_piece.1), channel_id=1, source_target_pairs={{0,2},{1,3},{2,0},{3,1},{4,6},{5,7},{6,4},{7,5},{8,10},{9,11},{10,... | collective-permute-start | bytes 1572872 | tf_op jit(solution)/shard_map/ppermute | solution.py:562
  52.1 1.3 %copy-start.6 = (bf16[8,640,128]{2,1,0:T(8,128)(2,1)S(1)}, bf16[8,640,128]{2,1,0:T(8,128)(2,1)}, u32[]{:S(2)}) copy-start(bf16[8,640,128]{2,1,0:T(8,128)(2,1)} %copy-done.5) | copy-start | bytes 3932164
  54.4 6.8 %copy-start = (bf16[512,4096]{1,0:T(8,128)(2,1)S(1)}, bf16[512,4096]{1,0:T(8,128)(2,1)}, u32[]{:S(2)}) copy-start(bf16[512,4096]{1,0:T(8,128)(2,1)} %own_ref.5) | copy-start | bytes 12582916
  61.2 1.5 %copy-start.9 = (f32[640,16]{1,0:T(8,128)S(1)}, f32[640,16]{1,0:T(8,128)}, u32[]{:S(2)}) copy-start(f32[640,16]{1,0:T(8,128)} %copy-done.7) | copy-start | bytes 122884
  61.9 12.8 %collective-permute-start.11 = (bf16[160,1792]{1,0:T(8,128)(2,1)S(1)}, bf16[160,1792]{1,0:T(8,128)(2,1)S(1)}, u32[]{:S(2)}, u32[]{:S(2)}) collective-permute-start(bf16[160,1792]{1,0:T(8,128)(2,1)S(1)} %get-tuple-element.42), channel_id=1, source_target_pairs={{0,1},{1,0},{2,3},{3,2},{4,5},{5,4},{6,7},{7,6},{8,9},{9,8},{10,11... | collective-permute-start | bytes 1720328 | tf_op jit(solution)/shard_map/ppermute | solution.py:607
  62.0 10.1 %collective-permute-start.13 = (bf16[320,512]{1,0:T(8,128)(2,1)S(1)}, bf16[320,512]{1,0:T(8,128)(2,1)S(1)}, u32[]{:S(2)}, u32[]{:S(2)}) collective-permute-start(bf16[320,512]{1,0:T(8,128)(2,1)S(1)} %attend.3.near_ref), channel_id=1, source_target_pairs={{0,2},{1,3},{2,0},{3,1},{4,6},{5,7},{6,4},{7,5},{8,10},{9,11},{10,... | collective-permute-start | bytes 983048 | tf_op jit(solution)/shard_map/ppermute | solution.py:605
  70.4 7.5 %collective-permute-start.10 = (bf16[160,1792]{1,0:T(8,128)(2,1)S(1)}, bf16[160,1792]{1,0:T(8,128)(2,1)S(1)}, u32[]{:S(2)}, u32[]{:S(2)}) collective-permute-start(bf16[160,1792]{1,0:T(8,128)(2,1)S(1)} %get-tuple-element.40), channel_id=1, source_target_pairs={{0,1},{1,0},{2,3},{3,2},{4,5},{5,4},{6,7},{7,6},{8,9},{9,8},{10,11... | collective-permute-start | bytes 1720328 | tf_op jit(solution)/shard_map/ppermute | solution.py:613
  74.6 2.3 %collective-permute-start.16 = (bf16[160,2304]{1,0:T(8,128)(2,1)S(1)}, bf16[160,2304]{1,0:T(8,128)(2,1)S(1)}, u32[]{:S(2)}, u32[]{:S(2)}) collective-permute-start(bf16[160,2304]{1,0:T(8,128)(2,1)S(1)} %get-tuple-element.45), channel_id=1, source_target_pairs={{0,1},{1,0},{2,3},{3,2},{4,5},{5,4},{6,7},{7,6},{8,9},{9,8},{10,11... | collective-permute-start | bytes 2211848 | tf_op jit(solution)/shard_map/ppermute | solution.py:611
  74.8 15.4 %collective-permute-start.12 = (bf16[160,1792]{1,0:T(8,128)(2,1)S(1)}, bf16[160,1792]{1,0:T(8,128)(2,1)S(1)}, u32[]{:S(2)}, u32[]{:S(2)}) collective-permute-start(bf16[160,1792]{1,0:T(8,128)(2,1)S(1)} %add_convert_fusion), channel_id=1, source_target_pairs={{0,2},{1,3},{2,0},{3,1},{4,6},{5,7},{6,4},{7,5},{8,10},{9,11},{10,... | collective-permute-start | bytes 1720328 | tf_op jit(solution)/shard_map/ppermute | solution.py:608
  (6 other events, 5.3 us)
